TPU v7x, 128 devices: a whole 4x4x4 slice. The times are simulated.
128 devices in a mesh: sp: 16 (over z, y), tp: 8 (over x, core).
Axes of the slice: x: 4, y: 4, z: 4, core: 2. Of those that a mesh axis runs over, the one named last changes fastest.
Arguments:
- queries: bfloat16 [16384, 1024], P('sp', 'tp'), may hold values from -6 to 6
- keys: bfloat16 [16384, 1024], P('sp', 'tp'), may hold values from -6 to 6
- values: bfloat16 [16384, 1024], P('sp', 'tp'), may hold values from -6 to 6
- cum_gates: float32 [16384, 16], P('sp', 'tp'), may hold values from -2050 to 0, as said below
- doc_ids: int32 [16384], P('sp'), may hold values from 0 to 1, never falling along the last dimension, each value on 1 to 12288 neighbouring positions
- residual: bfloat16 [16384, 2048], P('sp', 'tp'), may hold values from -100 to 100
- w_out: bfloat16 [1024, 2048], P('tp'), may hold values from -0.1875 to 0.1875
- norm_gain: bfloat16 [2048], P('tp'), may hold values from 0.099609375 to 1.8984375
- w_up: bfloat16 [2048, 8192], P('sp', 'tp'), may hold values from -0.125 to 0.125
- w_down: bfloat16 [8192, 2048], P('tp', 'sp'), may hold values from -0.0625 to 0.0625
Outputs:
- output: bfloat16 [16384, 2048], P('sp', 'tp')
Inputs may be any that keep to these rules, and one draw needn't show every extreme that they name: `cum_gates`: along positions each head's values never rise. `doc_ids`: document numbers never fall along positions; a document holds 1 to three quarters of 16384 positions.
All inputs are finite; a program needn't handle non-finite values.
Results may differ from a plain program's by a relative error of at most 0.015.
Values may be sent and summed in bfloat16 or wider, within the bound.
No kernel may reach another device: no remote copies, remote signals or barrier semaphores. Data moves between devices by JAX's collectives and lax.ppermute only.
A program may use at most 128 MiB of HBM per device.

v0:
```python
import math

import jax
import jax.numpy as jnp
from jax import lax
from jax.sharding import PartitionSpec as P

D = 2048
HD = 64


eps = 1e-06
far_below = -1e30


def gather_turned(arrays, axis, dims):
    turned = [jnp.moveaxis(a, dim, 0) for a, dim in zip(arrays, dims)]
    widths = [t[0].size for t in turned]
    both = jnp.concatenate([t.reshape(-1, w) for t, w in zip(turned, widths)], axis=1)
    whole = lax.all_gather(both, axis, axis=0, tiled=True)
    parts = jnp.split(whole, [sum(widths[:k]) for k in range(1, len(widths))], axis=1)
    return tuple(
        (
            jnp.moveaxis(b.reshape(-1, *t.shape[1:]), 0, dim)
            for b, t, dim in zip(parts, turned, dims)
        )
    )


def joined_along(parts, dim):
    dims = list(parts.shape[1:])
    dims[dim] *= parts.shape[0]
    return jnp.moveaxis(parts, 0, dim).reshape(dims)


def copy_for_each(value, axis):
    peers = lax.axis_size(axis)
    return lax.all_to_all(
        jnp.broadcast_to(value[None], (peers, *value.shape)), axis, 0, 0, tiled=True
    )


def gather_directly(value, axis, dim):
    return joined_along(copy_for_each(value, axis), dim)


def side_by_side(arrays, axis, dim, along):
    both = jnp.concatenate(arrays, axis=along)
    whole, at, outs = (lax.all_gather(both, axis, axis=dim, tiled=True), 0, [])
    for a in arrays:
        outs.append(lax.slice_in_dim(whole, at, at + a.shape[along], axis=along))
        at += a.shape[along]
    return tuple(outs)


def taken_together(value, axis):
    everything = copy_for_each(value, axis)
    return jnp.sum(everything, axis=0)


def attend_span(state_carry, context, key_blk, value_blk, document_block, gate_blk, key_start):
    queries_three, gate_rows, doc_rows, q_pos = context
    running_max, weight_sum, accumulated = state_carry
    key_span = key_blk.shape[0]
    head_count = queries_three.shape[1]
    key_three = key_blk.reshape(key_span, head_count, HD)
    value_three = value_blk.reshape(key_span, head_count, HD)
    key_pos = key_start + jnp.arange(key_span, dtype=jnp.int32)
    scores = jnp.einsum(
        "qhd,khd->hqk", queries_three, key_three, preferred_element_type=jnp.float32
    ) * HD ** (-0.5)
    scores = scores + gate_rows[:, :, None] - gate_blk[:, None, :]
    visible = (
        (key_pos[None, :] <= q_pos[:, None]) & (document_block[None, :] == doc_rows[:, None])
    )[None]
    masked = jnp.where(visible, scores, far_below)
    new_max = jnp.maximum(running_max, jnp.max(masked, axis=-1))
    weights = jnp.where(visible, jnp.exp(masked - new_max[..., None]), 0.0)
    shrink = jnp.exp(running_max - new_max)
    weight_sum = weight_sum * shrink + jnp.sum(weights, axis=-1)
    product = jnp.einsum(
        "hqk,khd->hqd",
        weights.astype(jnp.bfloat16),
        value_three,
        preferred_element_type=jnp.float32,
    )
    accumulated = accumulated * shrink[..., None] + product
    return (new_max, weight_sum, accumulated)


def fold_piece(state_carry, context, shard_piece, gates_t):
    key_piece, value_piece, doc_piece = shard_piece
    piece_rows = key_piece.shape[0]
    key_span = math.gcd(piece_rows, 1024)
    q_last = context[3][-1]
    doc_first = context[2][0]

    def key_step(step_index, inner_carry):
        offset = step_index * key_span
        key_blk = lax.dynamic_slice_in_dim(key_piece, offset, key_span, 0)
        value_blk = lax.dynamic_slice_in_dim(value_piece, offset, key_span, 0)
        document_block = lax.dynamic_slice_in_dim(doc_piece, offset, key_span, 0)
        gate_blk = lax.dynamic_slice_in_dim(gates_t, jnp.maximum(offset, 0), key_span, 1)
        live = (offset >= 0) & (offset <= q_last) & (document_block[-1] >= doc_first)

        def compute(given):
            return attend_span(given, context, key_blk, value_blk, document_block, gate_blk, offset)

        def passing(given):
            return given

        return lax.cond(live, compute, passing, inner_carry)

    return lax.fori_loop(0, piece_rows // key_span, key_step, state_carry)


def body(queries, keys, values, cum_gates, doc_ids, residual, w_out, norm_gain, w_up, w_down):
    tok_rows = queries.shape[0]
    head_cols = queries.shape[1]
    head_count = head_cols // HD
    row_start = lax.axis_index("sp") * tok_rows
    up_whole, down_whole = gather_turned((w_up, w_down), "sp", (0, 1))
    proj_cols = lax.all_to_all(w_out, "tp", split_axis=1, concat_axis=0, tiled=True)
    gates_t = jnp.transpose(gather_directly(cum_gates, "sp", 0))
    q_pos = row_start + jnp.arange(tok_rows, dtype=jnp.int32)
    context = (queries.reshape(tok_rows, head_count, HD), jnp.transpose(cum_gates), doc_ids, q_pos)
    start_carry = (
        jnp.full((head_count, tok_rows), far_below, jnp.float32),
        jnp.zeros((head_count, tok_rows), jnp.float32),
        jnp.zeros((head_count, tok_rows, HD), jnp.float32),
    )
    running_max, weight_sum, accumulated = fold_piece(
        start_carry,
        context,
        (
            *side_by_side((keys, values), "sp", 0, 1),
            lax.all_gather(doc_ids, "sp", axis=0, tiled=True),
        ),
        gates_t,
    )
    attended = (accumulated / weight_sum[..., None]).astype(jnp.bfloat16)
    attended = jnp.transpose(attended, (1, 0, 2)).reshape(tok_rows, head_cols)
    group_total = lax.axis_size("tp")
    attended_whole = gather_directly(attended, "tp", 1)
    attended_groups = jnp.transpose(
        attended_whole.reshape(tok_rows, group_total, head_cols), (1, 0, 2)
    )
    proj_groups = proj_cols.reshape(group_total, head_cols, proj_cols.shape[1])
    group_terms = jnp.einsum(
        "gtc,gcd->gtd", attended_groups, proj_groups, preferred_element_type=jnp.float32
    )
    head_mixed = jnp.sum(group_terms.astype(jnp.bfloat16).astype(jnp.float32), axis=0)
    middle = (residual.astype(jnp.float32) + head_mixed).astype(jnp.bfloat16)
    middle_wide = middle.astype(jnp.float32)
    row_squares = taken_together(jnp.sum(middle_wide * middle_wide, axis=-1), "tp")
    scaled = middle_wide * lax.rsqrt(row_squares[:, None] / D + eps)
    normed = (scaled * norm_gain.astype(jnp.float32)).astype(jnp.bfloat16)
    features = lax.all_gather(normed, "tp", axis=1, tiled=True)
    up_proj = jnp.dot(features, up_whole, preferred_element_type=jnp.float32)
    hidden = jnp.square(jax.nn.relu(up_proj)).astype(jnp.bfloat16)
    down_terms = jnp.dot(hidden, down_whole, preferred_element_type=jnp.float32)
    feed = lax.psum_scatter(
        down_terms.astype(jnp.bfloat16), "tp", scatter_dimension=1, tiled=True
    ).astype(jnp.float32)
    return (middle_wide + feed).astype(jnp.bfloat16)


def solution(mesh):
    in_specs = (
        P("sp", "tp"),
        P("sp", "tp"),
        P("sp", "tp"),
        P("sp", "tp"),
        P("sp"),
        P("sp", "tp"),
        P("tp", None),
        P("tp"),
        P("sp", "tp"),
        P("tp", "sp"),
    )
    out_specs = P("sp", "tp")
    return jax.shard_map(body, mesh=mesh, in_specs=in_specs, out_specs=out_specs, check_vma=False)
```

profile of v0, /device:TPU:25, one launch (start us, length us, event | category | flops | bytes accessed | tf_op | source)
XLA Modules:
  0.0 375.0 jit_solution(2995979391306129125)
XLA Ops:
  6.5 1.1 copy.43
  7.6 1.1 copy.42
  8.7 0.8 pad_maximum_fusion
  9.6 1.1 copy.49
  10.8 1.8 pad_maximum_fusion.1
  12.6 1.4 broadcast_in_dim.65
  14.0 7.6 %all-to-all-start = ((f32[16,1024,2]{1,2,0:T(2,128)}), f32[16,1024,2]{1,2,0:T(2,128)S(1)}, u32[]{:S(2)}, u32[]{:S(2)}) async-start(f32[16,1024,2]{1,2,0:T(2,128)} %broadcast_in_dim.65), calls=%async_computation | async-start | bytes 262144 | tf_op jit(solution)/shard_map/all_to_all | solution.py:38
  21.6 0.7 slice.19
  22.3 1.2 slice.20
  23.5 1.1 copy.44
  24.6 1.3 copy.46
  25.9 1.0 copy.47
  27.0 18.5 %all_gather.12 = s32[16384]{0:T(1024)S(1)} all-gather(s32[1024]{0:T(1024)} %param.18), channel_id=1, replica_groups=mesh['sp'=16,'tp'=8] {'sp'}, dimensions={0}, use_global_device_ids=true | all-gather | bytes 69632 | tf_op jit(solution)/shard_map/all_gather | solution.py:137
  45.4 10.5 %all-to-all-start.2 = ((bf16[128,8,256]{2,0,1:T(8,128)(2,1)}), bf16[128,8,256]{2,0,1:T(8,128)(2,1)S(1)}, u32[]{:S(2)}, u32[]{:S(2)}) async-start(bf16[128,8,256]{2,0,1:T(8,128)(2,1)} %copy.47), calls=%async_computation.2 | async-start | bytes 1048576 | tf_op jit(solution)/shard_map/all_to_all | solution.py:123
  56.0 27.4 %all-gather.4.cloned.1.call-done = bf16[16384,256]{0,1:T(8,128)(2,1)} async-done(((bf16[1024,256]{0,1:T(8,128)(2,1)}), bf16[16384,256]{0,1:T(8,128)(2,1)}) %all-gather.4.cloned.1.call-update) | async-done | bytes 8388624 | tf_op jit(solution)/shard_map/all_gather | solution.py:49
  83.4 5.8 %fusion.28 = (bf16[16384,128]{0,1:T(8,128)(2,1)}, bf16[16384,128]{0,1:T(8,128)(2,1)}) fusion(bf16[16384,256]{0,1:T(8,128)(2,1)} %all-gather.4.cloned.1.call-done), kind=kLoop, calls=%fused_computation.41 | loop fusion | bytes 16777216 | tf_op jit(solution)/shard_map/slice | solution.py:51
  89.3 84.8 %while.18 = (s32[]{:T(128)}, f32[2,1024]{1,0:T(2,128)S(1)}, f32[2,1024]{1,0:T(2,128)S(1)}, f32[2,1024,64]{1,2,0:T(8,128)S(1)}, s32[]{:T(128)}, /*index=5*/s32[16...) while((s32[]{:T(128)}, f32[2,1024]{1,0:T(2,128)S(1)}, ...), condition=%wide.region_5.6_spmd.clone, body=%wide.region_0.5_spmd.clone.sunk | while | flops 580130816 | bytes 32481744 | solution.py:114
  90.1 0.6 slice.29
  91.9 11.0 %conditional.3 = ((f32[2,1024]{1,0:T(2,128)S(1)}, f32[2,1024]{1,0:T(2,128)S(1)}, f32[2,1024,64]{1,2,0:T(8,128)S(1)})) conditional(s32[]{:T(128)} %convert_element_type.88, (f32[2,1024]{1,0:T(2,128)S(1)}, f32[2,1024]{1,0:T(2,128)S(1)}, f32[2,1024,64]{1,2,0:T(8,128)S(1)}) %tuple.50, (s32[]{:T(128)}, s32[]{:T(128)}, s32[1024]{0:T(1024)S(1)}, ...), branch_computations={%region_1.0_spmd, %region_2.4_spmd} | conditional | flops 580130816 | bytes 32469052 | solution.py:112
  92.0 1.2 compare_and_fusion
  93.2 1.1 constant_dynamic-slice_fusion
  94.2 2.4 fusion.4
  96.7 3.0 fusion.3
  99.7 3.2 fusion.8
  105.4 11.1 %conditional.3 = ((f32[2,1024]{1,0:T(2,128)S(1)}, f32[2,1024]{1,0:T(2,128)S(1)}, f32[2,1024,64]{1,2,0:T(8,128)S(1)})) conditional(s32[]{:T(128)} %convert_element_type.88, (f32[2,1024]{1,0:T(2,128)S(1)}, f32[2,1024]{1,0:T(2,128)S(1)}, f32[2,1024,64]{1,2,0:T(8,128)S(1)}) %tuple.50, (s32[]{:T(128)}, s32[]{:T(128)}, s32[1024]{0:T(1024)S(1)}, ...), branch_computations={%region_1.0_spmd, %region_2.4_spmd} | conditional | flops 580130816 | bytes 32469052 | solution.py:112
  105.5 1.2 compare_and_fusion
  106.7 1.1 constant_dynamic-slice_fusion
  107.8 2.4 fusion.4
  110.2 3.0 fusion.3
  113.3 3.2 fusion.8
  117.2 0.6 slice.29
  119.0 11.1 %conditional.3 = ((f32[2,1024]{1,0:T(2,128)S(1)}, f32[2,1024]{1,0:T(2,128)S(1)}, f32[2,1024,64]{1,2,0:T(8,128)S(1)})) conditional(s32[]{:T(128)} %convert_element_type.88, (f32[2,1024]{1,0:T(2,128)S(1)}, f32[2,1024]{1,0:T(2,128)S(1)}, f32[2,1024,64]{1,2,0:T(8,128)S(1)}) %tuple.50, (s32[]{:T(128)}, s32[]{:T(128)}, s32[1024]{0:T(1024)S(1)}, ...), branch_computations={%region_1.0_spmd, %region_2.4_spmd} | conditional | flops 580130816 | bytes 32469052 | solution.py:112
  119.1 1.2 compare_and_fusion
  120.3 1.1 constant_dynamic-slice_fusion
  121.4 2.4 fusion.4
  123.8 3.0 fusion.3
  126.8 3.2 fusion.8
  130.8 0.6 slice.29
  132.6 11.0 %conditional.3 = ((f32[2,1024]{1,0:T(2,128)S(1)}, f32[2,1024]{1,0:T(2,128)S(1)}, f32[2,1024,64]{1,2,0:T(8,128)S(1)})) conditional(s32[]{:T(128)} %convert_element_type.88, (f32[2,1024]{1,0:T(2,128)S(1)}, f32[2,1024]{1,0:T(2,128)S(1)}, f32[2,1024,64]{1,2,0:T(8,128)S(1)}) %tuple.50, (s32[]{:T(128)}, s32[]{:T(128)}, s32[1024]{0:T(1024)S(1)}, ...), branch_computations={%region_1.0_spmd, %region_2.4_spmd} | conditional | flops 580130816 | bytes 32469052 | solution.py:112
  132.7 1.2 compare_and_fusion
  133.9 1.1 constant_dynamic-slice_fusion
  135.0 2.4 fusion.4
  137.4 3.0 fusion.3
  140.4 3.2 fusion.8
  146.9 0.6 slice.29
  149.5 0.6 slice.29
  152.0 0.6 slice.29
  154.5 0.6 slice.29
  157.1 0.6 slice.29
  159.6 0.6 slice.29
  167.3 0.6 slice.29
  169.8 0.6 slice.29
  172.4 0.6 slice.29
  174.7 31.0 %all_to_all.32 = bf16[8,1024,128]{2,1,0:T(8,128)(2,1)S(1)} all-to-all(bf16[8,1024,128]{2,1,0:T(8,128)(2,1)S(1)} %broadcast_in_dim.67), channel_id=1, replica_groups=mesh['sp'=16,'tp'=8] {'tp'}, dimensions={0} | all-to-all | bytes 4194304 | tf_op jit(solution)/shard_map/all_to_all | solution.py:38
  205.8 1.2 convert_reduce_fusion
  207.3 0.6 broadcast_in_dim.68
  207.9 4.3 %all-to-all-start.3 = ((f32[8,1,1024]{2,1,0:T(1,128)}), f32[8,1,1024]{2,1,0:T(1,128)S(1)}, u32[]{:S(2)}, u32[]{:S(2)}) async-start(f32[8,1,1024]{2,1,0:T(1,128)} %broadcast_in_dim.68), calls=%async_computation.3 | async-start | bytes 65536 | tf_op jit(solution)/shard_map/all_to_all | solution.py:38
  212.2 4.7 %all-to-all-done.3 = f32[8,1,1024]{2,1,0:T(1,128)S(1)} async-done(((f32[8,1,1024]{2,1,0:T(1,128)}), f32[8,1,1024]{2,1,0:T(1,128)S(1)}, u32[]{:S(2)}, u32[]{:S(2)}) %all-to-all-start.3) | async-done | bytes 32800 | tf_op jit(solution)/shard_map/all_to_all | solution.py:38
  217.0 1.0 fusion.25
  218.1 98.5 %all-gather.6.cloned.1.call-done = bf16[1024,2048]{1,0:T(8,128)(2,1)} async-done(((bf16[1024,256]{1,0:T(8,128)(2,1)}), bf16[1024,2048]{1,0:T(8,128)(2,1)}) %all-gather.6.cloned.1.call-update) | async-done | bytes 4194320 | tf_op jit(solution)/shard_map/all_gather | solution.py:158
  316.6 8.1 %multiply_convert_fusion = bf16[1024,1024]{1,0:T(8,128)(2,1)S(1)} fusion(bf16[1024,2048]{1,0:T(8,128)(2,1)} %all-gather.6.cloned.1.call-done, bf16[2048,2048]{0,1:T(8,128)(2,1)} %all-gather.8.cloned.1.call-done), kind=kOutput, calls=%fused_computation.25 | convolution fusion | flops 4298113024 | bytes 10485760 | tf_op jit(solution)/shard_map/dot_general | solution.py:159
  324.7 6.1 %fusion.18 = bf16[1024,2048]{1,0:T(8,128)(2,1)} fusion(bf16[1024,1024]{1,0:T(8,128)(2,1)S(1)} %multiply_convert_fusion, bf16[2048,2048]{0,1:T(8,128)(2,1)S(1)} %copy-done.3), kind=kOutput, calls=%fused_computation.26 | convolution fusion | flops 4297064448 | bytes 10485760 | tf_op jit(solution)/shard_map/dot_general | solution.py:161
  330.8 35.7 %reduce-scatter.2.cloned.1.call-done = bf16[1024,256]{1,0:T(8,128)(2,1)} async-done(((bf16[1024,2048]{1,0:T(8,128)(2,1)}), bf16[1024,256]{1,0:T(8,128)(2,1)}) %reduce-scatter.2.cloned.1.call-update) | async-done | bytes 524304 | tf_op jit(solution)/shard_map/reduce_scatter | solution.py:162
  366.5 2.0 fusion.26
  (100 shorter events, 4.1 us)
Async XLA Ops:
  6.5 76.9 %all-gather.4.cloned.1.call-start = ((), (), s32[]{:S(2)}) async-start(), calls=%async_computation.5 | async-start | bytes 8912896 | tf_op jit(solution)/shard_map/all_gather | solution.py:49
  9.6 208.5 %all-gather.8.cloned.1.call-start = ((), (), s32[]{:S(2)}) async-start(), calls=%async_computation.7 | async-start | bytes 8912896 | tf_op jit(solution)/shard_map/all_gather | solution.py:20
  14.0 31.4 %all-to-all-start = ((f32[16,1024,2]{1,2,0:T(2,128)}), f32[16,1024,2]{1,2,0:T(2,128)S(1)}, u32[]{:S(2)}, u32[]{:S(2)}) async-start(f32[16,1024,2]{1,2,0:T(2,128)} %broadcast_in_dim.65), calls=%async_computation | async-start | bytes 262144 | tf_op jit(solution)/shard_map/all_to_all | solution.py:38
  45.4 129.0 %all-to-all-start.2 = ((bf16[128,8,256]{2,0,1:T(8,128)(2,1)}), bf16[128,8,256]{2,0,1:T(8,128)(2,1)S(1)}, u32[]{:S(2)}, u32[]{:S(2)}) async-start(bf16[128,8,256]{2,0,1:T(8,128)(2,1)} %copy.47), calls=%async_computation.2 | async-start | bytes 1048576 | tf_op jit(solution)/shard_map/all_to_all | solution.py:123
  56.0 33.3 %copy-start.1 = (f32[1024,2]{0,1:T(2,128)S(1)}, f32[1024,2]{0,1:T(2,128)}, u32[]{:S(2)}) copy-start(f32[1024,2]{0,1:T(2,128)} %param.17) | copy-start | bytes 24580
  56.0 33.3 %copy-start.2 = (s32[1024]{0:T(1024)S(1)}, s32[1024]{0:T(1024)}, u32[]{:S(2)}) copy-start(s32[1024]{0:T(1024)} %param.18) | copy-start | bytes 12292
  174.2 32.8 %copy-start = (bf16[1024,256]{1,0:T(8,128)(2,1)S(1)}, bf16[1024,256]{1,0:T(8,128)(2,1)}, u32[]{:S(2)}) copy-start(bf16[1024,256]{1,0:T(8,128)(2,1)} %param.19) | copy-start | bytes 1572868
  174.2 38.0 %copy-start.4 = (bf16[256]{0:T(256)(128)(2,1)S(1)}, bf16[256]{0:T(256)(128)(2,1)}, u32[]{:S(2)}) copy-start(bf16[256]{0:T(256)(128)(2,1)} %param.21) | copy-start | bytes 1540
  207.9 9.0 %all-to-all-start.3 = ((f32[8,1,1024]{2,1,0:T(1,128)}), f32[8,1,1024]{2,1,0:T(1,128)S(1)}, u32[]{:S(2)}, u32[]{:S(2)}) async-start(f32[8,1,1024]{2,1,0:T(1,128)} %broadcast_in_dim.68), calls=%async_computation.3 | async-start | bytes 65536 | tf_op jit(solution)/shard_map/all_to_all | solution.py:38
  212.2 104.4 %all-gather.6.cloned.1.call-start = ((), (), s32[]{:S(2)}) async-start(), calls=%async_computation.6 | async-start | bytes 4718592 | tf_op jit(solution)/shard_map/all_gather | solution.py:158
  218.0 148.6 %reduce-scatter.2.cloned.1.call-start = ((), (), s32[]{:S(2)}) async-start(), calls=%async_computation.8 | async-start | bytes 4718592 | tf_op jit(solution)/shard_map/reduce_scatter | solution.py:162
  316.6 8.1 %copy-start.3 = (bf16[2048,2048]{0,1:T(8,128)(2,1)S(1)}, bf16[2048,2048]{0,1:T(8,128)(2,1)}, u32[]{:S(2)}) copy-start(bf16[2048,2048]{0,1:T(8,128)(2,1)} %all-gather.8.cloned.1.call-done) | copy-start | bytes 25165828
Sparse Core Ops, SparseCore 0:
  9.7 73.6 all-gather.3
  85.5 75.4 all-gather.7
  218.1 98.4 all-gather.5
  330.9 35.5 reduce-scatter.1
where the time goes:
time: 380 us; the launch traced here: 375 us
  waiting for transfers between devices  166 us (44%)
  blocking collectives  49.5 us (13%)
  matrix products  37.9 us (10%)
  loops' own time  31.6 us (8%)
  local copies, waits for them, and re-layouts  30.9 us (8%)
  other arithmetic  22.7 us (6%)
  starting transfers between devices  22.5 us (6%)
  between operations  13.3 us (4%)
    all_gather x1, waiting for transfers between devices, body(): features = lax.all_gather(normed, 'tp', axis=1, tiled=True)  98.5 us
    reduce_scatter x1, waiting for transfers between devices, body(): lax.psum_scatter(down_terms.astype(jnp.bfloat16), 'tp', scatter_dimension...  35.7 us
    another operation x1, loops' own time, fold_piece(): return lax.fori_loop(0, piece_rows // key_span, key_step, state_carry)  31.2 us
    all_to_all x1, blocking collectives, copy_for_each(): lax.all_to_all(jnp.broadcast_to(value[None], (peers, *value.shape)), axis...  31 us
    all_gather x1, waiting for transfers between devices, side_by_side(): whole, at, outs = (lax.all_gather(both, axis, axis=dim, tiled=True), 0, [])  27.4 us
    all_gather x1, blocking collectives, body(): lax.all_gather(doc_ids, 'sp', axis=0, tiled=True)  18.5 us
    dot_general x4, matrix products, attend_span(): jnp.einsum('hqk,khd->hqd', weights.astype(jnp.bfloat16), value_three, pre...  12.8 us
    reduce_sum x4, other arithmetic, attend_span(): weight_sum = weight_sum * shrink + jnp.sum(weights, axis=-1)  11.9 us
  transfers between devices with their start and end apart: 7, of which 4 were waited for; matrix products, arithmetic and copies ran while one was open for 19% of the time, Pallas kernels for 0%

commit v1 on v0

v1 whole, which is shorter than its diff:
```python
import functools

import jax
import jax.numpy as jnp
from jax import lax
from jax.experimental import pallas as pl
from jax.experimental.pallas import tpu as pltpu
from jax.sharding import Mesh, PartitionSpec as P

D = 2048
HD = 64
TOK = 1024
HALF = 512
KROWS = 256
VROWS = 256
GROWS = 32
KV_ROWS = KROWS + VROWS + GROWS
Q_ROWS = 256

eps = 1e-06
far_below = -1e30
lowest = -1e29
RING = (1, 3, 2)


DIMS = (((1,), (0,)), ((), ()))


def score(i, pq, kv, ke, qa, qb, s_ref):
    keys = jnp.concatenate([kv[i, 0:KROWS, :], ke[i]], axis=1)
    for j in range(2):
        for part, q_ref in enumerate((qa, qb)):
            s_ref[j, 256 * part : 256 * (part + 1), :] = lax.dot_general(
                keys, q_ref[pq, :, 256 * j : 256 * (j + 1)], DIMS, preferred_element_type=jnp.float32
            )


def hide(s_ref, ahead, k_zero, q_zero):
    for j in range(2):
        for part in range(2):
            row = lax.broadcasted_iota(jnp.int32, (256, 256), 0)
            lane = lax.broadcasted_iota(jnp.int32, (256, 256), 1)
            seen = (row - lane <= ahead + 256 * (j - part)) & (
                (row >= k_zero - 256 * part) | (lane < q_zero - 256 * j)
            )
            at = slice(256 * part, 256 * (part + 1))
            s_ref[j, at, :] = jnp.where(seen, s_ref[j, at, :], far_below)


def weigh(pq, s_ref, p_ref, m_ref, l_ref, shrink_ref):
    for j in range(2):
        cols = slice(256 * j, 256 * (j + 1))
        top = jnp.max(s_ref[j, 0:64, :].reshape(8, 8, 256), axis=0)
        for n in range(1, 8):
            top = jnp.maximum(top, jnp.max(s_ref[j, 64 * n : 64 * (n + 1), :].reshape(8, 8, 256), axis=0))
        m_old = m_ref[pq, :, cols]
        m_new = jnp.maximum(m_old, jnp.max(top, axis=0, keepdims=True))
        shrink = jnp.exp(m_old - m_new)
        m_ref[pq, :, cols] = m_new
        shrink_ref[:, cols] = shrink
        sums = jnp.zeros((8, 256), jnp.float32)
        for n in range(8):
            p = jnp.exp(s_ref[j, 64 * n : 64 * (n + 1), :] - m_new)
            sums = sums + jnp.sum(p.reshape(8, 8, 256), axis=0)
            p_ref[j, 64 * n : 64 * (n + 1), :] = p.astype(jnp.bfloat16)
        l_ref[pq, :, cols] = l_ref[pq, :, cols] * shrink + jnp.sum(sums, axis=0, keepdims=True)


def blend(i, pq, kv, p_ref, shrink_ref, acc_ref):
    values = jnp.concatenate([kv[i, KROWS + 64 * n : KROWS + 64 * (n + 1), :] for n in range(4)], axis=1)
    for j in range(2):
        cols = slice(256 * j, 256 * (j + 1))
        product = lax.dot_general(values, p_ref[j], DIMS, preferred_element_type=jnp.float32)
        acc_ref[pq, :, cols] = acc_ref[pq, :, cols] * shrink_ref[:, cols] + product


def attend_kernel(n_arr, first, last, sc, qt_ref, *rest):
    kv_in, rest = rest[:n_arr], rest[n_arr:]
    if first:
        state_in = ()
    else:
        state_in, rest = rest[:3], rest[3:]
    if last:
        out_ref, rest = rest[0], rest[1:]
    m_ref, l_ref, acc_ref, kv, ke, qa, qb, s_a, s_b, p_a, p_b, shrink_a, shrink_b, zero_s, todo, sems = rest
    copies = [
        pltpu.make_async_copy(kv_in[n], kv.at[pl.ds(4 * n, 4)], sems.at[n]) for n in range(n_arr)
    ]
    for copy in copies:
        copy.start()
    if first:
        m_ref[...] = jnp.full(m_ref.shape, lowest, jnp.float32)
        l_ref[...] = jnp.zeros(l_ref.shape, jnp.float32)
        acc_ref[...] = jnp.zeros(acc_ref.shape, jnp.float32)
    else:
        m_ref[...] = state_in[0][...]
        l_ref[...] = state_in[1][...]
        acc_ref[...] = state_in[2][...]
    row = lax.broadcasted_iota(jnp.int32, (128, HALF), 0)
    minus_a = jnp.where(row < 3, -1.0, 0.0).astype(jnp.bfloat16)
    minus_b = jnp.where((row >= 3) & (row < 6), -1.0, 0.0).astype(jnp.bfloat16)
    zeros = jnp.zeros((64, HALF), jnp.bfloat16)
    for pq in range(4):
        q = jnp.concatenate([qt_ref[pq, 64 * n : 64 * (n + 1), :] for n in range(4)], axis=1)
        qa[pq, 0:64, :] = q
        qa[pq, 64:128, :] = zeros
        qa[pq, 128:256, :] = minus_a
        qb[pq, 0:64, :] = zeros
        qb[pq, 64:128, :] = q
        qb[pq, 128:256, :] = minus_b
    for copy in copies:
        copy.wait()
    blank = jnp.zeros((112, 128), jnp.float32)

    def prepare(n, carry):
        for k in range(4):
            i = 4 * n + k
            g = kv[i, KROWS + VROWS : KV_ROWS, :].astype(jnp.float32)
            for half in range(2):
                turned = jnp.concatenate([g[16 * half : 16 * (half + 1)], blank], axis=0).T
                ke[i, 128 * half : 128 * (half + 1), :] = turned.astype(jnp.bfloat16)
            zero_s[i] = HALF - jnp.sum(g[8:16]).astype(jnp.int32)
        return carry

    lax.fori_loop(0, n_arr, prepare, 0)

    def list_keys(i, count):
        arr = i // 4
        k_start = ((i % 4) ^ sc[7 + 2 * arr]) * 4096 + sc[6 + 2 * arr]
        k_zero = zero_s[i]
        for pq in range(4):
            ahead = (pq ^ sc[1]) * 4096 + sc[0] - k_start
            q_zero = sc[2 + pq]
            live = (ahead > -HALF) & jnp.logical_not((k_zero == HALF) & (q_zero == 0))
            full = (ahead >= HALF) & ((k_zero == 0) | (q_zero == HALF))
            todo[count, 0] = i
            todo[count, 1] = pq
            todo[count, 2] = ahead
            todo[count, 3] = jnp.where(full, 0, 1)
            count = count + live.astype(jnp.int32)
        return count

    count = lax.fori_loop(0, 4 * n_arr, list_keys, 0)
    for extra in range(2):
        todo[count + extra, 0] = 0
        todo[count + extra, 1] = 0
        todo[count + extra, 2] = -100000
        todo[count + extra, 3] = 1

    p_b[...] = jnp.zeros(p_b.shape, jnp.bfloat16)
    shrink_b[...] = jnp.ones(shrink_b.shape, jnp.float32)
    score(todo[0, 0], todo[0, 1], kv, ke, qa, qb, s_a)

    def step(t, now, later):
        s_now, p_now, shrink_now = now
        s_later, p_later, shrink_later = later
        before = jnp.maximum(t - 1, 0)

        @pl.when(todo[t, 3] == 1)
        def _():
            hide(s_now, todo[t, 2], zero_s[todo[t, 0]], sc[2 + todo[t, 1]])

        score(todo[t + 1, 0], todo[t + 1, 1], kv, ke, qa, qb, s_later)
        weigh(todo[t, 1], s_now, p_now, m_ref, l_ref, shrink_now)
        blend(todo[before, 0], todo[before, 1], kv, p_later, shrink_later, acc_ref)

    def two_steps(n, carry):
        side_a, side_b = (s_a, p_a, shrink_a), (s_b, p_b, shrink_b)
        step(2 * n, side_a, side_b)
        step(2 * n + 1, side_b, side_a)
        return carry

    rounds = (count + 1) // 2
    lax.fori_loop(0, rounds, two_steps, 0)

    @pl.when(rounds > 0)
    def _():
        at = 2 * rounds - 1
        blend(todo[at, 0], todo[at, 1], kv, p_b, shrink_b, acc_ref)

    if last:

        def finish(pq, carry):
            out = (acc_ref[pq] / l_ref[pq]).astype(jnp.bfloat16)
            block = pq ^ sc[1]
            for quarter in range(4):
                out_ref[quarter * 4 + block] = out[:, 128 * quarter : 128 * (quarter + 1)]
            return carry

        lax.fori_loop(0, 4, finish, 0)


def attend(scalars, qt, arrays, state, first, last):
    n_arr = len(arrays)
    vmem = pl.BlockSpec(memory_space=pltpu.VMEM)
    shapes = [
        jax.ShapeDtypeStruct((4, 1, HALF), jnp.float32),
        jax.ShapeDtypeStruct((4, 1, HALF), jnp.float32),
        jax.ShapeDtypeStruct((4, HD, HALF), jnp.float32),
    ]
    scratch = [
        pltpu.VMEM((4 * n_arr, KV_ROWS, 128), jnp.bfloat16),
        pltpu.VMEM((4 * n_arr, 256, 128), jnp.bfloat16),
        pltpu.VMEM((4, 256, HALF), jnp.bfloat16),
        pltpu.VMEM((4, 256, HALF), jnp.bfloat16),
        pltpu.VMEM((2, HALF, 256), jnp.float32),
        pltpu.VMEM((2, HALF, 256), jnp.float32),
        pltpu.VMEM((2, HALF, 256), jnp.bfloat16),
        pltpu.VMEM((2, HALF, 256), jnp.bfloat16),
        pltpu.VMEM((1, HALF), jnp.float32),
        pltpu.VMEM((1, HALF), jnp.float32),
        pltpu.SMEM((4 * n_arr,), jnp.int32),
        pltpu.SMEM((16 * n_arr + 2, 4), jnp.int32),
        pltpu.SemaphoreType.DMA((n_arr,)),
    ]
    if last:
        out_shape = jax.ShapeDtypeStruct((16, HD, 128), jnp.bfloat16)
        out_specs = vmem
        scratch = [pltpu.VMEM(s.shape, s.dtype) for s in shapes] + scratch
    else:
        out_shape = shapes
        out_specs = [vmem] * 3
    state = () if first else tuple(state)
    return pl.pallas_call(
        functools.partial(attend_kernel, n_arr, first, last),
        out_shape=out_shape,
        in_specs=[pl.BlockSpec(memory_space=pltpu.SMEM), vmem]
        + [pl.BlockSpec(memory_space=pl.ANY)] * n_arr
        + [vmem] * len(state),
        out_specs=out_specs,
        scratch_shapes=scratch,
        compiler_params=pltpu.CompilerParams(vmem_limit_bytes=40 * 1024 * 1024),
        cost_estimate=pl.CostEstimate(
            flops=4_000_000_000 * n_arr, bytes_accessed=1_000_000 * n_arr, transcendentals=0
        ),
        name="attend_first" if first else ("attend_last" if last else "attend_more"),
    )(scalars, qt, *arrays, *state)


def dense_kernel(sc, att_ref, res_ref, *rest):
    w_in, (mid_ref, gain_ref, w_all, sems) = rest[:8], rest[8:]
    copies = []
    for n in range(8):
        at = pl.multiple_of(sc[n], 128)
        lanes = pl.ds(pl.multiple_of(sc[n] * 2, 256), 256)
        copies.append(pltpu.make_async_copy(w_in[n].at[pl.ds(0, 128)], w_all.at[pl.ds(at, 128)], sems.at[n]))
        copies.append(
            pltpu.make_async_copy(w_in[n].at[pl.ds(128, 8), pl.ds(0, 256)], gain_ref.at[:, lanes], sems.at[8 + n])
        )
    for copy in copies:
        copy.start()
    for copy in copies:
        copy.wait()
    att = att_ref[...].reshape(1024, 128)
    for n in range(8):
        tp = 2 * (n % 4) + n // 4
        cols = slice(256 * tp, 256 * (tp + 1))
        mixed = lax.dot_general(
            att, w_all[:, cols], (((0,), (0,)), ((), ())), preferred_element_type=jnp.float32
        )
        mid_ref[:, cols] = (res_ref[n].astype(jnp.float32) + mixed).astype(jnp.bfloat16)


def dense(scalars, att, res, pieces):
    vmem = pl.BlockSpec(memory_space=pltpu.VMEM)
    return pl.pallas_call(
        dense_kernel,
        out_shape=[
            jax.ShapeDtypeStruct((128, D), jnp.bfloat16),
            jax.ShapeDtypeStruct((8, D), jnp.bfloat16),
        ],
        in_specs=[pl.BlockSpec(memory_space=pltpu.SMEM), vmem, vmem] + [pl.BlockSpec(memory_space=pl.ANY)] * 8,
        out_specs=[vmem, vmem],
        scratch_shapes=[pltpu.VMEM((1024, D), jnp.bfloat16), pltpu.SemaphoreType.DMA((16,))],
        compiler_params=pltpu.CompilerParams(vmem_limit_bytes=24 * 1024 * 1024),
        cost_estimate=pl.CostEstimate(flops=1_000_000_000, bytes_accessed=4_000_000, transcendentals=0),
        name="dense",
    )(scalars, att, res, *pieces)


def up_kernel(sc, gain_ref, w_in, *rest):
    mids, (h_ref, own_ref, w_up, mid_all, sems) = rest[:8], rest[8:]
    fetches = [pltpu.make_async_copy(mids[n], mid_all.at[pl.ds(128 * n, 128)], sems.at[16 + n]) for n in range(8)]
    copies = [
        pltpu.make_async_copy(w_in.at[pl.ds(256 * n, 128)], w_up.at[pl.ds(128 * n, 128)], sems.at[n]) for n in range(16)
    ]
    for copy in copies + fetches:
        copy.start()
    gain = gain_ref[0:1, :].astype(jnp.float32)
    for copy in copies:
        copy.wait()
    lanes = pl.ds(pl.multiple_of(sc[8], 256), 256)
    for n in range(0, 8, 2):
        for k in range(2):
            fetches[n + k].wait()
            own_ref[pl.ds(pl.multiple_of(sc[n + k], 128), 128), :] = mid_all[128 * (n + k) : 128 * (n + k + 1), lanes]
        wide = mid_all[128 * n : 128 * (n + 2), :].astype(jnp.float32)
        scale = lax.rsqrt(jnp.sum(wide * wide, axis=-1, keepdims=True) / D + eps)
        normed = (wide * scale * gain).astype(jnp.bfloat16)
        h = jnp.dot(normed, w_up[...], preferred_element_type=jnp.float32)
        h = jnp.square(jnp.maximum(h, 0.0)).astype(jnp.bfloat16)
        for k in range(2):
            h_ref[pl.ds(pl.multiple_of(sc[n + k], 128), 128), :] = h[128 * k : 128 * (k + 1)]


def up(scalars, gain, w, mids):
    vmem = pl.BlockSpec(memory_space=pltpu.VMEM)
    return pl.pallas_call(
        up_kernel,
        out_shape=[
            jax.ShapeDtypeStruct((1024, 1024), jnp.bfloat16),
            jax.ShapeDtypeStruct((1024, 256), jnp.bfloat16),
        ],
        in_specs=[pl.BlockSpec(memory_space=pltpu.SMEM), vmem] + [pl.BlockSpec(memory_space=pl.ANY)] * 9,
        out_specs=[vmem, vmem],
        scratch_shapes=[
            pltpu.VMEM((D, 1024), jnp.bfloat16),
            pltpu.VMEM((1024, D), jnp.bfloat16),
            pltpu.SemaphoreType.DMA((24,)),
        ],
        compiler_params=pltpu.CompilerParams(vmem_limit_bytes=40 * 1024 * 1024),
        cost_estimate=pl.CostEstimate(flops=4_300_000_000, bytes_accessed=8_000_000, transcendentals=0),
        name="up",
    )(scalars, gain, w, *mids)


def down_kernel(sc, h_ref, w_in, mine_ref, other_ref, w_down, sems):
    copies = []
    for k in range(4):
        at = pl.multiple_of((sc[0] + k) * 256 + 128, 128)
        copies.append(pltpu.make_async_copy(w_in.at[pl.ds(at, 128)], w_down.at[pl.ds(128 * k, 128)], sems.at[k]))
    for copy in copies:
        copy.start()
    for copy in copies:
        copy.wait()
    for n, out_ref in ((1 - sc[1], other_ref), (sc[1], mine_ref)):
        rows = w_down[pl.ds(pl.multiple_of(n * 256, 256), 256), :]
        product = lax.dot_general(
            h_ref[...], rows, (((1,), (1,)), ((), ())), preferred_element_type=jnp.float32
        )
        out_ref[...] = product.astype(out_ref.dtype)


def down(scalars, h, w):
    vmem = pl.BlockSpec(memory_space=pltpu.VMEM)
    return pl.pallas_call(
        down_kernel,
        out_shape=[
            jax.ShapeDtypeStruct((1024, 256), jnp.bfloat16),
            jax.ShapeDtypeStruct((1024, 256), jnp.bfloat16),
        ],
        in_specs=[pl.BlockSpec(memory_space=pltpu.SMEM), vmem, pl.BlockSpec(memory_space=pl.ANY)],
        out_specs=[vmem, vmem],
        scratch_shapes=[pltpu.VMEM((512, 1024), jnp.bfloat16), pltpu.SemaphoreType.DMA((4,))],
        compiler_params=pltpu.CompilerParams(vmem_limit_bytes=24 * 1024 * 1024),
        cost_estimate=pl.CostEstimate(flops=1_100_000_000, bytes_accessed=4_000_000, transcendentals=0),
        name="down",
    )(scalars, h, w)


def shifted(value, axis, by):
    n = lax.axis_size(axis)
    return lax.ppermute(value, axis, [(i, (i - by) % n) for i in range(n)])


def partner(value):
    return lax.ppermute(value, "c", [(0, 1), (1, 0)])


def body(queries, keys, values, cum_gates, doc_ids, residual, w_out, norm_gain, w_up, w_down):
    z, y, x, c = (lax.axis_index(a) for a in ("z", "y", "x", "c"))

    q_t = jnp.transpose(queries * jnp.bfloat16(0.125)).reshape(2, HD, 2, 4, 128)
    q_msg = jnp.transpose(q_t, (0, 2, 3, 1, 4)).reshape(2, 2, Q_ROWS, 128)
    v_t = jnp.transpose(values).reshape(2, HD, 2, 4, 128)
    v_msg = jnp.transpose(v_t, (0, 2, 3, 1, 4)).reshape(2, 2, VROWS, 128)
    k_msg = jnp.transpose(keys.reshape(2, 2, KROWS, 2, HD), (3, 0, 2, 1, 4)).reshape(2, 2, KROWS, 128)
    gates = jnp.transpose(cum_gates).reshape(2, 2, 2, 2, 128)
    hi = lax.reduce_precision(gates, 8, 7)
    mid = lax.reduce_precision(gates - hi, 8, 7)
    low = gates - hi - mid
    three = jnp.transpose(jnp.stack([hi, mid, low]), (1, 2, 4, 3, 0, 5)).reshape(2, 2, 2, 6, 128)
    docs = jnp.broadcast_to(doc_ids.astype(jnp.float32).reshape(1, 2, 4, 128), (2, 2, 4, 128))
    docs = jnp.stack([docs, jnp.zeros_like(docs)], axis=2)
    three = jnp.pad(three, ((0, 0), (0, 0), (0, 0), (0, 2), (0, 0)))
    docs = jnp.pad(docs, ((0, 0), (0, 0), (0, 0), (0, 4), (0, 0)))
    g_msg = jnp.concatenate([three, docs], axis=3).reshape(2, 2, GROWS, 128).astype(jnp.bfloat16)
    messages = jnp.concatenate([k_msg, v_msg, g_msg, q_msg], axis=2)

    received = []
    for step in range(4):
        pairs = []
        for zs in range(4):
            for cs in range(2):
                j = 2 * cs + ((zs & 1) ^ (step & 1))
                cd = (zs >> 1) ^ (step >> 1)
                pairs.append((zs * 2 + cs, j * 2 + cd))
        head = (z & 1) ^ (step & 1)
        half = (z >> 1) ^ (step >> 1)
        message = lax.dynamic_slice(messages, (head, half, 0, 0), (1, 1, KV_ROWS + Q_ROWS, 128))[0, 0]
        received.append(lax.ppermute(message, ("z", "c"), pairs))
    qt = jnp.stack([r[KV_ROWS:] for r in received])
    kv_own = jnp.stack([r[:KV_ROWS] for r in received])

    kv_mine = [kv_own] + [shifted(kv_own, "y", r) for r in RING]

    kv_own, w_out, residual, norm_gain, w_up, w_down = lax.optimization_barrier(
        (kv_own, w_out, residual, norm_gain, w_up, w_down)
    )
    both = jnp.concatenate([w_up, jnp.transpose(w_down)], axis=0)

    q_zero = HALF - jnp.sum(kv_own[:, KROWS + VROWS + 8 : KROWS + VROWS + 16].astype(jnp.float32), axis=(1, 2))
    mask_a = (z & 1) | (c << 1)
    mask_b = (z & 1) | ((1 - c) << 1)
    base = [y * TOK + c * HALF, mask_a] + [q_zero[n].astype(jnp.int32) for n in range(4)]

    def places(rs):
        out = []
        for r in rs:
            at = ((y + r) % 4) * TOK
            out += [at + c * HALF, mask_a, at + (1 - c) * HALF, mask_b]
        return jnp.stack(base + out).astype(jnp.int32)

    kv_near = partner(kv_own)
    state = attend(places([0]), qt, [kv_own, kv_near], (), True, False)
    gain_row = jnp.pad(norm_gain[None], ((0, 7), (0, D - 256)))
    w_msg = jnp.concatenate([w_out, gain_row], axis=0)
    w_mine = [w_msg] + [shifted(w_msg, "x", r) for r in RING]
    res = lax.all_to_all(residual.reshape(8, 128, 256), ("c", "x"), 0, 0, tiled=True)
    kv_mine[1:], state, both = lax.optimization_barrier((kv_mine[1:], state, both))
    both = lax.all_gather(both, ("z", "y"), axis=0, tiled=True)
    kv_other = [None] + [partner(piece) for piece in kv_mine[1:]]
    pieces = [piece for pair in zip(kv_mine[1:], kv_other[1:]) for piece in pair]
    out = attend(places(RING), qt, pieces, state, False, True)

    w_mine, res, out = lax.optimization_barrier((w_mine, res, out))
    w_pieces = [w for mine in w_mine for w in (mine, partner(mine))]

    attended = lax.all_to_all(out, ("x", "z"), 0, 0, tiled=True)

    order = [((x + r) % 4, cs) for r in (0, 1, 3, 2) for cs in (c, 1 - c)]
    rows_at = jnp.stack([xs * 256 + cs * 128 for xs, cs in order]).astype(jnp.int32)
    middle, gain = dense(rows_at, attended, res, w_pieces)

    mid_mine = [middle] + [shifted(middle, "x", r) for r in RING]
    mids = [m for mine in mid_mine for m in (mine, partner(mine))]
    token_at = jnp.stack([cs * 512 + xs * 128 for xs, cs in order] + [(2 * x + c) * 256]).astype(jnp.int32)
    hidden, middle_own = up(token_at, gain, both, mids)

    total = middle_own.astype(jnp.float32)
    for r in (2, 1, 3, 0):
        mine, other = down(jnp.stack([((x + r) % 4) * 4, c]).astype(jnp.int32), hidden, both)
        chip = mine.astype(jnp.float32) + partner(other).astype(jnp.float32)
        if r:
            chip = shifted(chip.astype(jnp.bfloat16), "x", -r).astype(jnp.float32)
        total = total + chip
    return total.astype(jnp.bfloat16)


def solution(mesh):
    split = Mesh(mesh.devices.reshape(4, 4, 4, 2), ("z", "y", "x", "c"))
    sp, tp = ("z", "y"), ("x", "c")
    in_specs = (
        P(sp, tp),
        P(sp, tp),
        P(sp, tp),
        P(sp, tp),
        P(sp),
        P(sp, tp),
        P(tp, None),
        P(tp),
        P(sp, tp),
        P(tp, sp),
    )
    return jax.shard_map(body, mesh=split, in_specs=in_specs, out_specs=P(sp, tp), check_vma=False)
```

time: 380 us -> 209 us (0.55)
  the two profiles are of different devices: /device:TPU:25 before, /device:TPU:1 now
where the time goes in v1:
time: 209 us
  waiting for transfers between devices  63.9 us (31%)
  starting transfers between devices  58.1 us (28%)
  Pallas kernels  45 us (22%)
  local copies, waits for them, and re-layouts  19.1 us (9%)
  between operations  16.6 us (8%)
  other arithmetic  5.89 us (3%)
    ppermute x12, waiting for transfers between devices, shifted(): return lax.ppermute(value, axis, [(i, (i - by) % n) for i in range(n)])  42 us
    ppermute x16, starting transfers between devices, partner(): return lax.ppermute(value, 'c', [(0, 1), (1, 0)])  23.6 us
    pallas_call x2, Pallas kernels, attend(): pl.pallas_call(functools.partial(attend_kernel, n_arr, first, last), out_...  23.2 us
    ppermute x12, starting transfers between devices, shifted(): return lax.ppermute(value, axis, [(i, (i - by) % n) for i in range(n)])  15.7 us
    unnamed x47, local copies, waits for them, and re-layouts  15 us
    ppermute x4, starting transfers between devices, body(): received.append(lax.ppermute(message, ('z', 'c'), pairs))  10 us
    pallas_call x1, Pallas kernels, up(): pl.pallas_call(up_kernel, out_shape=[jax.ShapeDtypeStruct((1024, 1024), j...  9.34 us
    all_to_all x1, waiting for transfers between devices, body(): lax.all_to_all(residual.reshape(8, 128, 256), ('c', 'x'), 0, 0, tiled=True)  8.74 us
  transfers between devices with their start and end apart: 35, of which 10 were waited for; matrix products, arithmetic and copies ran while one was open for 2% of the time, Pallas kernels for 16%

profile of v1, /device:TPU:1, one launch (start us, length us, event | category | flops | bytes accessed | tf_op | source)
XLA Modules:
  0.0 208.6 jit_solution(582594591275266503)
XLA Ops:
  6.5 0.8 reshape.84
  7.3 0.7 convert_convert_fusion
  8.2 1.0 multiply_bitcast_fusion
  9.4 0.2 reshape.86
  10.5 0.2 reshape.80
  10.7 0.2 pad_maximum_fusion
  11.2 4.7 %collective-permute-start.3 = (bf16[800,128]{1,0:T(8,128)(2,1)S(1)}, bf16[800,128]{1,0:T(8,128)(2,1)S(1)}, u32[]{:S(2)}, u32[]{:S(2)}) collective-permute-start(bf16[800,128]{1,0:T(8,128)(2,1)S(1)} %bitcast.90), channel_id=1, source_target_pairs={{0,33},{1,97},{32,1},{33,65},{64,32},{65,96},{96,0},{97,64},{2,35}... | collective-permute-start | bytes 614408 | tf_op jit(solution)/shard_map/ppermute | solution.py:401
  16.0 1.8 collective-permute-start.2
  18.3 3.5 %collective-permute-start = (bf16[800,128]{1,0:T(8,128)(2,1)S(1)}, bf16[800,128]{1,0:T(8,128)(2,1)S(1)}, u32[]{:S(2)}, u32[]{:S(2)}) collective-permute-start(bf16[800,128]{1,0:T(8,128)(2,1)S(1)} %bitcast.93), channel_id=1, source_target_pairs={{0,0},{1,64},{32,32},{33,96},{64,1},{65,65},{96,33},{97,97},{2,2},... | collective-permute-start | bytes 614408 | tf_op jit(solution)/shard_map/ppermute | solution.py:401
  22.0 3.2 %collective-permute-done.1 = bf16[800,128]{1,0:T(8,128)(2,1)S(1)} collective-permute-done((bf16[800,128]{1,0:T(8,128)(2,1)S(1)}, bf16[800,128]{1,0:T(8,128)(2,1)S(1)}, u32[]{:S(2)}, u32[]{:S(2)}) %collective-permute-start.1) | collective-permute-done | bytes 204832 | tf_op jit(solution)/shard_map/ppermute | solution.py:401
  25.2 2.2 %collective-permute-done = bf16[800,128]{1,0:T(8,128)(2,1)S(1)} collective-permute-done((bf16[800,128]{1,0:T(8,128)(2,1)S(1)}, bf16[800,128]{1,0:T(8,128)(2,1)S(1)}, u32[]{:S(2)}, u32[]{:S(2)}) %collective-permute-start) | collective-permute-done | bytes 204832 | tf_op jit(solution)/shard_map/ppermute | solution.py:401
  27.6 2.8 %collective-permute-start.7 = (bf16[4,544,128]{2,1,0:T(8,128)(2,1)S(1)}, bf16[4,544,128]{2,1,0:T(8,128)(2,1)S(1)}, u32[]{:S(2)}, u32[]{:S(2)}) collective-permute-start(bf16[4,544,128]{2,1,0:T(8,128)(2,1)S(1)} %pad_maximum_fusion.1.rest_0_), channel_id=1, source_target_pairs={{0,24},{8,0},{16,8},{24,16},{1,25},{9,1},{17,9},{25,17},{2,26},{10... | collective-permute-start | bytes 1671176 | tf_op jit(solution)/shard_map/ppermute | solution.py:363
  30.4 1.6 collective-permute-start.9
  32.3 0.7 fusion.4
  35.7 0.8 pad_maximum_fusion.2
  36.5 8.1 %attend_first.1 = (f32[4,1,512]{2,1,0:T(1,128)S(1)}, f32[4,1,512]{2,1,0:T(1,128)S(1)}, f32[4,64,512]{2,1,0:T(8,128)S(1)}) custom-call(s32[10]{0:T(128)S(1)} %stack.226.sc, bf16[4,256,128]{2,1,0:T(8,128)(2,1)S(1)} %pad_maximum_fusion.3.qt_ref, bf16[4,544,128]{2,1,0:T(8,128)(2,1)S(1)} %pad_maximum_fusion.1.rest_0_, ...), custom_call_target="tpu_custom_call" | custom-call | flops 8000000000 | bytes 2000000 | tf_op jit(solution)/shard_map/attend_first/pallas_call | solution.py:224
  44.7 9.1 %collective-permute-done.7.rest_0_ = bf16[4,544,128]{2,1,0:T(8,128)(2,1)S(1)} collective-permute-done((bf16[4,544,128]{2,1,0:T(8,128)(2,1)S(1)}, bf16[4,544,128]{2,1,0:T(8,128)(2,1)S(1)}, u32[]{:S(2)}, u32[]{:S(2)}) %collective-permute-start.7) | collective-permute-done | bytes 557088 | tf_op jit(solution)/shard_map/ppermute | solution.py:363
  53.8 2.4 %collective-permute-done.9.rest_4_ = bf16[4,544,128]{2,1,0:T(8,128)(2,1)} collective-permute-done((bf16[4,544,128]{2,1,0:T(8,128)(2,1)S(1)}, bf16[4,544,128]{2,1,0:T(8,128)(2,1)}, u32[]{:S(2)}, u32[]{:S(2)}) %collective-permute-start.9) | collective-permute-done | bytes 557088 | tf_op jit(solution)/shard_map/ppermute | solution.py:363
  56.2 2.6 %collective-permute-start.11 = (bf16[4,544,128]{2,1,0:T(8,128)(2,1)S(1)}, bf16[4,544,128]{2,1,0:T(8,128)(2,1)}, u32[]{:S(2)}, u32[]{:S(2)}) collective-permute-start(bf16[4,544,128]{2,1,0:T(8,128)(2,1)S(1)} %collective-permute-done.7.rest_0_), channel_id=1, source_target_pairs={{0,1},{1,0},{2,3},{3,2},{4,5},{5,4},{6,7},{7,6},{8,9},{9,8},{10,11... | collective-permute-start | bytes 1671176 | tf_op jit(solution)/shard_map/ppermute | solution.py:367
  58.9 0.4 collective-permute-start.13
  59.4 2.5 %collective-permute-start.4 = (bf16[136,2048]{1,0:T(8,128)(2,1)S(1)}, bf16[136,2048]{1,0:T(8,128)(2,1)S(1)}, u32[]{:S(2)}, u32[]{:S(2)}) collective-permute-start(bf16[136,2048]{1,0:T(8,128)(2,1)S(1)} %fusion.1.rest_0_), channel_id=1, source_target_pairs={{0,6},{2,0},{4,2},{6,4},{1,7},{3,1},{5,3},{7,5},{8,14},{10,8},{12,... | collective-permute-start | bytes 1671176 | tf_op jit(solution)/shard_map/ppermute | solution.py:363
  62.0 4.9 %all-to-all-start = ((bf16[8,128,256]{2,1,0:T(8,128)(2,1)}), bf16[8,128,256]{2,1,0:T(8,128)(2,1)S(1)}, u32[]{:S(2)}, u32[]{:S(2)}) async-start(bf16[8,128,256]{2,1,0:T(8,128)(2,1)} %bitcast.88), calls=%async_computation | async-start | bytes 1048576 | tf_op jit(solution)/shard_map/all_to_all | solution.py:429
  67.0 2.9 %collective-permute-start.6 = (bf16[136,2048]{1,0:T(8,128)(2,1)S(1)}, bf16[136,2048]{1,0:T(8,128)(2,1)S(1)}, u32[]{:S(2)}, u32[]{:S(2)}) collective-permute-start(bf16[136,2048]{1,0:T(8,128)(2,1)S(1)} %fusion.1.rest_0_), channel_id=1, source_target_pairs={{0,4},{2,6},{4,0},{6,2},{1,5},{3,7},{5,1},{7,3},{8,12},{10,14},{12... | collective-permute-start | bytes 1671176 | tf_op jit(solution)/shard_map/ppermute | solution.py:363
  69.9 1.1 copy-done.2
  71.0 0.7 copy-done.14
  71.6 15.1 %attend_last.1 = bf16[16,64,128]{2,1,0:T(8,128)(2,1)} custom-call(s32[18]{0:T(128)S(1)} %stack.218.sc, bf16[4,256,128]{2,1,0:T(8,128)(2,1)S(1)} %pad_maximum_fusion.3.qt_ref, bf16[4,544,128]{2,1,0:T(8,128)(2,1)S(1)} %copy-done.2, bf16[4,544,128]{2,1,0:T(8,128)(2,1)} %collective-permute-done.11.rest_1_, bf16[4,544,128]{2,1,0:T(8,128)(2,1)} %collective-permute-done.8.rest_2_, ...), custom_call_target="tpu_custom_call" | custom-call | flops 24000000000 | bytes 6000000 | tf_op jit(solution)/shard_map/attend_last/pallas_call | solution.py:224
  86.7 8.7 %all-to-all-done.res_ref = bf16[8,128,256]{2,1,0:T(8,128)(2,1)S(1)} async-done(((bf16[8,128,256]{2,1,0:T(8,128)(2,1)}), bf16[8,128,256]{2,1,0:T(8,128)(2,1)S(1)}, u32[]{:S(2)}, u32[]{:S(2)}) %all-to-all-start) | async-done | bytes 524320 | tf_op jit(solution)/shard_map/all_to_all | solution.py:429
  95.6 0.5 collective-permute-start.15
  96.1 0.3 collective-permute-start.16
  96.3 0.2 collective-permute-start.17
  96.6 3.9 %all-to-all-start.1 = ((bf16[16,64,128]{2,1,0:T(8,128)(2,1)}), bf16[16,64,128]{2,1,0:T(8,128)(2,1)S(1)}, u32[]{:S(2)}, u32[]{:S(2)}) async-start(bf16[16,64,128]{2,1,0:T(8,128)(2,1)} %attend_last.1), calls=%async_computation.1 | async-start | bytes 524288 | tf_op jit(solution)/shard_map/all_to_all | solution.py:439
  100.6 7.6 %all-to-all-done.1.att_ref = bf16[16,64,128]{2,1,0:T(8,128)(2,1)S(1)} async-done(((bf16[16,64,128]{2,1,0:T(8,128)(2,1)}), bf16[16,64,128]{2,1,0:T(8,128)(2,1)S(1)}, u32[]{:S(2)}, u32[]{:S(2)}) %all-to-all-start.1) | async-done | bytes 262176 | tf_op jit(solution)/shard_map/all_to_all | solution.py:439
  108.3 3.8 %dense.1 = (bf16[128,2048]{1,0:T(8,128)(2,1)}, bf16[8,2048]{1,0:T(8,128)(2,1)S(1)}) custom-call(s32[8]{0:T(128)S(1)} %stack.201.sc, bf16[16,64,128]{2,1,0:T(8,128)(2,1)S(1)} %all-to-all-done.1.att_ref, bf16[8,128,256]{2,1,0:T(8,128)(2,1)S(1)} %all-to-all-done.res_ref, bf16[136,2048]{1,0:T(8,128)(2,1)S(1)} %fusion.1.rest_0_, ...), custom_call_target="tpu_custom_call" | custom-call | flops 1000000000 | bytes 4000000 | tf_op jit(solution)/shard_map/dense/pallas_call | solution.py:266
  112.2 1.6 collective-permute-start.19
  113.7 1.3 collective-permute-start.23
  115.0 2.5 %collective-permute-start.18 = (bf16[128,2048]{1,0:T(8,128)(2,1)}, bf16[128,2048]{1,0:T(8,128)(2,1)S(1)}, u32[]{:S(2)}, u32[]{:S(2)}) collective-permute-start(bf16[128,2048]{1,0:T(8,128)(2,1)} %get-tuple-element.62.rest_0_), channel_id=1, source_target_pairs={{0,1},{1,0},{2,3},{3,2},{4,5},{5,4},{6,7},{7,6},{8,9},{9,8},{10,11... | collective-permute-start | bytes 1572872 | tf_op jit(solution)/shard_map/ppermute | solution.py:367
  117.5 7.2 %collective-permute-done.19.rest_2_ = bf16[128,2048]{1,0:T(8,128)(2,1)S(1)} collective-permute-done((bf16[128,2048]{1,0:T(8,128)(2,1)}, bf16[128,2048]{1,0:T(8,128)(2,1)S(1)}, u32[]{:S(2)}, u32[]{:S(2)}) %collective-permute-start.19) | collective-permute-done | bytes 524320 | tf_op jit(solution)/shard_map/ppermute | solution.py:363
  124.7 12.8 %collective-permute-start.20 = (bf16[128,2048]{1,0:T(8,128)(2,1)S(1)}, bf16[128,2048]{1,0:T(8,128)(2,1)S(1)}, u32[]{:S(2)}, u32[]{:S(2)}) collective-permute-start(bf16[128,2048]{1,0:T(8,128)(2,1)S(1)} %collective-permute-done.19.rest_2_), channel_id=1, source_target_pairs={{0,1},{1,0},{2,3},{3,2},{4,5},{5,4},{6,7},{7,6},{8,9},{9,8},{10,11... | collective-permute-start | bytes 1572872 | tf_op jit(solution)/shard_map/ppermute | solution.py:367
  137.5 0.8 copy-done.3
  138.3 2.5 %collective-permute-start.22 = (bf16[128,2048]{1,0:T(8,128)(2,1)S(1)}, bf16[128,2048]{1,0:T(8,128)(2,1)}, u32[]{:S(2)}, u32[]{:S(2)}) collective-permute-start(bf16[128,2048]{1,0:T(8,128)(2,1)S(1)} %collective-permute-done.21.rest_4_), channel_id=1, source_target_pairs={{0,1},{1,0},{2,3},{3,2},{4,5},{5,4},{6,7},{7,6},{8,9},{9,8},{10,11... | collective-permute-start | bytes 1572872 | tf_op jit(solution)/shard_map/ppermute | solution.py:367
  140.7 0.8 copy-done.5
  141.5 0.8 copy-done.7
  142.5 0.8 copy-done.9
  143.3 0.8 copy-done.11
  144.2 1.2 copy-done.4
  145.4 1.3 copy-done.6
  146.6 1.0 copy-done.8
  147.7 1.0 copy-done.10
  148.7 1.0 copy-done.12
  149.8 9.3 %up.1 = (bf16[1024,1024]{1,0:T(8,128)(2,1)S(1)}, bf16[1024,256]{1,0:T(8,128)(2,1)S(1)}) custom-call(s32[9]{0:T(128)S(1)} %stack.192.sc, bf16[8,2048]{1,0:T(8,128)(2,1)S(1)} %get-tuple-element.60.gain_ref, bf16[4096,1024]{1,0:T(8,128)(2,1)} %all-gather.2.cloned.1.call-done.w_in, bf16[128,2048]{1,0:T(8,128)(2,1)} %get-tuple-element.62.rest_0_, ...), custom_call_target="tpu_custom_call" | custom-call | flops 4300000256 | bytes 8000000 | tf_op jit(solution)/shard_map/up/pallas_call | solution.py:308
  159.1 2.7 %down.4 = (bf16[1024,256]{1,0:T(8,128)(2,1)S(1)}, bf16[1024,256]{1,0:T(8,128)(2,1)}) custom-call(s32[2]{0:T(128)S(1)} %get-tuple-element.84.sc, bf16[1024,1024]{1,0:T(8,128)(2,1)S(1)} %get-tuple-element.64.h_ref, bf16[4096,1024]{1,0:T(8,128)(2,1)S(1)} %bitcast.80), custom_call_target="tpu_custom_call" | custom-call | flops 1100000000 | bytes 4000000 | tf_op jit(solution)/shard_map/down/pallas_call | solution.py:346
  161.9 0.6 collective-permute-start.25
  162.4 3.4 %copy-done = bf16[4096,1024]{1,0:T(8,128)(2,1)S(1)} copy-done((bf16[4096,1024]{1,0:T(8,128)(2,1)S(1)}, bf16[4096,1024]{1,0:T(8,128)(2,1)}, u32[]{:S(2)}) %copy-start) | copy-done | bytes 8388632
  165.8 2.0 down.5
  167.8 0.3 collective-permute-start.27
  168.2 2.0 down.6
  170.2 0.6 collective-permute-start.29
  170.7 2.0 down.7
  172.8 1.2 add_convert_fusion.3
  174.2 1.9 collective-permute-start.28
  176.3 0.9 collective-permute-start.30
  177.2 11.4 %collective-permute-done.26 = bf16[1024,256]{1,0:T(8,128)(2,1)S(1)} collective-permute-done((bf16[1024,256]{1,0:T(8,128)(2,1)S(1)}, bf16[1024,256]{1,0:T(8,128)(2,1)S(1)}, u32[]{:S(2)}, u32[]{:S(2)}) %collective-permute-start.26) | collective-permute-done | bytes 524320 | tf_op jit(solution)/shard_map/ppermute | solution.py:363
  188.6 11.9 %collective-permute-done.28 = bf16[1024,256]{1,0:T(8,128)(2,1)S(1)} collective-permute-done((bf16[1024,256]{1,0:T(8,128)(2,1)S(1)}, bf16[1024,256]{1,0:T(8,128)(2,1)S(1)}, u32[]{:S(2)}, u32[]{:S(2)}) %collective-permute-start.28) | collective-permute-done | bytes 524320 | tf_op jit(solution)/shard_map/ppermute | solution.py:363
  200.5 1.2 add_convert_fusion
  (115 shorter events, 4.1 us)
Async XLA Ops:
  6.5 3.2 %copy-start.16 = (bf16[1024,128]{1,0:T(8,128)(2,1)S(1)}, bf16[1024,128]{1,0:T(8,128)(2,1)}, u32[]{:S(2)}) copy-start(bf16[1024,128]{1,0:T(8,128)(2,1)} %param.12) | copy-start | bytes 786436
  6.5 137.6 %all-gather.2.cloned.1.call-start = ((), (), s32[]{:S(2)}) async-start(), calls=%async_computation.2 | async-start | bytes 8912896 | tf_op jit(solution)/shard_map/all_gather | solution.py:431
  9.4 1.0 copy-start.17
  11.2 20.9 %copy-start.18 = (bf16[1024,128]{1,0:T(8,128)(2,1)S(1)}, bf16[1024,128]{1,0:T(8,128)(2,1)}, u32[]{:S(2)}) copy-start(bf16[1024,128]{1,0:T(8,128)(2,1)} %param.19) | copy-start | bytes 786436
  11.2 10.6 %collective-permute-start.3 = (bf16[800,128]{1,0:T(8,128)(2,1)S(1)}, bf16[800,128]{1,0:T(8,128)(2,1)S(1)}, u32[]{:S(2)}, u32[]{:S(2)}) collective-permute-start(bf16[800,128]{1,0:T(8,128)(2,1)S(1)} %bitcast.90), channel_id=1, source_target_pairs={{0,33},{1,97},{32,1},{33,65},{64,32},{65,96},{96,0},{97,64},{2,35}... | collective-permute-start | bytes 614408 | tf_op jit(solution)/shard_map/ppermute | solution.py:401
  16.0 5.9 %collective-permute-start.2 = (bf16[800,128]{1,0:T(8,128)(2,1)S(1)}, bf16[800,128]{1,0:T(8,128)(2,1)S(1)}, u32[]{:S(2)}, u32[]{:S(2)}) collective-permute-start(bf16[800,128]{1,0:T(8,128)(2,1)S(1)} %bitcast.91), channel_id=1, source_target_pairs={{0,1},{1,65},{32,33},{33,97},{64,0},{65,64},{96,32},{97,96},{2,3},... | collective-permute-start | bytes 614408 | tf_op jit(solution)/shard_map/ppermute | solution.py:401
  18.0 7.1 %collective-permute-start.1 = (bf16[800,128]{1,0:T(8,128)(2,1)S(1)}, bf16[800,128]{1,0:T(8,128)(2,1)S(1)}, u32[]{:S(2)}, u32[]{:S(2)}) collective-permute-start(bf16[800,128]{1,0:T(8,128)(2,1)S(1)} %bitcast.92), channel_id=1, source_target_pairs={{0,32},{1,96},{32,0},{33,64},{64,33},{65,97},{96,1},{97,65},{2,34}... | collective-permute-start | bytes 614408 | tf_op jit(solution)/shard_map/ppermute | solution.py:401
  18.3 9.0 %collective-permute-start = (bf16[800,128]{1,0:T(8,128)(2,1)S(1)}, bf16[800,128]{1,0:T(8,128)(2,1)S(1)}, u32[]{:S(2)}, u32[]{:S(2)}) collective-permute-start(bf16[800,128]{1,0:T(8,128)(2,1)S(1)} %bitcast.93), channel_id=1, source_target_pairs={{0,0},{1,64},{32,32},{33,96},{64,1},{65,65},{96,33},{97,97},{2,2},... | collective-permute-start | bytes 614408 | tf_op jit(solution)/shard_map/ppermute | solution.py:401
  21.8 13.8 %copy-start.19 = (bf16[128,1024]{1,0:T(8,128)(2,1)S(1)}, bf16[128,1024]{1,0:T(8,128)(2,1)}, u32[]{:S(2)}) copy-start(bf16[128,1024]{1,0:T(8,128)(2,1)} %param.18) | copy-start | bytes 786436
  27.5 9.0 %collective-permute-start.10 = (bf16[4,544,128]{2,1,0:T(8,128)(2,1)S(1)}, bf16[4,544,128]{2,1,0:T(8,128)(2,1)S(1)}, u32[]{:S(2)}, u32[]{:S(2)}) collective-permute-start(bf16[4,544,128]{2,1,0:T(8,128)(2,1)S(1)} %pad_maximum_fusion.1.rest_0_), channel_id=1, source_target_pairs={{0,1},{1,0},{2,3},{3,2},{4,5},{5,4},{6,7},{7,6},{8,9},{9,8},{10,11... | collective-permute-start | bytes 1671176 | tf_op jit(solution)/shard_map/ppermute | solution.py:367
  27.6 26.2 %collective-permute-start.7 = (bf16[4,544,128]{2,1,0:T(8,128)(2,1)S(1)}, bf16[4,544,128]{2,1,0:T(8,128)(2,1)S(1)}, u32[]{:S(2)}, u32[]{:S(2)}) collective-permute-start(bf16[4,544,128]{2,1,0:T(8,128)(2,1)S(1)} %pad_maximum_fusion.1.rest_0_), channel_id=1, source_target_pairs={{0,24},{8,0},{16,8},{24,16},{1,25},{9,1},{17,9},{25,17},{2,26},{10... | collective-permute-start | bytes 1671176 | tf_op jit(solution)/shard_map/ppermute | solution.py:363
  30.4 23.4 %collective-permute-start.8 = (bf16[4,544,128]{2,1,0:T(8,128)(2,1)S(1)}, bf16[4,544,128]{2,1,0:T(8,128)(2,1)}, u32[]{:S(2)}, u32[]{:S(2)}) collective-permute-start(bf16[4,544,128]{2,1,0:T(8,128)(2,1)S(1)} %pad_maximum_fusion.1.rest_0_), channel_id=1, source_target_pairs={{0,8},{8,16},{16,24},{24,0},{1,9},{9,17},{17,25},{25,1},{2,10},{10... | collective-permute-start | bytes 1671176 | tf_op jit(solution)/shard_map/ppermute | solution.py:363
  30.4 25.7 %collective-permute-start.9 = (bf16[4,544,128]{2,1,0:T(8,128)(2,1)S(1)}, bf16[4,544,128]{2,1,0:T(8,128)(2,1)}, u32[]{:S(2)}, u32[]{:S(2)}) collective-permute-start(bf16[4,544,128]{2,1,0:T(8,128)(2,1)S(1)} %pad_maximum_fusion.1.rest_0_), channel_id=1, source_target_pairs={{0,16},{8,24},{16,0},{24,8},{1,17},{9,25},{17,1},{25,9},{2,18},{10... | collective-permute-start | bytes 1671176 | tf_op jit(solution)/shard_map/ppermute | solution.py:363
  36.5 22.8 %copy-start.20 = (bf16[256]{0:T(256)(128)(2,1)S(1)}, bf16[256]{0:T(256)(128)(2,1)}, u32[]{:S(2)}) copy-start(bf16[256]{0:T(256)(128)(2,1)} %param.17) | copy-start | bytes 1540
  36.5 22.8 %copy-start.15 = (bf16[128,2048]{1,0:T(8,128)(2,1)S(1)}, bf16[128,2048]{1,0:T(8,128)(2,1)}, u32[]{:S(2)}) copy-start(bf16[128,2048]{1,0:T(8,128)(2,1)} %param.16) | copy-start | bytes 1572868
  44.7 17.3 %copy-start.13 = (f32[4,1,512]{2,1,0:T(1,128)}, f32[4,1,512]{2,1,0:T(1,128)S(1)}, u32[]{:S(2)}) copy-start(f32[4,1,512]{2,1,0:T(1,128)S(1)} %get-tuple-element.52.rest_7_) | copy-start | bytes 24580
  53.8 13.2 %copy-start.1 = (bf16[4,544,128]{2,1,0:T(8,128)(2,1)}, bf16[4,544,128]{2,1,0:T(8,128)(2,1)S(1)}, u32[]{:S(2)}) copy-start(bf16[4,544,128]{2,1,0:T(8,128)(2,1)S(1)} %collective-permute-done.7.rest_0_) | copy-start | bytes 1671172
  56.2 10.7 %collective-permute-start.11 = (bf16[4,544,128]{2,1,0:T(8,128)(2,1)S(1)}, bf16[4,544,128]{2,1,0:T(8,128)(2,1)}, u32[]{:S(2)}, u32[]{:S(2)}) collective-permute-start(bf16[4,544,128]{2,1,0:T(8,128)(2,1)S(1)} %collective-permute-done.7.rest_0_), channel_id=1, source_target_pairs={{0,1},{1,0},{2,3},{3,2},{4,5},{5,4},{6,7},{7,6},{8,9},{9,8},{10,11... | collective-permute-start | bytes 1671176 | tf_op jit(solution)/shard_map/ppermute | solution.py:367
  58.8 11.1 %collective-permute-start.12 = (bf16[4,544,128]{2,1,0:T(8,128)(2,1)}, bf16[4,544,128]{2,1,0:T(8,128)(2,1)}, u32[]{:S(2)}, u32[]{:S(2)}) collective-permute-start(bf16[4,544,128]{2,1,0:T(8,128)(2,1)} %collective-permute-done.8.rest_2_), channel_id=1, source_target_pairs={{0,1},{1,0},{2,3},{3,2},{4,5},{5,4},{6,7},{7,6},{8,9},{9,8},{10,11... | collective-permute-start | bytes 1671176 | tf_op jit(solution)/shard_map/ppermute | solution.py:367
  58.9 11.0 %collective-permute-start.13 = (bf16[4,544,128]{2,1,0:T(8,128)(2,1)}, bf16[4,544,128]{2,1,0:T(8,128)(2,1)}, u32[]{:S(2)}, u32[]{:S(2)}) collective-permute-start(bf16[4,544,128]{2,1,0:T(8,128)(2,1)} %collective-permute-done.9.rest_4_), channel_id=1, source_target_pairs={{0,1},{1,0},{2,3},{3,2},{4,5},{5,4},{6,7},{7,6},{8,9},{9,8},{10,11... | collective-permute-start | bytes 1671176 | tf_op jit(solution)/shard_map/ppermute | solution.py:367
  59.4 36.1 %collective-permute-start.4 = (bf16[136,2048]{1,0:T(8,128)(2,1)S(1)}, bf16[136,2048]{1,0:T(8,128)(2,1)S(1)}, u32[]{:S(2)}, u32[]{:S(2)}) collective-permute-start(bf16[136,2048]{1,0:T(8,128)(2,1)S(1)} %fusion.1.rest_0_), channel_id=1, source_target_pairs={{0,6},{2,0},{4,2},{6,4},{1,7},{3,1},{5,3},{7,5},{8,14},{10,8},{12,... | collective-permute-start | bytes 1671176 | tf_op jit(solution)/shard_map/ppermute | solution.py:363
  61.9 33.5 %collective-permute-start.5 = (bf16[136,2048]{1,0:T(8,128)(2,1)S(1)}, bf16[136,2048]{1,0:T(8,128)(2,1)S(1)}, u32[]{:S(2)}, u32[]{:S(2)}) collective-permute-start(bf16[136,2048]{1,0:T(8,128)(2,1)S(1)} %fusion.1.rest_0_), channel_id=1, source_target_pairs={{0,2},{2,4},{4,6},{6,0},{1,3},{3,5},{5,7},{7,1},{8,10},{10,12},{12... | collective-permute-start | bytes 1671176 | tf_op jit(solution)/shard_map/ppermute | solution.py:363
  62.0 33.5 %all-to-all-start = ((bf16[8,128,256]{2,1,0:T(8,128)(2,1)}), bf16[8,128,256]{2,1,0:T(8,128)(2,1)S(1)}, u32[]{:S(2)}, u32[]{:S(2)}) async-start(bf16[8,128,256]{2,1,0:T(8,128)(2,1)} %bitcast.88), calls=%async_computation | async-start | bytes 1048576 | tf_op jit(solution)/shard_map/all_to_all | solution.py:429
  67.0 28.5 %collective-permute-start.6 = (bf16[136,2048]{1,0:T(8,128)(2,1)S(1)}, bf16[136,2048]{1,0:T(8,128)(2,1)S(1)}, u32[]{:S(2)}, u32[]{:S(2)}) collective-permute-start(bf16[136,2048]{1,0:T(8,128)(2,1)S(1)} %fusion.1.rest_0_), channel_id=1, source_target_pairs={{0,4},{2,6},{4,0},{6,2},{1,5},{3,7},{5,1},{7,3},{8,12},{10,14},{12... | collective-permute-start | bytes 1671176 | tf_op jit(solution)/shard_map/ppermute | solution.py:363
  69.9 1.1 copy-start.2
  71.0 0.7 copy-start.14
  95.5 12.8 %collective-permute-start.14 = (bf16[136,2048]{1,0:T(8,128)(2,1)S(1)}, bf16[136,2048]{1,0:T(8,128)(2,1)}, u32[]{:S(2)}, u32[]{:S(2)}) collective-permute-start(bf16[136,2048]{1,0:T(8,128)(2,1)S(1)} %fusion.1.rest_0_), channel_id=1, source_target_pairs={{0,1},{1,0},{2,3},{3,2},{4,5},{5,4},{6,7},{7,6},{8,9},{9,8},{10,11... | collective-permute-start | bytes 1671176 | tf_op jit(solution)/shard_map/ppermute | solution.py:367
  95.6 12.7 %collective-permute-start.15 = (bf16[136,2048]{1,0:T(8,128)(2,1)S(1)}, bf16[136,2048]{1,0:T(8,128)(2,1)}, u32[]{:S(2)}, u32[]{:S(2)}) collective-permute-start(bf16[136,2048]{1,0:T(8,128)(2,1)S(1)} %collective-permute-done.4.rest_2_), channel_id=1, source_target_pairs={{0,1},{1,0},{2,3},{3,2},{4,5},{5,4},{6,7},{7,6},{8,9},{9,8},{10,11... | collective-permute-start | bytes 1671176 | tf_op jit(solution)/shard_map/ppermute | solution.py:367
  96.1 12.2 %collective-permute-start.16 = (bf16[136,2048]{1,0:T(8,128)(2,1)S(1)}, bf16[136,2048]{1,0:T(8,128)(2,1)}, u32[]{:S(2)}, u32[]{:S(2)}) collective-permute-start(bf16[136,2048]{1,0:T(8,128)(2,1)S(1)} %collective-permute-done.5.rest_4_), channel_id=1, source_target_pairs={{0,1},{1,0},{2,3},{3,2},{4,5},{5,4},{6,7},{7,6},{8,9},{9,8},{10,11... | collective-permute-start | bytes 1671176 | tf_op jit(solution)/shard_map/ppermute | solution.py:367
  96.3 11.9 %collective-permute-start.17 = (bf16[136,2048]{1,0:T(8,128)(2,1)S(1)}, bf16[136,2048]{1,0:T(8,128)(2,1)}, u32[]{:S(2)}, u32[]{:S(2)}) collective-permute-start(bf16[136,2048]{1,0:T(8,128)(2,1)S(1)} %collective-permute-done.6.rest_6_), channel_id=1, source_target_pairs={{0,1},{1,0},{2,3},{3,2},{4,5},{5,4},{6,7},{7,6},{8,9},{9,8},{10,11... | collective-permute-start | bytes 1671176 | tf_op jit(solution)/shard_map/ppermute | solution.py:367
  96.6 11.7 %all-to-all-start.1 = ((bf16[16,64,128]{2,1,0:T(8,128)(2,1)}), bf16[16,64,128]{2,1,0:T(8,128)(2,1)S(1)}, u32[]{:S(2)}, u32[]{:S(2)}) async-start(bf16[16,64,128]{2,1,0:T(8,128)(2,1)} %attend_last.1), calls=%async_computation.1 | async-start | bytes 524288 | tf_op jit(solution)/shard_map/all_to_all | solution.py:439
  112.2 12.5 %collective-permute-start.19 = (bf16[128,2048]{1,0:T(8,128)(2,1)}, bf16[128,2048]{1,0:T(8,128)(2,1)S(1)}, u32[]{:S(2)}, u32[]{:S(2)}) collective-permute-start(bf16[128,2048]{1,0:T(8,128)(2,1)} %get-tuple-element.62.rest_0_), channel_id=1, source_target_pairs={{0,6},{2,0},{4,2},{6,4},{1,7},{3,1},{5,3},{7,5},{8,14},{10,8},{12,... | collective-permute-start | bytes 1572872 | tf_op jit(solution)/shard_map/ppermute | solution.py:363
  113.7 24.5 %collective-permute-start.21 = (bf16[128,2048]{1,0:T(8,128)(2,1)}, bf16[128,2048]{1,0:T(8,128)(2,1)S(1)}, u32[]{:S(2)}, u32[]{:S(2)}) collective-permute-start(bf16[128,2048]{1,0:T(8,128)(2,1)} %get-tuple-element.62.rest_0_), channel_id=1, source_target_pairs={{0,2},{2,4},{4,6},{6,0},{1,3},{3,5},{5,7},{7,1},{8,10},{10,12},{12... | collective-permute-start | bytes 1572872 | tf_op jit(solution)/shard_map/ppermute | solution.py:363
  113.7 27.8 %collective-permute-start.23 = (bf16[128,2048]{1,0:T(8,128)(2,1)}, bf16[128,2048]{1,0:T(8,128)(2,1)S(1)}, u32[]{:S(2)}, u32[]{:S(2)}) collective-permute-start(bf16[128,2048]{1,0:T(8,128)(2,1)} %get-tuple-element.62.rest_0_), channel_id=1, source_target_pairs={{0,4},{2,6},{4,0},{6,2},{1,5},{3,7},{5,1},{7,3},{8,12},{10,14},{12... | collective-permute-start | bytes 1572872 | tf_op jit(solution)/shard_map/ppermute | solution.py:363
  115.0 27.5 %collective-permute-start.18 = (bf16[128,2048]{1,0:T(8,128)(2,1)}, bf16[128,2048]{1,0:T(8,128)(2,1)S(1)}, u32[]{:S(2)}, u32[]{:S(2)}) collective-permute-start(bf16[128,2048]{1,0:T(8,128)(2,1)} %get-tuple-element.62.rest_0_), channel_id=1, source_target_pairs={{0,1},{1,0},{2,3},{3,2},{4,5},{5,4},{6,7},{7,6},{8,9},{9,8},{10,11... | collective-permute-start | bytes 1572872 | tf_op jit(solution)/shard_map/ppermute | solution.py:367
  124.7 18.6 %collective-permute-start.20 = (bf16[128,2048]{1,0:T(8,128)(2,1)S(1)}, bf16[128,2048]{1,0:T(8,128)(2,1)S(1)}, u32[]{:S(2)}, u32[]{:S(2)}) collective-permute-start(bf16[128,2048]{1,0:T(8,128)(2,1)S(1)} %collective-permute-done.19.rest_2_), channel_id=1, source_target_pairs={{0,1},{1,0},{2,3},{3,2},{4,5},{5,4},{6,7},{7,6},{8,9},{9,8},{10,11... | collective-permute-start | bytes 1572872 | tf_op jit(solution)/shard_map/ppermute | solution.py:367
  137.5 0.8 copy-start.3
  138.3 5.9 %collective-permute-start.22 = (bf16[128,2048]{1,0:T(8,128)(2,1)S(1)}, bf16[128,2048]{1,0:T(8,128)(2,1)}, u32[]{:S(2)}, u32[]{:S(2)}) collective-permute-start(bf16[128,2048]{1,0:T(8,128)(2,1)S(1)} %collective-permute-done.21.rest_4_), channel_id=1, source_target_pairs={{0,1},{1,0},{2,3},{3,2},{4,5},{5,4},{6,7},{7,6},{8,9},{9,8},{10,11... | collective-permute-start | bytes 1572872 | tf_op jit(solution)/shard_map/ppermute | solution.py:367
  140.7 0.8 copy-start.5
  141.5 2.6 %collective-permute-start.24 = (bf16[128,2048]{1,0:T(8,128)(2,1)S(1)}, bf16[128,2048]{1,0:T(8,128)(2,1)}, u32[]{:S(2)}, u32[]{:S(2)}) collective-permute-start(bf16[128,2048]{1,0:T(8,128)(2,1)S(1)} %collective-permute-done.23.rest_6_), channel_id=1, source_target_pairs={{0,1},{1,0},{2,3},{3,2},{4,5},{5,4},{6,7},{7,6},{8,9},{9,8},{10,11... | collective-permute-start | bytes 1572872 | tf_op jit(solution)/shard_map/ppermute | solution.py:367
  141.5 0.8 copy-start.7
  142.5 0.8 copy-start.9
  143.3 0.8 copy-start.11
  144.2 14.9 %slice-start = ((s8[8388608]{0:T(1024)(128)(4,1)}), s8[4194304]{0:T(1024)(128)(4,1)S(1)}, s32[]{:S(2)}) async-start(s8[8388608]{0:T(1024)(128)(4,1)} %bitcast.79), calls=%async_computation.3 | async-start | bytes 8388608
  144.2 1.2 copy-start.4
  145.4 1.3 copy-start.6
  146.6 1.0 copy-start.8
  147.7 1.0 copy-start.10
  148.7 1.0 copy-start.12
  149.8 9.4 %slice-start.1 = ((s8[8388608]{0:T(1024)(128)(4,1)}), s8[4194304]{0:T(1024)(128)(4,1)S(1)}, s32[]{:S(2)}) async-start(s8[8388608]{0:T(1024)(128)(4,1)} %bitcast.79), calls=%async_computation.4 | async-start | bytes 8388608
  161.9 10.9 %collective-permute-start.25 = (bf16[1024,256]{1,0:T(8,128)(2,1)}, bf16[1024,256]{1,0:T(8,128)(2,1)}, u32[]{:S(2)}, u32[]{:S(2)}) collective-permute-start(bf16[1024,256]{1,0:T(8,128)(2,1)} %get-tuple-element.66), channel_id=1, source_target_pairs={{0,1},{1,0},{2,3},{3,2},{4,5},{5,4},{6,7},{7,6},{8,9},{9,8},{10,11... | collective-permute-start | bytes 1572872 | tf_op jit(solution)/shard_map/ppermute | solution.py:367
  162.4 3.4 %copy-start = (bf16[4096,1024]{1,0:T(8,128)(2,1)S(1)}, bf16[4096,1024]{1,0:T(8,128)(2,1)}, u32[]{:S(2)}) copy-start(bf16[4096,1024]{1,0:T(8,128)(2,1)} %all-gather.2.cloned.1.call-done.w_in) | copy-start | bytes 25165828
  167.8 6.3 %collective-permute-start.27 = (bf16[1024,256]{1,0:T(8,128)(2,1)S(1)}, bf16[1024,256]{1,0:T(8,128)(2,1)S(1)}, u32[]{:S(2)}, u32[]{:S(2)}) collective-permute-start(bf16[1024,256]{1,0:T(8,128)(2,1)S(1)} %get-tuple-element.68), channel_id=1, source_target_pairs={{0,1},{1,0},{2,3},{3,2},{4,5},{5,4},{6,7},{7,6},{8,9},{9,8},{10,11... | collective-permute-start | bytes 1572872 | tf_op jit(solution)/shard_map/ppermute | solution.py:367
  170.2 6.0 %collective-permute-start.29 = (bf16[1024,256]{1,0:T(8,128)(2,1)S(1)}, bf16[1024,256]{1,0:T(8,128)(2,1)S(1)}, u32[]{:S(2)}, u32[]{:S(2)}) collective-permute-start(bf16[1024,256]{1,0:T(8,128)(2,1)S(1)} %get-tuple-element.70), channel_id=1, source_target_pairs={{0,1},{1,0},{2,3},{3,2},{4,5},{5,4},{6,7},{7,6},{8,9},{9,8},{10,11... | collective-permute-start | bytes 1572872 | tf_op jit(solution)/shard_map/ppermute | solution.py:367
  172.7 4.5 %collective-permute-start.31 = (bf16[1024,256]{1,0:T(8,128)(2,1)S(1)}, bf16[1024,256]{1,0:T(8,128)(2,1)S(1)}, u32[]{:S(2)}, u32[]{:S(2)}) collective-permute-start(bf16[1024,256]{1,0:T(8,128)(2,1)S(1)} %get-tuple-element.72), channel_id=1, source_target_pairs={{0,1},{1,0},{2,3},{3,2},{4,5},{5,4},{6,7},{7,6},{8,9},{9,8},{10,11... | collective-permute-start | bytes 1572872 | tf_op jit(solution)/shard_map/ppermute | solution.py:367
  174.0 14.6 %collective-permute-start.26 = (bf16[1024,256]{1,0:T(8,128)(2,1)S(1)}, bf16[1024,256]{1,0:T(8,128)(2,1)S(1)}, u32[]{:S(2)}, u32[]{:S(2)}) collective-permute-start(bf16[1024,256]{1,0:T(8,128)(2,1)S(1)} %add_convert_fusion.3), channel_id=1, source_target_pairs={{0,4},{2,6},{4,0},{6,2},{1,5},{3,7},{5,1},{7,3},{8,12},{10,14},{12... | collective-permute-start | bytes 1572872 | tf_op jit(solution)/shard_map/ppermute | solution.py:363
  174.2 26.3 %collective-permute-start.28 = (bf16[1024,256]{1,0:T(8,128)(2,1)S(1)}, bf16[1024,256]{1,0:T(8,128)(2,1)S(1)}, u32[]{:S(2)}, u32[]{:S(2)}) collective-permute-start(bf16[1024,256]{1,0:T(8,128)(2,1)S(1)} %add_convert_fusion.2), channel_id=1, source_target_pairs={{0,2},{2,4},{4,6},{6,0},{1,3},{3,5},{5,7},{7,1},{8,10},{10,12},{12... | collective-permute-start | bytes 1572872 | tf_op jit(solution)/shard_map/ppermute | solution.py:363
  176.3 24.2 %collective-permute-start.30 = (bf16[1024,256]{1,0:T(8,128)(2,1)S(1)}, bf16[1024,256]{1,0:T(8,128)(2,1)S(1)}, u32[]{:S(2)}, u32[]{:S(2)}) collective-permute-start(bf16[1024,256]{1,0:T(8,128)(2,1)S(1)} %add_convert_fusion.1), channel_id=1, source_target_pairs={{0,6},{2,0},{4,2},{6,4},{1,7},{3,1},{5,3},{7,5},{8,14},{10,8},{12,... | collective-permute-start | bytes 1572872 | tf_op jit(solution)/shard_map/ppermute | solution.py:363
Sparse Core Ops, SparseCore 0:
  56.3 73.9 all-gather.1

commit v2 on v1

--- a/solution.py
+++ b/solution.py
@@ -2,6 +2,7 @@
 
 import jax
 import jax.numpy as jnp
+import numpy as np
 from jax import lax
 from jax.experimental import pallas as pl
 from jax.experimental.pallas import tpu as pltpu
@@ -21,6 +22,10 @@
 far_below = -1e30
 lowest = -1e29
 RING = (1, 3, 2)
+
+
+def in_hbm(arrays):
+    return [pltpu.with_memory_space_constraint(a, pltpu.HBM) for a in arrays]
 
 
 DIMS = (((1,), (0,)), ((), ()))
@@ -74,7 +79,7 @@
         acc_ref[pq, :, cols] = acc_ref[pq, :, cols] * shrink_ref[:, cols] + product
 
 
-def attend_kernel(n_arr, first, last, sc, qt_ref, *rest):
+def attend_kernel(n_arr, first, last, tab, zeros_q, qt_ref, *rest):
     kv_in, rest = rest[:n_arr], rest[n_arr:]
     if first:
         state_in = ()
@@ -83,6 +88,7 @@
     if last:
         out_ref, rest = rest[0], rest[1:]
     m_ref, l_ref, acc_ref, kv, ke, qa, qb, s_a, s_b, p_a, p_b, shrink_a, shrink_b, zero_s, todo, sems = rest
+    at_keys = 2 if first else 6
     copies = [
         pltpu.make_async_copy(kv_in[n], kv.at[pl.ds(4 * n, 4)], sems.at[n]) for n in range(n_arr)
     ]
@@ -126,11 +132,11 @@
 
     def list_keys(i, count):
         arr = i // 4
-        k_start = ((i % 4) ^ sc[7 + 2 * arr]) * 4096 + sc[6 + 2 * arr]
+        k_start = ((i % 4) ^ tab[at_keys + 1 + 2 * arr]) * 4096 + tab[at_keys + 2 * arr]
         k_zero = zero_s[i]
         for pq in range(4):
-            ahead = (pq ^ sc[1]) * 4096 + sc[0] - k_start
-            q_zero = sc[2 + pq]
+            ahead = (pq ^ tab[1]) * 4096 + tab[0] - k_start
+            q_zero = zeros_q[pq]
             live = (ahead > -HALF) & jnp.logical_not((k_zero == HALF) & (q_zero == 0))
             full = (ahead >= HALF) & ((k_zero == 0) | (q_zero == HALF))
             todo[count, 0] = i
@@ -158,7 +164,7 @@
 
         @pl.when(todo[t, 3] == 1)
         def _():
-            hide(s_now, todo[t, 2], zero_s[todo[t, 0]], sc[2 + todo[t, 1]])
+            hide(s_now, todo[t, 2], zero_s[todo[t, 0]], zeros_q[todo[t, 1]])
 
         score(todo[t + 1, 0], todo[t + 1, 1], kv, ke, qa, qb, s_later)
         weigh(todo[t, 1], s_now, p_now, m_ref, l_ref, shrink_now)
@@ -182,7 +188,7 @@
 
         def finish(pq, carry):
             out = (acc_ref[pq] / l_ref[pq]).astype(jnp.bfloat16)
-            block = pq ^ sc[1]
+            block = pq ^ tab[1]
             for quarter in range(4):
                 out_ref[quarter * 4 + block] = out[:, 128 * quarter : 128 * (quarter + 1)]
             return carry
@@ -190,7 +196,7 @@
         lax.fori_loop(0, 4, finish, 0)
 
 
-def attend(scalars, qt, arrays, state, first, last):
+def attend(table, zeros_q, qt, arrays, state, first, last):
     n_arr = len(arrays)
     vmem = pl.BlockSpec(memory_space=pltpu.VMEM)
     shapes = [
@@ -224,8 +230,9 @@
     return pl.pallas_call(
         functools.partial(attend_kernel, n_arr, first, last),
         out_shape=out_shape,
-        in_specs=[pl.BlockSpec(memory_space=pltpu.SMEM), vmem]
-        + [pl.BlockSpec(memory_space=pl.ANY)] * n_arr
+        in_specs=[pl.BlockSpec(memory_space=pltpu.SMEM)] * 2
+        + [vmem]
+        + [pl.BlockSpec(memory_space=pltpu.HBM)] * n_arr
         + [vmem] * len(state),
         out_specs=out_specs,
         scratch_shapes=scratch,
@@ -234,15 +241,15 @@
             flops=4_000_000_000 * n_arr, bytes_accessed=1_000_000 * n_arr, transcendentals=0
         ),
         name="attend_first" if first else ("attend_last" if last else "attend_more"),
-    )(scalars, qt, *arrays, *state)
+    )(table, zeros_q, qt, *in_hbm(arrays), *state)
 
 
 def dense_kernel(sc, att_ref, res_ref, *rest):
     w_in, (mid_ref, gain_ref, w_all, sems) = rest[:8], rest[8:]
     copies = []
     for n in range(8):
-        at = pl.multiple_of(sc[n], 128)
-        lanes = pl.ds(pl.multiple_of(sc[n] * 2, 256), 256)
+        at = pl.multiple_of(sc[18 + n], 128)
+        lanes = pl.ds(pl.multiple_of(sc[18 + n] * 2, 256), 256)
         copies.append(pltpu.make_async_copy(w_in[n].at[pl.ds(0, 128)], w_all.at[pl.ds(at, 128)], sems.at[n]))
         copies.append(
             pltpu.make_async_copy(w_in[n].at[pl.ds(128, 8), pl.ds(0, 256)], gain_ref.at[:, lanes], sems.at[8 + n])
@@ -269,38 +276,38 @@
             jax.ShapeDtypeStruct((128, D), jnp.bfloat16),
             jax.ShapeDtypeStruct((8, D), jnp.bfloat16),
         ],
-        in_specs=[pl.BlockSpec(memory_space=pltpu.SMEM), vmem, vmem] + [pl.BlockSpec(memory_space=pl.ANY)] * 8,
+        in_specs=[pl.BlockSpec(memory_space=pltpu.SMEM), vmem, vmem] + [pl.BlockSpec(memory_space=pltpu.HBM)] * 8,
         out_specs=[vmem, vmem],
         scratch_shapes=[pltpu.VMEM((1024, D), jnp.bfloat16), pltpu.SemaphoreType.DMA((16,))],
         compiler_params=pltpu.CompilerParams(vmem_limit_bytes=24 * 1024 * 1024),
         cost_estimate=pl.CostEstimate(flops=1_000_000_000, bytes_accessed=4_000_000, transcendentals=0),
         name="dense",
-    )(scalars, att, res, *pieces)
+    )(scalars, att, res, *in_hbm(pieces))
 
 
 def up_kernel(sc, gain_ref, w_in, *rest):
-    mids, (h_ref, own_ref, w_up, mid_all, sems) = rest[:8], rest[8:]
+    mids, (h_ref, own_ref, w_up, mid_all, normed, sems) = rest[:8], rest[8:]
     fetches = [pltpu.make_async_copy(mids[n], mid_all.at[pl.ds(128 * n, 128)], sems.at[16 + n]) for n in range(8)]
     copies = [
         pltpu.make_async_copy(w_in.at[pl.ds(256 * n, 128)], w_up.at[pl.ds(128 * n, 128)], sems.at[n]) for n in range(16)
     ]
-    for copy in copies + fetches:
+    for copy in fetches + copies:
         copy.start()
     gain = gain_ref[0:1, :].astype(jnp.float32)
+    lanes = pl.ds(pl.multiple_of(sc[34], 256), 256)
+    for n in range(8):
+        fetches[n].wait()
+        own_ref[pl.ds(pl.multiple_of(sc[26 + n], 128), 128), :] = mid_all[128 * n : 128 * (n + 1), lanes]
+        wide = mid_all[128 * n : 128 * (n + 1), :].astype(jnp.float32)
+        scale = lax.rsqrt(jnp.sum(wide * wide, axis=-1, keepdims=True) / D + eps)
+        normed[128 * n : 128 * (n + 1), :] = (wide * scale * gain).astype(jnp.bfloat16)
     for copy in copies:
         copy.wait()
-    lanes = pl.ds(pl.multiple_of(sc[8], 256), 256)
     for n in range(0, 8, 2):
-        for k in range(2):
-            fetches[n + k].wait()
-            own_ref[pl.ds(pl.multiple_of(sc[n + k], 128), 128), :] = mid_all[128 * (n + k) : 128 * (n + k + 1), lanes]
-        wide = mid_all[128 * n : 128 * (n + 2), :].astype(jnp.float32)
-        scale = lax.rsqrt(jnp.sum(wide * wide, axis=-1, keepdims=True) / D + eps)
-        normed = (wide * scale * gain).astype(jnp.bfloat16)
-        h = jnp.dot(normed, w_up[...], preferred_element_type=jnp.float32)
+        h = jnp.dot(normed[128 * n : 128 * (n + 2), :], w_up[...], preferred_element_type=jnp.float32)
         h = jnp.square(jnp.maximum(h, 0.0)).astype(jnp.bfloat16)
         for k in range(2):
-            h_ref[pl.ds(pl.multiple_of(sc[n + k], 128), 128), :] = h[128 * k : 128 * (k + 1)]
+            h_ref[pl.ds(pl.multiple_of(sc[26 + n + k], 128), 128), :] = h[128 * k : 128 * (k + 1)]
 
 
 def up(scalars, gain, w, mids):
@@ -311,51 +318,60 @@
             jax.ShapeDtypeStruct((1024, 1024), jnp.bfloat16),
             jax.ShapeDtypeStruct((1024, 256), jnp.bfloat16),
         ],
-        in_specs=[pl.BlockSpec(memory_space=pltpu.SMEM), vmem] + [pl.BlockSpec(memory_space=pl.ANY)] * 9,
+        in_specs=[pl.BlockSpec(memory_space=pltpu.SMEM), vmem] + [pl.BlockSpec(memory_space=pltpu.HBM)] * 9,
         out_specs=[vmem, vmem],
         scratch_shapes=[
             pltpu.VMEM((D, 1024), jnp.bfloat16),
+            pltpu.VMEM((1024, D), jnp.bfloat16),
             pltpu.VMEM((1024, D), jnp.bfloat16),
             pltpu.SemaphoreType.DMA((24,)),
         ],
         compiler_params=pltpu.CompilerParams(vmem_limit_bytes=40 * 1024 * 1024),
         cost_estimate=pl.CostEstimate(flops=4_300_000_000, bytes_accessed=8_000_000, transcendentals=0),
         name="up",
-    )(scalars, gain, w, *mids)
-
-
-def down_kernel(sc, h_ref, w_in, mine_ref, other_ref, w_down, sems):
+    )(scalars, gain, *in_hbm([w, *mids]))
+
+
+def down_kernel(steps, sc, h_ref, w_in, *rest):
+    count = len(steps)
+    outs, (w_down, sems) = rest[: 2 * count], rest[2 * count :]
     copies = []
-    for k in range(4):
-        at = pl.multiple_of((sc[0] + k) * 256 + 128, 128)
-        copies.append(pltpu.make_async_copy(w_in.at[pl.ds(at, 128)], w_down.at[pl.ds(128 * k, 128)], sems.at[k]))
+    for n, r in enumerate(steps):
+        for k in range(4):
+            at = pl.multiple_of((sc[36 + r] + k) * 256 + 128, 128)
+            copies.append(
+                pltpu.make_async_copy(
+                    w_in.at[pl.ds(at, 128)], w_down.at[pl.ds(128 * (4 * n + k), 128)], sems.at[4 * n + k]
+                )
+            )
     for copy in copies:
         copy.start()
-    for copy in copies:
-        copy.wait()
-    for n, out_ref in ((1 - sc[1], other_ref), (sc[1], mine_ref)):
-        rows = w_down[pl.ds(pl.multiple_of(n * 256, 256), 256), :]
-        product = lax.dot_general(
-            h_ref[...], rows, (((1,), (1,)), ((), ())), preferred_element_type=jnp.float32
-        )
-        out_ref[...] = product.astype(out_ref.dtype)
-
-
-def down(scalars, h, w):
+    for n in range(count):
+        for copy in copies[4 * n : 4 * n + 4]:
+            copy.wait()
+        for which, out_ref in ((1 - sc[35], outs[2 * n]), (sc[35], outs[2 * n + 1])):
+            rows = w_down[pl.ds(pl.multiple_of(512 * n + which * 256, 256), 256), :]
+            product = lax.dot_general(
+                h_ref[...], rows, (((1,), (1,)), ((), ())), preferred_element_type=jnp.float32
+            )
+            out_ref[...] = product.astype(out_ref.dtype)
+
+
+def down(scalars, h, w, steps):
+    count = len(steps)
     vmem = pl.BlockSpec(memory_space=pltpu.VMEM)
     return pl.pallas_call(
-        down_kernel,
-        out_shape=[
-            jax.ShapeDtypeStruct((1024, 256), jnp.bfloat16),
-            jax.ShapeDtypeStruct((1024, 256), jnp.bfloat16),
-        ],
-        in_specs=[pl.BlockSpec(memory_space=pltpu.SMEM), vmem, pl.BlockSpec(memory_space=pl.ANY)],
-        out_specs=[vmem, vmem],
-        scratch_shapes=[pltpu.VMEM((512, 1024), jnp.bfloat16), pltpu.SemaphoreType.DMA((4,))],
+        functools.partial(down_kernel, steps),
+        out_shape=[jax.ShapeDtypeStruct((1024, 256), jnp.bfloat16)] * (2 * count),
+        in_specs=[pl.BlockSpec(memory_space=pltpu.SMEM), vmem, pl.BlockSpec(memory_space=pltpu.HBM)],
+        out_specs=[vmem] * (2 * count),
+        scratch_shapes=[pltpu.VMEM((512 * count, 1024), jnp.bfloat16), pltpu.SemaphoreType.DMA((4 * count,))],
         compiler_params=pltpu.CompilerParams(vmem_limit_bytes=24 * 1024 * 1024),
-        cost_estimate=pl.CostEstimate(flops=1_100_000_000, bytes_accessed=4_000_000, transcendentals=0),
+        cost_estimate=pl.CostEstimate(
+            flops=1_100_000_000 * count, bytes_accessed=4_000_000, transcendentals=0
+        ),
         name="down",
-    )(scalars, h, w)
+    )(scalars, h, *in_hbm([w]))
 
 
 def shifted(value, axis, by):
@@ -367,8 +383,29 @@
     return lax.ppermute(value, "c", [(0, 1), (1, 0)])
 
 
+def places():
+    rows = []
+    for d in range(128):
+        z, y, x, c = d // 32, d // 8 % 4, d // 2 % 4, d % 2
+        mask = [(z & 1) | (k << 1) for k in range(2)]
+        row = [y * TOK + c * HALF, mask[c]]
+        for r in (0,) + RING:
+            for half in (c, 1 - c):
+                row += [(y + r) % 4 * TOK + half * HALF, mask[half]]
+        order = [((x + r) % 4, k) for r in (0,) + RING for k in (c, 1 - c)]
+        row += [xs * 256 + k * 128 for xs, k in order]
+        row += [k * 512 + xs * 128 for xs, k in order]
+        row += [(2 * x + c) * 256, c] + [(x + r) % 4 * 4 for r in range(4)]
+        rows.append(row)
+    return np.asarray(rows, np.int32)
+
+
+PLACES = places()
+
+
 def body(queries, keys, values, cum_gates, doc_ids, residual, w_out, norm_gain, w_up, w_down):
     z, y, x, c = (lax.axis_index(a) for a in ("z", "y", "x", "c"))
+    table = lax.dynamic_slice(jnp.asarray(PLACES), (((z * 4 + y) * 4 + x) * 2 + c, 0), (1, 40)).reshape(40)
 
     q_t = jnp.transpose(queries * jnp.bfloat16(0.125)).reshape(2, HD, 2, 4, 128)
     q_msg = jnp.transpose(q_t, (0, 2, 3, 1, 4)).reshape(2, 2, Q_ROWS, 128)
@@ -399,61 +436,49 @@
         half = (z >> 1) ^ (step >> 1)
         message = lax.dynamic_slice(messages, (head, half, 0, 0), (1, 1, KV_ROWS + Q_ROWS, 128))[0, 0]
         received.append(lax.ppermute(message, ("z", "c"), pairs))
-    qt = jnp.stack([r[KV_ROWS:] for r in received])
-    kv_own = jnp.stack([r[:KV_ROWS] for r in received])
-
-    kv_mine = [kv_own] + [shifted(kv_own, "y", r) for r in RING]
-
-    kv_own, w_out, residual, norm_gain, w_up, w_down = lax.optimization_barrier(
-        (kv_own, w_out, residual, norm_gain, w_up, w_down)
-    )
-    both = jnp.concatenate([w_up, jnp.transpose(w_down)], axis=0)
-
-    q_zero = HALF - jnp.sum(kv_own[:, KROWS + VROWS + 8 : KROWS + VROWS + 16].astype(jnp.float32), axis=(1, 2))
-    mask_a = (z & 1) | (c << 1)
-    mask_b = (z & 1) | ((1 - c) << 1)
-    base = [y * TOK + c * HALF, mask_a] + [q_zero[n].astype(jnp.int32) for n in range(4)]
-
-    def places(rs):
-        out = []
-        for r in rs:
-            at = ((y + r) % 4) * TOK
-            out += [at + c * HALF, mask_a, at + (1 - c) * HALF, mask_b]
-        return jnp.stack(base + out).astype(jnp.int32)
-
-    kv_near = partner(kv_own)
-    state = attend(places([0]), qt, [kv_own, kv_near], (), True, False)
     gain_row = jnp.pad(norm_gain[None], ((0, 7), (0, D - 256)))
     w_msg = jnp.concatenate([w_out, gain_row], axis=0)
     w_mine = [w_msg] + [shifted(w_msg, "x", r) for r in RING]
+
+    qt = jnp.stack([r[KV_ROWS:] for r in received])
+    kv_own = jnp.stack([r[:KV_ROWS] for r in received])
+
+    kv_mine = [kv_own] + [shifted(kv_own, "y", r) for r in RING]
+
+    kv_own, residual, w_up, w_down = lax.optimization_barrier((kv_own, residual, w_up, w_down))
+    both = jnp.concatenate([w_up, jnp.transpose(w_down)], axis=0)
+
+    docs_own = kv_own[:, KROWS + VROWS + 8 : KROWS + VROWS + 16].astype(jnp.float32)
+    zeros_q = (HALF - jnp.sum(docs_own, axis=(1, 2))).astype(jnp.int32)
+
+    kv_near = partner(kv_own)
+    state = attend(table, zeros_q, qt, [kv_own, kv_near], (), True, False)
     res = lax.all_to_all(residual.reshape(8, 128, 256), ("c", "x"), 0, 0, tiled=True)
     kv_mine[1:], state, both = lax.optimization_barrier((kv_mine[1:], state, both))
     both = lax.all_gather(both, ("z", "y"), axis=0, tiled=True)
     kv_other = [None] + [partner(piece) for piece in kv_mine[1:]]
     pieces = [piece for pair in zip(kv_mine[1:], kv_other[1:]) for piece in pair]
-    out = attend(places(RING), qt, pieces, state, False, True)
+    out = attend(table, zeros_q, qt, pieces, state, False, True)
 
     w_mine, res, out = lax.optimization_barrier((w_mine, res, out))
     w_pieces = [w for mine in w_mine for w in (mine, partner(mine))]
 
     attended = lax.all_to_all(out, ("x", "z"), 0, 0, tiled=True)
 
-    order = [((x + r) % 4, cs) for r in (0, 1, 3, 2) for cs in (c, 1 - c)]
-    rows_at = jnp.stack([xs * 256 + cs * 128 for xs, cs in order]).astype(jnp.int32)
-    middle, gain = dense(rows_at, attended, res, w_pieces)
+    middle, gain = dense(table, attended, res, w_pieces)
 
     mid_mine = [middle] + [shifted(middle, "x", r) for r in RING]
     mids = [m for mine in mid_mine for m in (mine, partner(mine))]
-    token_at = jnp.stack([cs * 512 + xs * 128 for xs, cs in order] + [(2 * x + c) * 256]).astype(jnp.int32)
-    hidden, middle_own = up(token_at, gain, both, mids)
-
-    total = middle_own.astype(jnp.float32)
-    for r in (2, 1, 3, 0):
-        mine, other = down(jnp.stack([((x + r) % 4) * 4, c]).astype(jnp.int32), hidden, both)
-        chip = mine.astype(jnp.float32) + partner(other).astype(jnp.float32)
-        if r:
-            chip = shifted(chip.astype(jnp.bfloat16), "x", -r).astype(jnp.float32)
-        total = total + chip
+    hidden, middle_own = up(table, gain, both, mids)
+
+    parts = {}
+    for steps in ((2,), (0,), (1, 3)):
+        products = down(table, hidden, both, steps)
+        for n, r in enumerate(steps):
+            parts[r] = products[2 * n + 1].astype(jnp.float32) + partner(products[2 * n]).astype(jnp.float32)
+    total = middle_own.astype(jnp.float32) + parts[0]
+    for r in (2, 1, 3):
+        total = total + shifted(parts[r].astype(jnp.bfloat16), "x", -r).astype(jnp.float32)
     return total.astype(jnp.bfloat16)
 
 

time: 209 us -> 197 us (0.943)
  local copies, waits for them, and re-layouts: 19.1 us -> 7.66 us
  blocking collectives: 0 us -> 11 us
  starting transfers between devices: 58.1 us -> 52.2 us
  waiting for transfers between devices: 63.9 us -> 60.2 us
  between operations: 16.6 us -> 14 us
    unnamed x47 -> x45, local copies, waits for them, and re-layouts: 15 us -> 3.85 us
    all_to_all x0 -> x1, blocking collectives: none -> 11 us  [body(): attended = lax.all_to_all(out, ('x', 'z'), 0, 0, tiled=True)]
    ppermute x12, waiting for transfers between devices: 42 us -> 50.5 us  [shifted(): return lax.ppermute(value, axis, [(i, (i - by) % n) for i in range(n)])]
    all_to_all x1 -> x0, waiting for transfers between devices: 7.65 us -> none  [body(): attended = lax.all_to_all(out, ('x', 'z'), 0, 0, tiled=True)]
    all_to_all x1, waiting for transfers between devices: 8.74 us -> 2.1 us  [body(): lax.all_to_all(residual.reshape(8, 128, 256), ('c', 'x'), 0, 0, tiled=True)]
    all_to_all x1 -> x0, starting transfers between devices: 3.9 us -> none  [body(): attended = lax.all_to_all(out, ('x', 'z'), 0, 0, tiled=True)]
    ppermute x16, waiting for transfers between devices: 0.04 us -> 2.8 us  [partner(): return lax.ppermute(value, 'c', [(0, 1), (1, 0)])]
    pallas_call x4 -> x3, Pallas kernels: 8.6 us -> 10.5 us  [down(): pl.pallas_call(functools.partial(down_kernel, steps), out_shape=[jax.Shap...]
  transfers between devices with their start and end apart: 35 -> 34, of which waited for: 10 -> 14; matrix products, arithmetic and copies ran while one was open for 2% -> 1% of each run, Pallas kernels for 16% -> 18%
where the time goes in v2:
time: 197 us; the launch traced here: 196 us
  waiting for transfers between devices  60.2 us (31%)
  starting transfers between devices  52.2 us (26%)
  Pallas kernels  46.4 us (24%)
  between operations  14 us (7%)
  blocking collectives  11 us (6%)
  local copies, waits for them, and re-layouts  7.66 us (4%)
  other arithmetic  4.69 us (2%)
    ppermute x12, waiting for transfers between devices, shifted(): return lax.ppermute(value, axis, [(i, (i - by) % n) for i in range(n)])  50.5 us
    pallas_call x2, Pallas kernels, attend(): pl.pallas_call(functools.partial(attend_kernel, n_arr, first, last), out_...  23.5 us
    ppermute x16, starting transfers between devices, partner(): return lax.ppermute(value, 'c', [(0, 1), (1, 0)])  21.8 us
    ppermute x12, starting transfers between devices, shifted(): return lax.ppermute(value, axis, [(i, (i - by) % n) for i in range(n)])  15.2 us
    all_to_all x1, blocking collectives, body(): attended = lax.all_to_all(out, ('x', 'z'), 0, 0, tiled=True)  11 us
    pallas_call x3, Pallas kernels, down(): pl.pallas_call(functools.partial(down_kernel, steps), out_shape=[jax.Shap...  10.5 us
    ppermute x4, starting transfers between devices, body(): received.append(lax.ppermute(message, ('z', 'c'), pairs))  10 us
    pallas_call x1, Pallas kernels, up(): pl.pallas_call(up_kernel, out_shape=[jax.ShapeDtypeStruct((1024, 1024), j...  8.63 us
  transfers between devices with their start and end apart: 34, of which 14 were waited for; matrix products, arithmetic and copies ran while one was open for 1% of the time, Pallas kernels for 18%

profile of v2, /device:TPU:1, one launch (start us, length us, event | category | flops | bytes accessed | tf_op | source)
XLA Modules:
  0.0 196.1 jit_solution(18421020077213826514)
XLA Ops:
  6.5 0.8 reshape.80
  7.3 0.7 convert_convert_fusion
  8.2 1.0 multiply_bitcast_fusion
  9.2 0.1 copy.37
  9.4 0.2 reshape.82
  9.9 0.2 reshape.78
  10.5 0.2 reshape.76
  10.7 0.2 pad_maximum_fusion
  11.0 0.2 copy.45
  11.2 4.7 %collective-permute-start.6 = (bf16[800,128]{1,0:T(8,128)(2,1)S(1)}, bf16[800,128]{1,0:T(8,128)(2,1)S(1)}, u32[]{:S(2)}, u32[]{:S(2)}) collective-permute-start(bf16[800,128]{1,0:T(8,128)(2,1)S(1)} %bitcast.56), channel_id=1, source_target_pairs={{0,33},{1,97},{32,1},{33,65},{64,32},{65,96},{96,0},{97,64},{2,35}... | collective-permute-start | bytes 614408 | tf_op jit(solution)/shard_map/ppermute | solution.py:438
  15.9 0.2 copy.44
  16.0 1.8 collective-permute-start.5
  17.9 0.2 copy.43
  18.1 0.2 copy.42
  18.3 3.5 %collective-permute-start.3 = (bf16[800,128]{1,0:T(8,128)(2,1)S(1)}, bf16[800,128]{1,0:T(8,128)(2,1)S(1)}, u32[]{:S(2)}, u32[]{:S(2)}) collective-permute-start(bf16[800,128]{1,0:T(8,128)(2,1)S(1)} %bitcast.59), channel_id=1, source_target_pairs={{0,0},{1,64},{32,32},{33,96},{64,1},{65,65},{96,33},{97,97},{2,2},... | collective-permute-start | bytes 614408 | tf_op jit(solution)/shard_map/ppermute | solution.py:438
  21.8 0.7 fusion.4.tab.sc
  22.6 2.6 %collective-permute-done.4 = bf16[800,128]{1,0:T(8,128)(2,1)S(1)} collective-permute-done((bf16[800,128]{1,0:T(8,128)(2,1)S(1)}, bf16[800,128]{1,0:T(8,128)(2,1)S(1)}, u32[]{:S(2)}, u32[]{:S(2)}) %collective-permute-start.4) | collective-permute-done | bytes 204832 | tf_op jit(solution)/shard_map/ppermute | solution.py:438
  25.2 2.2 %collective-permute-done.3 = bf16[800,128]{1,0:T(8,128)(2,1)S(1)} collective-permute-done((bf16[800,128]{1,0:T(8,128)(2,1)S(1)}, bf16[800,128]{1,0:T(8,128)(2,1)S(1)}, u32[]{:S(2)}, u32[]{:S(2)}) %collective-permute-start.3) | collective-permute-done | bytes 204832 | tf_op jit(solution)/shard_map/ppermute | solution.py:438
  27.4 2.8 %collective-permute-start.7 = (bf16[4,544,128]{2,1,0:T(8,128)(2,1)S(1)}, bf16[4,544,128]{2,1,0:T(8,128)(2,1)}, u32[]{:S(2)}, u32[]{:S(2)}) collective-permute-start(bf16[4,544,128]{2,1,0:T(8,128)(2,1)S(1)} %pad_maximum_fusion.1.rest_0_), channel_id=1, source_target_pairs={{0,24},{8,0},{16,8},{24,16},{1,25},{9,1},{17,9},{25,17},{2,26},{10... | collective-permute-start | bytes 1671176 | tf_op jit(solution)/shard_map/ppermute | solution.py:379
  30.2 1.6 collective-permute-start.9
  31.9 0.1 copy.46
  32.4 0.8 pad_maximum_fusion.2
  33.2 0.9 collective-permute-done.10.rest_1_
  34.1 0.8 copy-done.14
  34.9 9.0 %attend_first.1 = (f32[4,1,512]{2,1,0:T(1,128)S(1)}, f32[4,1,512]{2,1,0:T(1,128)S(1)}, f32[4,64,512]{2,1,0:T(8,128)S(1)}) custom-call(s32[40]{0:T(128)S(1)} %fusion.4.tab.sc, s32[4]{0:T(128)S(1)} %subtract_convert_fusion.zeros_q, bf16[4,256,128]{2,1,0:T(8,128)(2,1)S(1)} %pad_maximum_fusion.3.qt_ref, bf16[4,544,128]{2,1,0:T(8,128)(2,1)} %copy-done.2, ...), custom_call_target="tpu_custom_call" | custom-call | flops 8000000000 | bytes 2000000 | tf_op jit(solution)/shard_map/attend_first/pallas_call | solution.py:230
  43.9 7.7 %collective-permute-done.7.rest_0_ = bf16[4,544,128]{2,1,0:T(8,128)(2,1)} collective-permute-done((bf16[4,544,128]{2,1,0:T(8,128)(2,1)S(1)}, bf16[4,544,128]{2,1,0:T(8,128)(2,1)}, u32[]{:S(2)}, u32[]{:S(2)}) %collective-permute-start.7) | collective-permute-done | bytes 557088 | tf_op jit(solution)/shard_map/ppermute | solution.py:379
  51.7 3.5 %collective-permute-done.8.rest_2_ = bf16[4,544,128]{2,1,0:T(8,128)(2,1)} collective-permute-done((bf16[4,544,128]{2,1,0:T(8,128)(2,1)S(1)}, bf16[4,544,128]{2,1,0:T(8,128)(2,1)}, u32[]{:S(2)}, u32[]{:S(2)}) %collective-permute-start.8) | collective-permute-done | bytes 557088 | tf_op jit(solution)/shard_map/ppermute | solution.py:379
  55.3 0.5 collective-permute-start.12
  55.9 2.5 %collective-permute-start = (bf16[136,2048]{1,0:T(8,128)(2,1)S(1)}, bf16[136,2048]{1,0:T(8,128)(2,1)S(1)}, u32[]{:S(2)}, u32[]{:S(2)}) collective-permute-start(bf16[136,2048]{1,0:T(8,128)(2,1)S(1)} %fusion.1.rest_0_), channel_id=1, source_target_pairs={{0,6},{2,0},{4,2},{6,4},{1,7},{3,1},{5,3},{7,5},{8,14},{10,8},{12,... | collective-permute-start | bytes 1671176 | tf_op jit(solution)/shard_map/ppermute | solution.py:379
  58.5 5.2 %all-to-all-start = ((bf16[8,128,256]{2,1,0:T(8,128)(2,1)}), bf16[8,128,256]{2,1,0:T(8,128)(2,1)S(1)}, u32[]{:S(2)}, u32[]{:S(2)}) async-start(bf16[8,128,256]{2,1,0:T(8,128)(2,1)} %bitcast.23), calls=%async_computation | async-start | bytes 1048576 | tf_op jit(solution)/shard_map/all_to_all | solution.py:456
  63.7 2.9 %collective-permute-start.2 = (bf16[136,2048]{1,0:T(8,128)(2,1)S(1)}, bf16[136,2048]{1,0:T(8,128)(2,1)}, u32[]{:S(2)}, u32[]{:S(2)}) collective-permute-start(bf16[136,2048]{1,0:T(8,128)(2,1)S(1)} %fusion.1.rest_0_), channel_id=1, source_target_pairs={{0,4},{2,6},{4,0},{6,2},{1,5},{3,7},{5,1},{7,3},{8,12},{10,14},{12... | collective-permute-start | bytes 1671176 | tf_op jit(solution)/shard_map/ppermute | solution.py:379
  66.6 14.4 %attend_last.1 = bf16[16,64,128]{2,1,0:T(8,128)(2,1)S(1)} custom-call(s32[40]{0:T(128)S(1)} %fusion.4.tab.sc, s32[4]{0:T(128)S(1)} %subtract_convert_fusion.zeros_q, bf16[4,256,128]{2,1,0:T(8,128)(2,1)S(1)} %pad_maximum_fusion.3.qt_ref, bf16[4,544,128]{2,1,0:T(8,128)(2,1)} %collective-permute-done.7.rest_0_, ...), custom_call_target="tpu_custom_call" | custom-call | flops 24000000000 | bytes 6000000 | tf_op jit(solution)/shard_map/attend_last/pallas_call | solution.py:230
  81.0 8.9 %collective-permute-done.2.rest_6_ = bf16[136,2048]{1,0:T(8,128)(2,1)} collective-permute-done((bf16[136,2048]{1,0:T(8,128)(2,1)S(1)}, bf16[136,2048]{1,0:T(8,128)(2,1)}, u32[]{:S(2)}, u32[]{:S(2)}) %collective-permute-start.2) | collective-permute-done | bytes 557088 | tf_op jit(solution)/shard_map/ppermute | solution.py:379
  89.9 2.1 %all-to-all-done.res_ref = bf16[8,128,256]{2,1,0:T(8,128)(2,1)S(1)} async-done(((bf16[8,128,256]{2,1,0:T(8,128)(2,1)}), bf16[8,128,256]{2,1,0:T(8,128)(2,1)S(1)}, u32[]{:S(2)}, u32[]{:S(2)}) %all-to-all-start) | async-done | bytes 524320 | tf_op jit(solution)/shard_map/all_to_all | solution.py:456
  92.0 0.5 collective-permute-start.15
  92.5 0.5 collective-permute-start.17
  93.0 11.0 %all_to_all.10.att_ref = bf16[16,64,128]{2,1,0:T(8,128)(2,1)S(1)} all-to-all(bf16[16,64,128]{2,1,0:T(8,128)(2,1)S(1)} %attend_last.1), channel_id=1, replica_groups=mesh['z'=4,'y'=4,'x'=4,'c'=2] {'x','z'}, dimensions={0} | all-to-all | bytes 524288 | tf_op jit(solution)/shard_map/all_to_all | solution.py:466
  104.1 0.8 copy-done.5
  104.9 0.1 copy-done.6
  105.0 0.3 copy-done.7
  105.3 0.8 copy-done.8
  106.1 3.8 %dense.1 = (bf16[128,2048]{1,0:T(8,128)(2,1)S(1)}, bf16[8,2048]{1,0:T(8,128)(2,1)S(1)}) custom-call(s32[40]{0:T(128)S(1)} %fusion.4.tab.sc, bf16[16,64,128]{2,1,0:T(8,128)(2,1)S(1)} %all_to_all.10.att_ref, bf16[8,128,256]{2,1,0:T(8,128)(2,1)S(1)} %all-to-all-done.res_ref, bf16[136,2048]{1,0:T(8,128)(2,1)} %copy-done.1, bf16[136,2048]{1,0:T(8,128)(2,1)} %copy-done.5, ...), custom_call_target="tpu_custom_call" | custom-call | flops 1000000000 | bytes 4000000 | tf_op jit(solution)/shard_map/dense/pallas_call | solution.py:273
  109.9 1.5 collective-permute-start.19
  111.5 1.3 collective-permute-start.23
  112.7 2.4 %collective-permute-start.18 = (bf16[128,2048]{1,0:T(8,128)(2,1)S(1)}, bf16[128,2048]{1,0:T(8,128)(2,1)S(1)}, u32[]{:S(2)}, u32[]{:S(2)}) collective-permute-start(bf16[128,2048]{1,0:T(8,128)(2,1)S(1)} %get-tuple-element.58.rest_0_), channel_id=1, source_target_pairs={{0,1},{1,0},{2,3},{3,2},{4,5},{5,4},{6,7},{7,6},{8,9},{9,8},{10,11... | collective-permute-start | bytes 1572872 | tf_op jit(solution)/shard_map/ppermute | solution.py:383
  115.2 6.9 %collective-permute-done.19.rest_2_ = bf16[128,2048]{1,0:T(8,128)(2,1)S(1)} collective-permute-done((bf16[128,2048]{1,0:T(8,128)(2,1)S(1)}, bf16[128,2048]{1,0:T(8,128)(2,1)S(1)}, u32[]{:S(2)}, u32[]{:S(2)}) %collective-permute-start.19) | collective-permute-done | bytes 524320 | tf_op jit(solution)/shard_map/ppermute | solution.py:379
  122.1 4.5 %collective-permute-start.20 = (bf16[128,2048]{1,0:T(8,128)(2,1)S(1)}, bf16[128,2048]{1,0:T(8,128)(2,1)S(1)}, u32[]{:S(2)}, u32[]{:S(2)}) collective-permute-start(bf16[128,2048]{1,0:T(8,128)(2,1)S(1)} %collective-permute-done.19.rest_2_), channel_id=1, source_target_pairs={{0,1},{1,0},{2,3},{3,2},{4,5},{5,4},{6,7},{7,6},{8,9},{9,8},{10,11... | collective-permute-start | bytes 1572872 | tf_op jit(solution)/shard_map/ppermute | solution.py:383
  126.5 0.1 collective-permute-done.21.rest_4_
  126.7 11.6 %collective-permute-start.22 = (bf16[128,2048]{1,0:T(8,128)(2,1)S(1)}, bf16[128,2048]{1,0:T(8,128)(2,1)S(1)}, u32[]{:S(2)}, u32[]{:S(2)}) collective-permute-start(bf16[128,2048]{1,0:T(8,128)(2,1)S(1)} %collective-permute-done.21.rest_4_), channel_id=1, source_target_pairs={{0,1},{1,0},{2,3},{3,2},{4,5},{5,4},{6,7},{7,6},{8,9},{9,8},{10,11... | collective-permute-start | bytes 1572872 | tf_op jit(solution)/shard_map/ppermute | solution.py:383
  138.4 1.4 collective-permute-done.22.rest_5_
  139.8 0.8 copy-done.20
  140.7 8.6 %up.1 = (bf16[1024,1024]{1,0:T(8,128)(2,1)S(1)}, bf16[1024,256]{1,0:T(8,128)(2,1)S(1)}) custom-call(s32[40]{0:T(128)S(1)} %fusion.4.tab.sc, bf16[8,2048]{1,0:T(8,128)(2,1)S(1)} %get-tuple-element.56.gain_ref, bf16[4096,1024]{1,0:T(8,128)(2,1)} %all-gather.2.cloned.1.call-done.w_in, bf16[128,2048]{1,0:T(8,128)(2,1)} %copy-done, bf16[128,2048]{1,0:T(8,128)(2,1)} %copy-done.18, ...), custom_call_target="tpu_custom_call" | custom-call | flops 4300000256 | bytes 8000000 | tf_op jit(solution)/shard_map/up/pallas_call | solution.py:315
  149.3 3.1 %down.4 = (bf16[1024,256]{1,0:T(8,128)(2,1)S(1)}, bf16[1024,256]{1,0:T(8,128)(2,1)S(1)}) custom-call(s32[40]{0:T(128)S(1)} %fusion.4.tab.sc, bf16[1024,1024]{1,0:T(8,128)(2,1)S(1)} %get-tuple-element.60.h_ref, bf16[4096,1024]{1,0:T(8,128)(2,1)} %all-gather.2.cloned.1.call-done.w_in), custom_call_target="tpu_custom_call" | custom-call | flops 1100000000 | bytes 4000000 | tf_op jit(solution)/shard_map/down/pallas_call | solution.py:363
  152.4 0.7 collective-permute-start.26
  153.1 4.4 %down.5 = (bf16[1024,256]{1,0:T(8,128)(2,1)S(1)}, bf16[1024,256]{1,0:T(8,128)(2,1)S(1)}, bf16[1024,256]{1,0:T(8,128)(2,1)S(1)}, bf16[1024,256]{1,0:T(8,128)(2,1)S(1)}) custom-call(s32[40]{0:T(128)S(1)} %fusion.4.tab.sc, bf16[1024,1024]{1,0:T(8,128)(2,1)S(1)} %get-tuple-element.60.h_ref, bf16[4096,1024]{1,0:T(8,128)(2,1)} %all-gather.2.cloned.1.call-done.w_in), custom_call_target="tpu_custom_call" | custom-call | flops 2200000000 | bytes 4000000 | tf_op jit(solution)/shard_map/down/pallas_call | solution.py:363
  157.5 0.2 collective-permute-start.28
  157.7 3.1 %down.3 = (bf16[1024,256]{1,0:T(8,128)(2,1)S(1)}, bf16[1024,256]{1,0:T(8,128)(2,1)S(1)}) custom-call(s32[40]{0:T(128)S(1)} %fusion.4.tab.sc, bf16[1024,1024]{1,0:T(8,128)(2,1)S(1)} %get-tuple-element.60.h_ref, bf16[4096,1024]{1,0:T(8,128)(2,1)} %all-gather.2.cloned.1.call-done.w_in), custom_call_target="tpu_custom_call" | custom-call | flops 1100000000 | bytes 4000000 | tf_op jit(solution)/shard_map/down/pallas_call | solution.py:363
  160.7 0.5 collective-permute-start.25
  161.7 1.4 collective-permute-start.29
  163.1 0.4 collective-permute-done.30
  163.6 1.0 collective-permute-start.31
  164.7 11.5 %collective-permute-done.27 = bf16[1024,256]{1,0:T(8,128)(2,1)S(1)} collective-permute-done((bf16[1024,256]{1,0:T(8,128)(2,1)S(1)}, bf16[1024,256]{1,0:T(8,128)(2,1)S(1)}, u32[]{:S(2)}, u32[]{:S(2)}) %collective-permute-start.27) | collective-permute-done | bytes 524320 | tf_op jit(solution)/shard_map/ppermute | solution.py:379
  176.2 11.8 %collective-permute-done.29 = bf16[1024,256]{1,0:T(8,128)(2,1)S(1)} collective-permute-done((bf16[1024,256]{1,0:T(8,128)(2,1)S(1)}, bf16[1024,256]{1,0:T(8,128)(2,1)S(1)}, u32[]{:S(2)}, u32[]{:S(2)}) %collective-permute-start.29) | collective-permute-done | bytes 524320 | tf_op jit(solution)/shard_map/ppermute | solution.py:379
  188.0 1.2 add_convert_fusion
  (104 shorter events, 2.7 us)
Async XLA Ops:
  6.5 3.2 %copy-start.10 = (bf16[1024,128]{1,0:T(8,128)(2,1)S(1)}, bf16[1024,128]{1,0:T(8,128)(2,1)}, u32[]{:S(2)}) copy-start(bf16[1024,128]{1,0:T(8,128)(2,1)} %param.13) | copy-start | bytes 786436
  6.5 134.1 %all-gather.2.cloned.1.call-start = ((), (), s32[]{:S(2)}) async-start(), calls=%async_computation.2 | async-start | bytes 8912896 | tf_op jit(solution)/shard_map/all_gather | solution.py:458
  9.4 1.0 copy-start.11
  11.2 20.7 %copy-start.12 = (bf16[1024,128]{1,0:T(8,128)(2,1)S(1)}, bf16[1024,128]{1,0:T(8,128)(2,1)}, u32[]{:S(2)}) copy-start(bf16[1024,128]{1,0:T(8,128)(2,1)} %param.20) | copy-start | bytes 786436
  11.2 11.3 %collective-permute-start.6 = (bf16[800,128]{1,0:T(8,128)(2,1)S(1)}, bf16[800,128]{1,0:T(8,128)(2,1)S(1)}, u32[]{:S(2)}, u32[]{:S(2)}) collective-permute-start(bf16[800,128]{1,0:T(8,128)(2,1)S(1)} %bitcast.56), channel_id=1, source_target_pairs={{0,33},{1,97},{32,1},{33,65},{64,32},{65,96},{96,0},{97,64},{2,35}... | collective-permute-start | bytes 614408 | tf_op jit(solution)/shard_map/ppermute | solution.py:438
  16.0 6.5 %collective-permute-start.5 = (bf16[800,128]{1,0:T(8,128)(2,1)S(1)}, bf16[800,128]{1,0:T(8,128)(2,1)S(1)}, u32[]{:S(2)}, u32[]{:S(2)}) collective-permute-start(bf16[800,128]{1,0:T(8,128)(2,1)S(1)} %bitcast.57), channel_id=1, source_target_pairs={{0,1},{1,65},{32,33},{33,97},{64,0},{65,64},{96,32},{97,96},{2,3},... | collective-permute-start | bytes 614408 | tf_op jit(solution)/shard_map/ppermute | solution.py:438
  18.0 7.1 %collective-permute-start.4 = (bf16[800,128]{1,0:T(8,128)(2,1)S(1)}, bf16[800,128]{1,0:T(8,128)(2,1)S(1)}, u32[]{:S(2)}, u32[]{:S(2)}) collective-permute-start(bf16[800,128]{1,0:T(8,128)(2,1)S(1)} %bitcast.58), channel_id=1, source_target_pairs={{0,32},{1,96},{32,0},{33,64},{64,33},{65,97},{96,1},{97,65},{2,34}... | collective-permute-start | bytes 614408 | tf_op jit(solution)/shard_map/ppermute | solution.py:438
  18.3 9.0 %collective-permute-start.3 = (bf16[800,128]{1,0:T(8,128)(2,1)S(1)}, bf16[800,128]{1,0:T(8,128)(2,1)S(1)}, u32[]{:S(2)}, u32[]{:S(2)}) collective-permute-start(bf16[800,128]{1,0:T(8,128)(2,1)S(1)} %bitcast.59), channel_id=1, source_target_pairs={{0,0},{1,64},{32,32},{33,96},{64,1},{65,65},{96,33},{97,97},{2,2},... | collective-permute-start | bytes 614408 | tf_op jit(solution)/shard_map/ppermute | solution.py:438
  22.5 9.8 %copy-start.13 = (bf16[128,1024]{1,0:T(8,128)(2,1)S(1)}, bf16[128,1024]{1,0:T(8,128)(2,1)}, u32[]{:S(2)}) copy-start(bf16[128,1024]{1,0:T(8,128)(2,1)} %param.19) | copy-start | bytes 786436
  27.4 6.7 %copy-start.2 = (bf16[4,544,128]{2,1,0:T(8,128)(2,1)}, bf16[4,544,128]{2,1,0:T(8,128)(2,1)S(1)}, u32[]{:S(2)}) copy-start(bf16[4,544,128]{2,1,0:T(8,128)(2,1)S(1)} %pad_maximum_fusion.1.rest_0_) | copy-start | bytes 1671172
  27.4 24.2 %collective-permute-start.7 = (bf16[4,544,128]{2,1,0:T(8,128)(2,1)S(1)}, bf16[4,544,128]{2,1,0:T(8,128)(2,1)}, u32[]{:S(2)}, u32[]{:S(2)}) collective-permute-start(bf16[4,544,128]{2,1,0:T(8,128)(2,1)S(1)} %pad_maximum_fusion.1.rest_0_), channel_id=1, source_target_pairs={{0,24},{8,0},{16,8},{24,16},{1,25},{9,1},{17,9},{25,17},{2,26},{10... | collective-permute-start | bytes 1671176 | tf_op jit(solution)/shard_map/ppermute | solution.py:379
  30.2 24.9 %collective-permute-start.8 = (bf16[4,544,128]{2,1,0:T(8,128)(2,1)S(1)}, bf16[4,544,128]{2,1,0:T(8,128)(2,1)}, u32[]{:S(2)}, u32[]{:S(2)}) collective-permute-start(bf16[4,544,128]{2,1,0:T(8,128)(2,1)S(1)} %pad_maximum_fusion.1.rest_0_), channel_id=1, source_target_pairs={{0,8},{8,16},{16,24},{24,0},{1,9},{9,17},{17,25},{25,1},{2,10},{10... | collective-permute-start | bytes 1671176 | tf_op jit(solution)/shard_map/ppermute | solution.py:379
  30.2 24.9 %collective-permute-start.9 = (bf16[4,544,128]{2,1,0:T(8,128)(2,1)S(1)}, bf16[4,544,128]{2,1,0:T(8,128)(2,1)}, u32[]{:S(2)}, u32[]{:S(2)}) collective-permute-start(bf16[4,544,128]{2,1,0:T(8,128)(2,1)S(1)} %pad_maximum_fusion.1.rest_0_), channel_id=1, source_target_pairs={{0,16},{8,24},{16,0},{24,8},{1,17},{9,25},{17,1},{25,9},{2,18},{10... | collective-permute-start | bytes 1671176 | tf_op jit(solution)/shard_map/ppermute | solution.py:379
  32.0 2.0 %collective-permute-start.10 = (bf16[4,544,128]{2,1,0:T(8,128)(2,1)S(1)}, bf16[4,544,128]{2,1,0:T(8,128)(2,1)S(1)}, u32[]{:S(2)}, u32[]{:S(2)}) collective-permute-start(bf16[4,544,128]{2,1,0:T(8,128)(2,1)S(1)} %pad_maximum_fusion.1.rest_0_), channel_id=1, source_target_pairs={{0,1},{1,0},{2,3},{3,2},{4,5},{5,4},{6,7},{7,6},{8,9},{9,8},{10,11... | collective-permute-start | bytes 1671176 | tf_op jit(solution)/shard_map/ppermute | solution.py:383
  33.2 22.7 %copy-start.21 = (bf16[256]{0:T(256)(128)(2,1)S(1)}, bf16[256]{0:T(256)(128)(2,1)}, u32[]{:S(2)}) copy-start(bf16[256]{0:T(256)(128)(2,1)} %param.18) | copy-start | bytes 1540
  33.2 22.7 %copy-start.9 = (bf16[128,2048]{1,0:T(8,128)(2,1)S(1)}, bf16[128,2048]{1,0:T(8,128)(2,1)}, u32[]{:S(2)}) copy-start(bf16[128,2048]{1,0:T(8,128)(2,1)} %param.17) | copy-start | bytes 1572868
  34.1 0.8 copy-start.14
  55.2 8.5 %collective-permute-start.11 = (bf16[4,544,128]{2,1,0:T(8,128)(2,1)}, bf16[4,544,128]{2,1,0:T(8,128)(2,1)}, u32[]{:S(2)}, u32[]{:S(2)}) collective-permute-start(bf16[4,544,128]{2,1,0:T(8,128)(2,1)} %collective-permute-done.7.rest_0_), channel_id=1, source_target_pairs={{0,1},{1,0},{2,3},{3,2},{4,5},{5,4},{6,7},{7,6},{8,9},{9,8},{10,11... | collective-permute-start | bytes 1671176 | tf_op jit(solution)/shard_map/ppermute | solution.py:383
  55.3 11.3 %collective-permute-start.12 = (bf16[4,544,128]{2,1,0:T(8,128)(2,1)}, bf16[4,544,128]{2,1,0:T(8,128)(2,1)}, u32[]{:S(2)}, u32[]{:S(2)}) collective-permute-start(bf16[4,544,128]{2,1,0:T(8,128)(2,1)} %collective-permute-done.8.rest_2_), channel_id=1, source_target_pairs={{0,1},{1,0},{2,3},{3,2},{4,5},{5,4},{6,7},{7,6},{8,9},{9,8},{10,11... | collective-permute-start | bytes 1671176 | tf_op jit(solution)/shard_map/ppermute | solution.py:383
  55.8 10.8 %collective-permute-start.13 = (bf16[4,544,128]{2,1,0:T(8,128)(2,1)}, bf16[4,544,128]{2,1,0:T(8,128)(2,1)}, u32[]{:S(2)}, u32[]{:S(2)}) collective-permute-start(bf16[4,544,128]{2,1,0:T(8,128)(2,1)} %collective-permute-done.9.rest_4_), channel_id=1, source_target_pairs={{0,1},{1,0},{2,3},{3,2},{4,5},{5,4},{6,7},{7,6},{8,9},{9,8},{10,11... | collective-permute-start | bytes 1671176 | tf_op jit(solution)/shard_map/ppermute | solution.py:383
  55.9 36.1 %copy-start.1 = (bf16[136,2048]{1,0:T(8,128)(2,1)}, bf16[136,2048]{1,0:T(8,128)(2,1)S(1)}, u32[]{:S(2)}) copy-start(bf16[136,2048]{1,0:T(8,128)(2,1)S(1)} %fusion.1.rest_0_) | copy-start | bytes 1671172
  55.9 25.1 %collective-permute-start = (bf16[136,2048]{1,0:T(8,128)(2,1)S(1)}, bf16[136,2048]{1,0:T(8,128)(2,1)S(1)}, u32[]{:S(2)}, u32[]{:S(2)}) collective-permute-start(bf16[136,2048]{1,0:T(8,128)(2,1)S(1)} %fusion.1.rest_0_), channel_id=1, source_target_pairs={{0,6},{2,0},{4,2},{6,4},{1,7},{3,1},{5,3},{7,5},{8,14},{10,8},{12,... | collective-permute-start | bytes 1671176 | tf_op jit(solution)/shard_map/ppermute | solution.py:379
  58.5 22.5 %collective-permute-start.1 = (bf16[136,2048]{1,0:T(8,128)(2,1)S(1)}, bf16[136,2048]{1,0:T(8,128)(2,1)S(1)}, u32[]{:S(2)}, u32[]{:S(2)}) collective-permute-start(bf16[136,2048]{1,0:T(8,128)(2,1)S(1)} %fusion.1.rest_0_), channel_id=1, source_target_pairs={{0,2},{2,4},{4,6},{6,0},{1,3},{3,5},{5,7},{7,1},{8,10},{10,12},{12... | collective-permute-start | bytes 1671176 | tf_op jit(solution)/shard_map/ppermute | solution.py:379
  58.5 33.5 %all-to-all-start = ((bf16[8,128,256]{2,1,0:T(8,128)(2,1)}), bf16[8,128,256]{2,1,0:T(8,128)(2,1)S(1)}, u32[]{:S(2)}, u32[]{:S(2)}) async-start(bf16[8,128,256]{2,1,0:T(8,128)(2,1)} %bitcast.23), calls=%async_computation | async-start | bytes 1048576 | tf_op jit(solution)/shard_map/all_to_all | solution.py:456
  63.7 26.2 %collective-permute-start.2 = (bf16[136,2048]{1,0:T(8,128)(2,1)S(1)}, bf16[136,2048]{1,0:T(8,128)(2,1)}, u32[]{:S(2)}, u32[]{:S(2)}) collective-permute-start(bf16[136,2048]{1,0:T(8,128)(2,1)S(1)} %fusion.1.rest_0_), channel_id=1, source_target_pairs={{0,4},{2,6},{4,0},{6,2},{1,5},{3,7},{5,1},{7,3},{8,12},{10,14},{12... | collective-permute-start | bytes 1671176 | tf_op jit(solution)/shard_map/ppermute | solution.py:379
  81.0 23.1 %copy-start.3 = (bf16[136,2048]{1,0:T(8,128)(2,1)}, bf16[136,2048]{1,0:T(8,128)(2,1)S(1)}, u32[]{:S(2)}) copy-start(bf16[136,2048]{1,0:T(8,128)(2,1)S(1)} %collective-permute-done.rest_2_) | copy-start | bytes 1671172
  81.0 23.1 %copy-start.4 = (bf16[136,2048]{1,0:T(8,128)(2,1)}, bf16[136,2048]{1,0:T(8,128)(2,1)S(1)}, u32[]{:S(2)}) copy-start(bf16[136,2048]{1,0:T(8,128)(2,1)S(1)} %collective-permute-done.1.rest_4_) | copy-start | bytes 1671172
  92.0 12.0 %collective-permute-start.14 = (bf16[136,2048]{1,0:T(8,128)(2,1)S(1)}, bf16[136,2048]{1,0:T(8,128)(2,1)S(1)}, u32[]{:S(2)}, u32[]{:S(2)}) collective-permute-start(bf16[136,2048]{1,0:T(8,128)(2,1)S(1)} %fusion.1.rest_0_), channel_id=1, source_target_pairs={{0,1},{1,0},{2,3},{3,2},{4,5},{5,4},{6,7},{7,6},{8,9},{9,8},{10,11... | collective-permute-start | bytes 1671176 | tf_op jit(solution)/shard_map/ppermute | solution.py:383
  92.0 12.0 %collective-permute-start.15 = (bf16[136,2048]{1,0:T(8,128)(2,1)S(1)}, bf16[136,2048]{1,0:T(8,128)(2,1)S(1)}, u32[]{:S(2)}, u32[]{:S(2)}) collective-permute-start(bf16[136,2048]{1,0:T(8,128)(2,1)S(1)} %collective-permute-done.rest_2_), channel_id=1, source_target_pairs={{0,1},{1,0},{2,3},{3,2},{4,5},{5,4},{6,7},{7,6},{8,9},{9,8},{10,11... | collective-permute-start | bytes 1671176 | tf_op jit(solution)/shard_map/ppermute | solution.py:383
  92.5 11.6 %collective-permute-start.16 = (bf16[136,2048]{1,0:T(8,128)(2,1)S(1)}, bf16[136,2048]{1,0:T(8,128)(2,1)S(1)}, u32[]{:S(2)}, u32[]{:S(2)}) collective-permute-start(bf16[136,2048]{1,0:T(8,128)(2,1)S(1)} %collective-permute-done.1.rest_4_), channel_id=1, source_target_pairs={{0,1},{1,0},{2,3},{3,2},{4,5},{5,4},{6,7},{7,6},{8,9},{9,8},{10,11... | collective-permute-start | bytes 1671176 | tf_op jit(solution)/shard_map/ppermute | solution.py:383
  92.5 11.6 %collective-permute-start.17 = (bf16[136,2048]{1,0:T(8,128)(2,1)}, bf16[136,2048]{1,0:T(8,128)(2,1)S(1)}, u32[]{:S(2)}, u32[]{:S(2)}) collective-permute-start(bf16[136,2048]{1,0:T(8,128)(2,1)} %collective-permute-done.2.rest_6_), channel_id=1, source_target_pairs={{0,1},{1,0},{2,3},{3,2},{4,5},{5,4},{6,7},{7,6},{8,9},{9,8},{10,11... | collective-permute-start | bytes 1671176 | tf_op jit(solution)/shard_map/ppermute | solution.py:383
  104.1 0.8 copy-start.5
  104.1 1.0 copy-start.6
  104.1 1.2 copy-start.7
  105.3 0.8 copy-start.8
  109.9 30.8 %copy-start = (bf16[128,2048]{1,0:T(8,128)(2,1)}, bf16[128,2048]{1,0:T(8,128)(2,1)S(1)}, u32[]{:S(2)}) copy-start(bf16[128,2048]{1,0:T(8,128)(2,1)S(1)} %get-tuple-element.58.rest_0_) | copy-start | bytes 1572868
  109.9 12.1 %collective-permute-start.19 = (bf16[128,2048]{1,0:T(8,128)(2,1)S(1)}, bf16[128,2048]{1,0:T(8,128)(2,1)S(1)}, u32[]{:S(2)}, u32[]{:S(2)}) collective-permute-start(bf16[128,2048]{1,0:T(8,128)(2,1)S(1)} %get-tuple-element.58.rest_0_), channel_id=1, source_target_pairs={{0,6},{2,0},{4,2},{6,4},{1,7},{3,1},{5,3},{7,5},{8,14},{10,8},{12,... | collective-permute-start | bytes 1572872 | tf_op jit(solution)/shard_map/ppermute | solution.py:379
  111.5 15.2 %collective-permute-start.21 = (bf16[128,2048]{1,0:T(8,128)(2,1)S(1)}, bf16[128,2048]{1,0:T(8,128)(2,1)S(1)}, u32[]{:S(2)}, u32[]{:S(2)}) collective-permute-start(bf16[128,2048]{1,0:T(8,128)(2,1)S(1)} %get-tuple-element.58.rest_0_), channel_id=1, source_target_pairs={{0,2},{2,4},{4,6},{6,0},{1,3},{3,5},{5,7},{7,1},{8,10},{10,12},{12... | collective-permute-start | bytes 1572872 | tf_op jit(solution)/shard_map/ppermute | solution.py:379
  111.5 26.8 %collective-permute-start.23 = (bf16[128,2048]{1,0:T(8,128)(2,1)S(1)}, bf16[128,2048]{1,0:T(8,128)(2,1)S(1)}, u32[]{:S(2)}, u32[]{:S(2)}) collective-permute-start(bf16[128,2048]{1,0:T(8,128)(2,1)S(1)} %get-tuple-element.58.rest_0_), channel_id=1, source_target_pairs={{0,4},{2,6},{4,0},{6,2},{1,5},{3,7},{5,1},{7,3},{8,12},{10,14},{12... | collective-permute-start | bytes 1572872 | tf_op jit(solution)/shard_map/ppermute | solution.py:379
  112.7 25.6 %collective-permute-start.18 = (bf16[128,2048]{1,0:T(8,128)(2,1)S(1)}, bf16[128,2048]{1,0:T(8,128)(2,1)S(1)}, u32[]{:S(2)}, u32[]{:S(2)}) collective-permute-start(bf16[128,2048]{1,0:T(8,128)(2,1)S(1)} %get-tuple-element.58.rest_0_), channel_id=1, source_target_pairs={{0,1},{1,0},{2,3},{3,2},{4,5},{5,4},{6,7},{7,6},{8,9},{9,8},{10,11... | collective-permute-start | bytes 1572872 | tf_op jit(solution)/shard_map/ppermute | solution.py:383
  122.1 18.6 %copy-start.15 = (bf16[128,2048]{1,0:T(8,128)(2,1)}, bf16[128,2048]{1,0:T(8,128)(2,1)S(1)}, u32[]{:S(2)}) copy-start(bf16[128,2048]{1,0:T(8,128)(2,1)S(1)} %collective-permute-done.19.rest_2_) | copy-start | bytes 1572868
  122.1 16.3 %collective-permute-start.20 = (bf16[128,2048]{1,0:T(8,128)(2,1)S(1)}, bf16[128,2048]{1,0:T(8,128)(2,1)S(1)}, u32[]{:S(2)}, u32[]{:S(2)}) collective-permute-start(bf16[128,2048]{1,0:T(8,128)(2,1)S(1)} %collective-permute-done.19.rest_2_), channel_id=1, source_target_pairs={{0,1},{1,0},{2,3},{3,2},{4,5},{5,4},{6,7},{7,6},{8,9},{9,8},{10,11... | collective-permute-start | bytes 1572872 | tf_op jit(solution)/shard_map/ppermute | solution.py:383
  126.7 14.0 %copy-start.16 = (bf16[128,2048]{1,0:T(8,128)(2,1)}, bf16[128,2048]{1,0:T(8,128)(2,1)S(1)}, u32[]{:S(2)}) copy-start(bf16[128,2048]{1,0:T(8,128)(2,1)S(1)} %collective-permute-done.21.rest_4_) | copy-start | bytes 1572868
  126.7 13.1 %collective-permute-start.22 = (bf16[128,2048]{1,0:T(8,128)(2,1)S(1)}, bf16[128,2048]{1,0:T(8,128)(2,1)S(1)}, u32[]{:S(2)}, u32[]{:S(2)}) collective-permute-start(bf16[128,2048]{1,0:T(8,128)(2,1)S(1)} %collective-permute-done.21.rest_4_), channel_id=1, source_target_pairs={{0,1},{1,0},{2,3},{3,2},{4,5},{5,4},{6,7},{7,6},{8,9},{9,8},{10,11... | collective-permute-start | bytes 1572872 | tf_op jit(solution)/shard_map/ppermute | solution.py:383
  138.3 2.4 %copy-start.17 = (bf16[128,2048]{1,0:T(8,128)(2,1)}, bf16[128,2048]{1,0:T(8,128)(2,1)S(1)}, u32[]{:S(2)}) copy-start(bf16[128,2048]{1,0:T(8,128)(2,1)S(1)} %collective-permute-done.23.rest_6_) | copy-start | bytes 1572868
  138.3 2.4 %collective-permute-start.24 = (bf16[128,2048]{1,0:T(8,128)(2,1)S(1)}, bf16[128,2048]{1,0:T(8,128)(2,1)}, u32[]{:S(2)}, u32[]{:S(2)}) collective-permute-start(bf16[128,2048]{1,0:T(8,128)(2,1)S(1)} %collective-permute-done.23.rest_6_), channel_id=1, source_target_pairs={{0,1},{1,0},{2,3},{3,2},{4,5},{5,4},{6,7},{7,6},{8,9},{9,8},{10,11... | collective-permute-start | bytes 1572872 | tf_op jit(solution)/shard_map/ppermute | solution.py:383
  138.3 2.3 %copy-start.18 = (bf16[128,2048]{1,0:T(8,128)(2,1)}, bf16[128,2048]{1,0:T(8,128)(2,1)S(1)}, u32[]{:S(2)}) copy-start(bf16[128,2048]{1,0:T(8,128)(2,1)S(1)} %collective-permute-done.18.rest_1_) | copy-start | bytes 1572868
  138.4 2.3 %copy-start.19 = (bf16[128,2048]{1,0:T(8,128)(2,1)}, bf16[128,2048]{1,0:T(8,128)(2,1)S(1)}, u32[]{:S(2)}) copy-start(bf16[128,2048]{1,0:T(8,128)(2,1)S(1)} %collective-permute-done.20.rest_3_) | copy-start | bytes 1572868
  139.8 0.8 copy-start.20
  152.4 8.9 %collective-permute-start.26 = (bf16[1024,256]{1,0:T(8,128)(2,1)S(1)}, bf16[1024,256]{1,0:T(8,128)(2,1)S(1)}, u32[]{:S(2)}, u32[]{:S(2)}) collective-permute-start(bf16[1024,256]{1,0:T(8,128)(2,1)S(1)} %get-tuple-element.64), channel_id=1, source_target_pairs={{0,1},{1,0},{2,3},{3,2},{4,5},{5,4},{6,7},{7,6},{8,9},{9,8},{10,11... | collective-permute-start | bytes 1572872 | tf_op jit(solution)/shard_map/ppermute | solution.py:383
  157.5 4.1 %collective-permute-start.28 = (bf16[1024,256]{1,0:T(8,128)(2,1)S(1)}, bf16[1024,256]{1,0:T(8,128)(2,1)S(1)}, u32[]{:S(2)}, u32[]{:S(2)}) collective-permute-start(bf16[1024,256]{1,0:T(8,128)(2,1)S(1)} %get-tuple-element.66), channel_id=1, source_target_pairs={{0,1},{1,0},{2,3},{3,2},{4,5},{5,4},{6,7},{7,6},{8,9},{9,8},{10,11... | collective-permute-start | bytes 1572872 | tf_op jit(solution)/shard_map/ppermute | solution.py:383
  160.7 3.9 %collective-permute-start.25 = (bf16[1024,256]{1,0:T(8,128)(2,1)S(1)}, bf16[1024,256]{1,0:T(8,128)(2,1)S(1)}, u32[]{:S(2)}, u32[]{:S(2)}) collective-permute-start(bf16[1024,256]{1,0:T(8,128)(2,1)S(1)} %get-tuple-element.62), channel_id=1, source_target_pairs={{0,1},{1,0},{2,3},{3,2},{4,5},{5,4},{6,7},{7,6},{8,9},{9,8},{10,11... | collective-permute-start | bytes 1572872 | tf_op jit(solution)/shard_map/ppermute | solution.py:383
  161.2 2.3 %collective-permute-start.30 = (bf16[1024,256]{1,0:T(8,128)(2,1)S(1)}, bf16[1024,256]{1,0:T(8,128)(2,1)S(1)}, u32[]{:S(2)}, u32[]{:S(2)}) collective-permute-start(bf16[1024,256]{1,0:T(8,128)(2,1)S(1)} %get-tuple-element.68), channel_id=1, source_target_pairs={{0,1},{1,0},{2,3},{3,2},{4,5},{5,4},{6,7},{7,6},{8,9},{9,8},{10,11... | collective-permute-start | bytes 1572872 | tf_op jit(solution)/shard_map/ppermute | solution.py:383
  161.5 14.7 %collective-permute-start.27 = (bf16[1024,256]{1,0:T(8,128)(2,1)S(1)}, bf16[1024,256]{1,0:T(8,128)(2,1)S(1)}, u32[]{:S(2)}, u32[]{:S(2)}) collective-permute-start(bf16[1024,256]{1,0:T(8,128)(2,1)S(1)} %add_convert_fusion.3), channel_id=1, source_target_pairs={{0,4},{2,6},{4,0},{6,2},{1,5},{3,7},{5,1},{7,3},{8,12},{10,14},{12... | collective-permute-start | bytes 1572872 | tf_op jit(solution)/shard_map/ppermute | solution.py:379
  161.7 26.3 %collective-permute-start.29 = (bf16[1024,256]{1,0:T(8,128)(2,1)S(1)}, bf16[1024,256]{1,0:T(8,128)(2,1)S(1)}, u32[]{:S(2)}, u32[]{:S(2)}) collective-permute-start(bf16[1024,256]{1,0:T(8,128)(2,1)S(1)} %add_convert_fusion.2), channel_id=1, source_target_pairs={{0,2},{2,4},{4,6},{6,0},{1,3},{3,5},{5,7},{7,1},{8,10},{10,12},{12... | collective-permute-start | bytes 1572872 | tf_op jit(solution)/shard_map/ppermute | solution.py:379
  163.6 24.4 %collective-permute-start.31 = (bf16[1024,256]{1,0:T(8,128)(2,1)S(1)}, bf16[1024,256]{1,0:T(8,128)(2,1)S(1)}, u32[]{:S(2)}, u32[]{:S(2)}) collective-permute-start(bf16[1024,256]{1,0:T(8,128)(2,1)S(1)} %add_convert_fusion.1), channel_id=1, source_target_pairs={{0,6},{2,0},{4,2},{6,4},{1,7},{3,1},{5,3},{7,5},{8,14},{10,8},{12,... | collective-permute-start | bytes 1572872 | tf_op jit(solution)/shard_map/ppermute | solution.py:379
Sparse Core Ops, SparseCore 0:
  55.3 71.1 all-gather.1

commit v3 on v2

--- a/solution.py
+++ b/solution.py
@@ -26,6 +26,77 @@
 
 def in_hbm(arrays):
     return [pltpu.with_memory_space_constraint(a, pltpu.HBM) for a in arrays]
+
+
+def pack_kernel(tab, *rest):
+    arrays, outs, (q_ref, v_ref, k_ref, g_ref, d_ref, msgs, sems) = rest[:5], rest[5:9], rest[9:]
+    copies = [
+        pltpu.make_async_copy(a, to, sems.at[n]) for n, (a, to) in enumerate(zip(arrays, (q_ref, v_ref, k_ref, g_ref, d_ref)))
+    ]
+    for copy in copies:
+        copy.start()
+    for copy in copies:
+        copy.wait()
+    q_t = (q_ref[...].astype(jnp.float32) * 0.125).T.astype(jnp.bfloat16)
+    v_t = v_ref[...].astype(jnp.float32).T.astype(jnp.bfloat16)
+    docs = d_ref[...].astype(jnp.float32)
+    hi = g_ref[...].astype(jnp.bfloat16).astype(jnp.float32)
+    rest_of = g_ref[...] - hi
+    mid = rest_of.astype(jnp.bfloat16).astype(jnp.float32)
+    low = (rest_of - mid).astype(jnp.bfloat16).astype(jnp.float32)
+
+    def blank(rows):
+        return jnp.zeros((rows, 128), jnp.float32)
+
+    def chunk(a, row, n):
+        return a[row : row + 1, 128 * n : 128 * (n + 1)]
+
+    for head in range(2):
+        lanes = slice(64 * head, 64 * (head + 1))
+        for half in range(2):
+            m = 2 * head + half
+            at = HALF * half
+            msgs[m, 0:KROWS, :] = jnp.concatenate(
+                [k_ref[at : at + 256, lanes], k_ref[at + 256 : at + 512, lanes]], axis=1
+            )
+            for n in range(4):
+                to = KROWS + 64 * n
+                msgs[m, to : to + 64, :] = v_t[lanes, at + 128 * n : at + 128 * (n + 1)]
+                tokens = at + 128 * n
+                to = KV_ROWS + 64 * n
+                msgs[m, to : to + 64, :] = q_t[lanes, tokens : tokens + 128]
+            for k in range(2):
+                rows = [chunk(a, head, 4 * half + k + 2 * side) for side in range(2) for a in (hi, mid, low)]
+                rows.append(blank(2))
+                if k == 0:
+                    rows += [chunk(docs, 0, 4 * half + n) for n in range(4)] + [blank(4)]
+                else:
+                    rows.append(blank(8))
+                to = KROWS + VROWS + 16 * k
+                msgs[m, to : to + 16, :] = jnp.concatenate(rows, axis=0).astype(jnp.bfloat16)
+    for step in range(4):
+        outs[step][...] = msgs[tab[40 + step]]
+
+
+def pack(table, q, k, v, g, d):
+    vmem = pl.BlockSpec(memory_space=pltpu.VMEM)
+    rows = KV_ROWS + Q_ROWS
+    return pl.pallas_call(
+        pack_kernel,
+        out_shape=[jax.ShapeDtypeStruct((rows, 128), jnp.bfloat16)] * 4,
+        in_specs=[pl.BlockSpec(memory_space=pltpu.SMEM)] + [pl.BlockSpec(memory_space=pltpu.HBM)] * 5,
+        out_specs=[vmem] * 4,
+        scratch_shapes=[pltpu.VMEM((TOK, 128), jnp.bfloat16)] * 3
+        + [
+            pltpu.VMEM((2, TOK), jnp.float32),
+            pltpu.VMEM((1, TOK), jnp.int32),
+            pltpu.VMEM((4, rows, 128), jnp.bfloat16),
+            pltpu.SemaphoreType.DMA((5,)),
+        ],
+        compiler_params=pltpu.CompilerParams(vmem_limit_bytes=16 * 1024 * 1024),
+        cost_estimate=pl.CostEstimate(flops=10_000_000, bytes_accessed=2_000_000, transcendentals=0),
+        name="pack",
+    )(table, *in_hbm([q, v, k, g, d]))
 
 
 DIMS = (((1,), (0,)), ((), ()))
@@ -396,6 +467,7 @@
         row += [xs * 256 + k * 128 for xs, k in order]
         row += [k * 512 + xs * 128 for xs, k in order]
         row += [(2 * x + c) * 256, c] + [(x + r) % 4 * 4 for r in range(4)]
+        row += [2 * ((z & 1) ^ (k & 1)) + ((z >> 1) ^ (k >> 1)) for k in range(4)]
         rows.append(row)
     return np.asarray(rows, np.int32)
 
@@ -405,24 +477,9 @@
 
 def body(queries, keys, values, cum_gates, doc_ids, residual, w_out, norm_gain, w_up, w_down):
     z, y, x, c = (lax.axis_index(a) for a in ("z", "y", "x", "c"))
-    table = lax.dynamic_slice(jnp.asarray(PLACES), (((z * 4 + y) * 4 + x) * 2 + c, 0), (1, 40)).reshape(40)
-
-    q_t = jnp.transpose(queries * jnp.bfloat16(0.125)).reshape(2, HD, 2, 4, 128)
-    q_msg = jnp.transpose(q_t, (0, 2, 3, 1, 4)).reshape(2, 2, Q_ROWS, 128)
-    v_t = jnp.transpose(values).reshape(2, HD, 2, 4, 128)
-    v_msg = jnp.transpose(v_t, (0, 2, 3, 1, 4)).reshape(2, 2, VROWS, 128)
-    k_msg = jnp.transpose(keys.reshape(2, 2, KROWS, 2, HD), (3, 0, 2, 1, 4)).reshape(2, 2, KROWS, 128)
-    gates = jnp.transpose(cum_gates).reshape(2, 2, 2, 2, 128)
-    hi = lax.reduce_precision(gates, 8, 7)
-    mid = lax.reduce_precision(gates - hi, 8, 7)
-    low = gates - hi - mid
-    three = jnp.transpose(jnp.stack([hi, mid, low]), (1, 2, 4, 3, 0, 5)).reshape(2, 2, 2, 6, 128)
-    docs = jnp.broadcast_to(doc_ids.astype(jnp.float32).reshape(1, 2, 4, 128), (2, 2, 4, 128))
-    docs = jnp.stack([docs, jnp.zeros_like(docs)], axis=2)
-    three = jnp.pad(three, ((0, 0), (0, 0), (0, 0), (0, 2), (0, 0)))
-    docs = jnp.pad(docs, ((0, 0), (0, 0), (0, 0), (0, 4), (0, 0)))
-    g_msg = jnp.concatenate([three, docs], axis=3).reshape(2, 2, GROWS, 128).astype(jnp.bfloat16)
-    messages = jnp.concatenate([k_msg, v_msg, g_msg, q_msg], axis=2)
+    table = lax.dynamic_slice(jnp.asarray(PLACES), (((z * 4 + y) * 4 + x) * 2 + c, 0), (1, 44)).reshape(44)
+
+    messages = pack(table, queries, keys, values, jnp.transpose(cum_gates), doc_ids.reshape(1, TOK))
 
     received = []
     for step in range(4):
@@ -432,10 +489,7 @@
                 j = 2 * cs + ((zs & 1) ^ (step & 1))
                 cd = (zs >> 1) ^ (step >> 1)
                 pairs.append((zs * 2 + cs, j * 2 + cd))
-        head = (z & 1) ^ (step & 1)
-        half = (z >> 1) ^ (step >> 1)
-        message = lax.dynamic_slice(messages, (head, half, 0, 0), (1, 1, KV_ROWS + Q_ROWS, 128))[0, 0]
-        received.append(lax.ppermute(message, ("z", "c"), pairs))
+        received.append(lax.ppermute(messages[step], ("z", "c"), pairs))
     gain_row = jnp.pad(norm_gain[None], ((0, 7), (0, D - 256)))
     w_msg = jnp.concatenate([w_out, gain_row], axis=0)
     w_mine = [w_msg] + [shifted(w_msg, "x", r) for r in RING]

time: 197 us -> 195 us (0.990)
  local copies, waits for them, and re-layouts: 7.66 us -> 4.55 us
  Pallas kernels: 46.4 us -> 48.7 us
    pallas_call x0 -> x1, Pallas kernels: none -> 2.06 us  [pack(): pl.pallas_call(pack_kernel, out_shape=[jax.ShapeDtypeStruct((rows, 128),...]
where the time goes in v3:
time: 195 us; the launch traced here: 194 us
  waiting for transfers between devices  60.7 us (31%)
  starting transfers between devices  52.1 us (27%)
  Pallas kernels  48.7 us (25%)
  between operations  13.8 us (7%)
  blocking collectives  11.5 us (6%)
  local copies, waits for them, and re-layouts  4.55 us (2%)
  other arithmetic  2.79 us (1%)
    ppermute x12, waiting for transfers between devices, shifted(): return lax.ppermute(value, axis, [(i, (i - by) % n) for i in range(n)])  49.8 us
    pallas_call x2, Pallas kernels, attend(): pl.pallas_call(functools.partial(attend_kernel, n_arr, first, last), out_...  23.7 us
    ppermute x16, starting transfers between devices, partner(): return lax.ppermute(value, 'c', [(0, 1), (1, 0)])  21.6 us
    ppermute x12, starting transfers between devices, shifted(): return lax.ppermute(value, axis, [(i, (i - by) % n) for i in range(n)])  15.3 us
    all_to_all x1, blocking collectives, body(): attended = lax.all_to_all(out, ('x', 'z'), 0, 0, tiled=True)  11.5 us
    pallas_call x3, Pallas kernels, down(): pl.pallas_call(functools.partial(down_kernel, steps), out_shape=[jax.Shap...  10.5 us
    ppermute x4, starting transfers between devices, body(): received.append(lax.ppermute(messages[step], ('z', 'c'), pairs))  10 us
    pallas_call x1, Pallas kernels, up(): pl.pallas_call(up_kernel, out_shape=[jax.ShapeDtypeStruct((1024, 1024), j...  8.63 us
  transfers between devices with their start and end apart: 34, of which 14 were waited for; matrix products, arithmetic and copies ran while one was open for 1% of the time, Pallas kernels for 18%

profile of v3, /device:TPU:1, one launch (start us, length us, event | category | flops | bytes accessed | tf_op | source)
XLA Modules:
  0.0 194.2 jit_solution(14700466805131845540)
XLA Ops:
  6.5 0.7 dynamic-slice_bitcast_fusion.tab.sc
  7.2 2.1 %pack.1 = (bf16[800,128]{1,0:T(8,128)(2,1)S(1)}, bf16[800,128]{1,0:T(8,128)(2,1)S(1)}, bf16[800,128]{1,0:T(8,128)(2,1)S(1)}, bf16[800,128]{1,0:T(8,128)(2,1)S(1)}) custom-call(s32[44]{0:T(128)S(1)} %dynamic-slice_bitcast_fusion.tab.sc, bf16[1024,128]{1,0:T(8,128)(2,1)} %rest_0_.1, bf16[1024,128]{1,0:T(8,128)(2,1)} %rest_1_.1, bf16[1024,128]{1,0:T(8,128)(2,1)} %rest_2_.1, ...), custom_call_target="tpu_custom_call" | custom-call | flops 10000000 | bytes 2000000 | tf_op jit(solution)/shard_map/pack/pallas_call | solution.py:84
  9.3 4.7 %collective-permute-start.6 = (bf16[800,128]{1,0:T(8,128)(2,1)S(1)}, bf16[800,128]{1,0:T(8,128)(2,1)S(1)}, u32[]{:S(2)}, u32[]{:S(2)}) collective-permute-start(bf16[800,128]{1,0:T(8,128)(2,1)S(1)} %get-tuple-element.44), channel_id=1, source_target_pairs={{0,33},{1,97},{32,1},{33,65},{64,32},{65,96},{96,0},{97,64},{2,35}... | collective-permute-start | bytes 614408 | tf_op jit(solution)/shard_map/ppermute | solution.py:492
  14.0 1.7 collective-permute-start.5
  15.7 3.6 %collective-permute-start.3 = (bf16[800,128]{1,0:T(8,128)(2,1)S(1)}, bf16[800,128]{1,0:T(8,128)(2,1)S(1)}, u32[]{:S(2)}, u32[]{:S(2)}) collective-permute-start(bf16[800,128]{1,0:T(8,128)(2,1)S(1)} %get-tuple-element.41), channel_id=1, source_target_pairs={{0,0},{1,64},{32,32},{33,96},{64,1},{65,65},{96,33},{97,97},{2,2},... | collective-permute-start | bytes 614408 | tf_op jit(solution)/shard_map/ppermute | solution.py:492
  19.4 0.2 collective-permute-done.5
  19.6 3.5 %collective-permute-done.4 = bf16[800,128]{1,0:T(8,128)(2,1)S(1)} collective-permute-done((bf16[800,128]{1,0:T(8,128)(2,1)S(1)}, bf16[800,128]{1,0:T(8,128)(2,1)S(1)}, u32[]{:S(2)}, u32[]{:S(2)}) %collective-permute-start.4) | collective-permute-done | bytes 204832 | tf_op jit(solution)/shard_map/ppermute | solution.py:492
  23.0 2.3 %collective-permute-done.3 = bf16[800,128]{1,0:T(8,128)(2,1)S(1)} collective-permute-done((bf16[800,128]{1,0:T(8,128)(2,1)S(1)}, bf16[800,128]{1,0:T(8,128)(2,1)S(1)}, u32[]{:S(2)}, u32[]{:S(2)}) %collective-permute-start.3) | collective-permute-done | bytes 204832 | tf_op jit(solution)/shard_map/ppermute | solution.py:492
  25.5 2.8 %collective-permute-start.7 = (bf16[4,544,128]{2,1,0:T(8,128)(2,1)S(1)}, bf16[4,544,128]{2,1,0:T(8,128)(2,1)}, u32[]{:S(2)}, u32[]{:S(2)}) collective-permute-start(bf16[4,544,128]{2,1,0:T(8,128)(2,1)S(1)} %pad_maximum_fusion.rest_0_), channel_id=1, source_target_pairs={{0,24},{8,0},{16,8},{24,16},{1,25},{9,1},{17,9},{25,17},{2,26},{10... | collective-permute-start | bytes 1671176 | tf_op jit(solution)/shard_map/ppermute | solution.py:450
  28.3 1.6 collective-permute-start.9
  30.0 0.1 copy.12
  30.1 0.1 collective-permute-start.10
  30.3 0.1 convert_reduce_fusion
  30.4 0.8 pad_maximum_fusion.1
  31.3 0.9 collective-permute-done.10.rest_1_
  32.2 0.8 copy-done.12
  33.0 9.1 %attend_first.1 = (f32[4,1,512]{2,1,0:T(1,128)S(1)}, f32[4,1,512]{2,1,0:T(1,128)S(1)}, f32[4,64,512]{2,1,0:T(8,128)S(1)}) custom-call(s32[44]{0:T(128)S(1)} %dynamic-slice_bitcast_fusion.tab.sc, s32[4]{0:T(128)S(1)} %subtract_convert_fusion.zeros_q, bf16[4,256,128]{2,1,0:T(8,128)(2,1)S(1)} %pad_maximum_fusion.2.qt_ref, bf16[4,544,128]{2,1,0:T(8,128)(2,1)} %copy-done.2, ...), custom_call_target="tpu_custom_call" | custom-call | flops 8000000000 | bytes 2000000 | tf_op jit(solution)/shard_map/attend_first/pallas_call | solution.py:301
  42.1 7.4 %collective-permute-done.7.rest_0_ = bf16[4,544,128]{2,1,0:T(8,128)(2,1)} collective-permute-done((bf16[4,544,128]{2,1,0:T(8,128)(2,1)S(1)}, bf16[4,544,128]{2,1,0:T(8,128)(2,1)}, u32[]{:S(2)}, u32[]{:S(2)}) %collective-permute-start.7) | collective-permute-done | bytes 557088 | tf_op jit(solution)/shard_map/ppermute | solution.py:450
  49.5 3.5 %collective-permute-done.8.rest_2_ = bf16[4,544,128]{2,1,0:T(8,128)(2,1)} collective-permute-done((bf16[4,544,128]{2,1,0:T(8,128)(2,1)S(1)}, bf16[4,544,128]{2,1,0:T(8,128)(2,1)}, u32[]{:S(2)}, u32[]{:S(2)}) %collective-permute-start.8) | collective-permute-done | bytes 557088 | tf_op jit(solution)/shard_map/ppermute | solution.py:450
  53.0 0.1 collective-permute-start.11
  53.1 0.5 collective-permute-start.12
  53.6 0.1 collective-permute-start.13
  53.8 2.5 %collective-permute-start = (bf16[136,2048]{1,0:T(8,128)(2,1)S(1)}, bf16[136,2048]{1,0:T(8,128)(2,1)S(1)}, u32[]{:S(2)}, u32[]{:S(2)}) collective-permute-start(bf16[136,2048]{1,0:T(8,128)(2,1)S(1)} %fusion.1.rest_0_), channel_id=1, source_target_pairs={{0,6},{2,0},{4,2},{6,4},{1,7},{3,1},{5,3},{7,5},{8,14},{10,8},{12,... | collective-permute-start | bytes 1671176 | tf_op jit(solution)/shard_map/ppermute | solution.py:450
  56.3 5.2 %all-to-all-start = ((bf16[8,128,256]{2,1,0:T(8,128)(2,1)}), bf16[8,128,256]{2,1,0:T(8,128)(2,1)S(1)}, u32[]{:S(2)}, u32[]{:S(2)}) async-start(bf16[8,128,256]{2,1,0:T(8,128)(2,1)} %bitcast.7), calls=%async_computation | async-start | bytes 1048576 | tf_op jit(solution)/shard_map/all_to_all | solution.py:510
  61.5 2.9 %collective-permute-start.2 = (bf16[136,2048]{1,0:T(8,128)(2,1)S(1)}, bf16[136,2048]{1,0:T(8,128)(2,1)}, u32[]{:S(2)}, u32[]{:S(2)}) collective-permute-start(bf16[136,2048]{1,0:T(8,128)(2,1)S(1)} %fusion.1.rest_0_), channel_id=1, source_target_pairs={{0,4},{2,6},{4,0},{6,2},{1,5},{3,7},{5,1},{7,3},{8,12},{10,14},{12... | collective-permute-start | bytes 1671176 | tf_op jit(solution)/shard_map/ppermute | solution.py:450
  64.4 14.6 %attend_last.1 = bf16[16,64,128]{2,1,0:T(8,128)(2,1)S(1)} custom-call(s32[44]{0:T(128)S(1)} %dynamic-slice_bitcast_fusion.tab.sc, s32[4]{0:T(128)S(1)} %subtract_convert_fusion.zeros_q, bf16[4,256,128]{2,1,0:T(8,128)(2,1)S(1)} %pad_maximum_fusion.2.qt_ref, bf16[4,544,128]{2,1,0:T(8,128)(2,1)} %collective-permute-done.7.rest_0_, ...), custom_call_target="tpu_custom_call" | custom-call | flops 24000000000 | bytes 6000000 | tf_op jit(solution)/shard_map/attend_last/pallas_call | solution.py:301
  79.0 8.7 %collective-permute-done.2.rest_6_ = bf16[136,2048]{1,0:T(8,128)(2,1)} collective-permute-done((bf16[136,2048]{1,0:T(8,128)(2,1)S(1)}, bf16[136,2048]{1,0:T(8,128)(2,1)}, u32[]{:S(2)}, u32[]{:S(2)}) %collective-permute-start.2) | collective-permute-done | bytes 557088 | tf_op jit(solution)/shard_map/ppermute | solution.py:450
  87.7 2.1 %all-to-all-done.res_ref = bf16[8,128,256]{2,1,0:T(8,128)(2,1)S(1)} async-done(((bf16[8,128,256]{2,1,0:T(8,128)(2,1)}), bf16[8,128,256]{2,1,0:T(8,128)(2,1)S(1)}, u32[]{:S(2)}, u32[]{:S(2)}) %all-to-all-start) | async-done | bytes 524320 | tf_op jit(solution)/shard_map/all_to_all | solution.py:510
  89.8 0.5 collective-permute-start.15
  90.3 0.5 collective-permute-start.17
  90.8 11.5 %all_to_all.10.att_ref = bf16[16,64,128]{2,1,0:T(8,128)(2,1)S(1)} all-to-all(bf16[16,64,128]{2,1,0:T(8,128)(2,1)S(1)} %attend_last.1), channel_id=1, replica_groups=mesh['z'=4,'y'=4,'x'=4,'c'=2] {'x','z'}, dimensions={0} | all-to-all | bytes 524288 | tf_op jit(solution)/shard_map/all_to_all | solution.py:520
  102.5 0.8 copy-done.5
  103.2 0.2 copy-done.6
  103.4 0.2 copy-done.7
  103.6 0.8 copy-done.8
  104.4 3.8 %dense.1 = (bf16[128,2048]{1,0:T(8,128)(2,1)S(1)}, bf16[8,2048]{1,0:T(8,128)(2,1)S(1)}) custom-call(s32[44]{0:T(128)S(1)} %dynamic-slice_bitcast_fusion.tab.sc, bf16[16,64,128]{2,1,0:T(8,128)(2,1)S(1)} %all_to_all.10.att_ref, bf16[8,128,256]{2,1,0:T(8,128)(2,1)S(1)} %all-to-all-done.res_ref, bf16[136,2048]{1,0:T(8,128)(2,1)} %copy-done.1, ...), custom_call_target="tpu_custom_call" | custom-call | flops 1000000000 | bytes 4000000 | tf_op jit(solution)/shard_map/dense/pallas_call | solution.py:344
  108.2 1.5 collective-permute-start.19
  109.8 1.4 collective-permute-start.23
  111.2 2.2 %collective-permute-start.18 = (bf16[128,2048]{1,0:T(8,128)(2,1)S(1)}, bf16[128,2048]{1,0:T(8,128)(2,1)S(1)}, u32[]{:S(2)}, u32[]{:S(2)}) collective-permute-start(bf16[128,2048]{1,0:T(8,128)(2,1)S(1)} %get-tuple-element.66.rest_0_), channel_id=1, source_target_pairs={{0,1},{1,0},{2,3},{3,2},{4,5},{5,4},{6,7},{7,6},{8,9},{9,8},{10,11... | collective-permute-start | bytes 1572872 | tf_op jit(solution)/shard_map/ppermute | solution.py:454
  113.4 6.9 %collective-permute-done.19.rest_2_ = bf16[128,2048]{1,0:T(8,128)(2,1)S(1)} collective-permute-done((bf16[128,2048]{1,0:T(8,128)(2,1)S(1)}, bf16[128,2048]{1,0:T(8,128)(2,1)S(1)}, u32[]{:S(2)}, u32[]{:S(2)}) %collective-permute-start.19) | collective-permute-done | bytes 524320 | tf_op jit(solution)/shard_map/ppermute | solution.py:450
  120.3 4.5 %collective-permute-start.20 = (bf16[128,2048]{1,0:T(8,128)(2,1)S(1)}, bf16[128,2048]{1,0:T(8,128)(2,1)S(1)}, u32[]{:S(2)}, u32[]{:S(2)}) collective-permute-start(bf16[128,2048]{1,0:T(8,128)(2,1)S(1)} %collective-permute-done.19.rest_2_), channel_id=1, source_target_pairs={{0,1},{1,0},{2,3},{3,2},{4,5},{5,4},{6,7},{7,6},{8,9},{9,8},{10,11... | collective-permute-start | bytes 1572872 | tf_op jit(solution)/shard_map/ppermute | solution.py:454
  124.8 11.7 %collective-permute-start.22 = (bf16[128,2048]{1,0:T(8,128)(2,1)S(1)}, bf16[128,2048]{1,0:T(8,128)(2,1)S(1)}, u32[]{:S(2)}, u32[]{:S(2)}) collective-permute-start(bf16[128,2048]{1,0:T(8,128)(2,1)S(1)} %collective-permute-done.21.rest_4_), channel_id=1, source_target_pairs={{0,1},{1,0},{2,3},{3,2},{4,5},{5,4},{6,7},{7,6},{8,9},{9,8},{10,11... | collective-permute-start | bytes 1572872 | tf_op jit(solution)/shard_map/ppermute | solution.py:454
  136.5 0.1 collective-permute-start.24
  136.6 1.4 collective-permute-done.22.rest_5_
  138.1 0.8 copy-done.18
  138.9 0.1 collective-permute-done.24.rest_7_
  139.0 8.6 %up.1 = (bf16[1024,1024]{1,0:T(8,128)(2,1)S(1)}, bf16[1024,256]{1,0:T(8,128)(2,1)S(1)}) custom-call(s32[44]{0:T(128)S(1)} %dynamic-slice_bitcast_fusion.tab.sc, bf16[8,2048]{1,0:T(8,128)(2,1)S(1)} %get-tuple-element.64.gain_ref, bf16[4096,1024]{1,0:T(8,128)(2,1)} %all-gather.2.cloned.1.call-done.w_in, bf16[128,2048]{1,0:T(8,128)(2,1)} %copy-done, ...), custom_call_target="tpu_custom_call" | custom-call | flops 4300000256 | bytes 8000000 | tf_op jit(solution)/shard_map/up/pallas_call | solution.py:386
  147.6 3.1 %down.4 = (bf16[1024,256]{1,0:T(8,128)(2,1)S(1)}, bf16[1024,256]{1,0:T(8,128)(2,1)S(1)}) custom-call(s32[44]{0:T(128)S(1)} %dynamic-slice_bitcast_fusion.tab.sc, bf16[1024,1024]{1,0:T(8,128)(2,1)S(1)} %get-tuple-element.68.h_ref, bf16[4096,1024]{1,0:T(8,128)(2,1)} %all-gather.2.cloned.1.call-done.w_in), custom_call_target="tpu_custom_call" | custom-call | flops 1100000000 | bytes 4000000 | tf_op jit(solution)/shard_map/down/pallas_call | solution.py:434
  150.7 0.4 collective-permute-start.26
  151.1 4.4 %down.5 = (bf16[1024,256]{1,0:T(8,128)(2,1)S(1)}, bf16[1024,256]{1,0:T(8,128)(2,1)S(1)}, bf16[1024,256]{1,0:T(8,128)(2,1)S(1)}, bf16[1024,256]{1,0:T(8,128)(2,1)S(1)}) custom-call(s32[44]{0:T(128)S(1)} %dynamic-slice_bitcast_fusion.tab.sc, bf16[1024,1024]{1,0:T(8,128)(2,1)S(1)} %get-tuple-element.68.h_ref, bf16[4096,1024]{1,0:T(8,128)(2,1)} %all-gather.2.cloned.1.call-done.w_in), custom_call_target="tpu_custom_call" | custom-call | flops 2200000000 | bytes 4000000 | tf_op jit(solution)/shard_map/down/pallas_call | solution.py:434
  155.5 0.2 collective-permute-start.28
  155.7 3.1 %down.3 = (bf16[1024,256]{1,0:T(8,128)(2,1)S(1)}, bf16[1024,256]{1,0:T(8,128)(2,1)S(1)}) custom-call(s32[44]{0:T(128)S(1)} %dynamic-slice_bitcast_fusion.tab.sc, bf16[1024,1024]{1,0:T(8,128)(2,1)S(1)} %get-tuple-element.68.h_ref, bf16[4096,1024]{1,0:T(8,128)(2,1)} %all-gather.2.cloned.1.call-done.w_in), custom_call_target="tpu_custom_call" | custom-call | flops 1100000000 | bytes 4000000 | tf_op jit(solution)/shard_map/down/pallas_call | solution.py:434
  158.8 0.5 collective-permute-start.25
  159.3 0.1 collective-permute-start.30
  159.4 0.1 add_convert_fusion.3
  159.5 0.1 collective-permute-start.27
  159.6 0.1 add_convert_fusion.2
  159.8 1.4 collective-permute-start.29
  161.2 0.4 collective-permute-done.30
  161.5 0.2 add_convert_fusion.1
  161.7 1.1 collective-permute-start.31
  162.8 11.5 %collective-permute-done.27 = bf16[1024,256]{1,0:T(8,128)(2,1)S(1)} collective-permute-done((bf16[1024,256]{1,0:T(8,128)(2,1)S(1)}, bf16[1024,256]{1,0:T(8,128)(2,1)S(1)}, u32[]{:S(2)}, u32[]{:S(2)}) %collective-permute-start.27) | collective-permute-done | bytes 524320 | tf_op jit(solution)/shard_map/ppermute | solution.py:450
  174.3 11.8 %collective-permute-done.29 = bf16[1024,256]{1,0:T(8,128)(2,1)S(1)} collective-permute-done((bf16[1024,256]{1,0:T(8,128)(2,1)S(1)}, bf16[1024,256]{1,0:T(8,128)(2,1)S(1)}, u32[]{:S(2)}, u32[]{:S(2)}) %collective-permute-start.29) | collective-permute-done | bytes 524320 | tf_op jit(solution)/shard_map/ppermute | solution.py:450
  186.1 1.2 add_convert_fusion
  (75 shorter events, 0.4 us)
Async XLA Ops:
  6.5 132.4 %all-gather.2.cloned.1.call-start = ((), (), s32[]{:S(2)}) async-start(), calls=%async_computation.2 | async-start | bytes 8912896 | tf_op jit(solution)/shard_map/all_gather | solution.py:512
  9.3 10.0 %collective-permute-start.6 = (bf16[800,128]{1,0:T(8,128)(2,1)S(1)}, bf16[800,128]{1,0:T(8,128)(2,1)S(1)}, u32[]{:S(2)}, u32[]{:S(2)}) collective-permute-start(bf16[800,128]{1,0:T(8,128)(2,1)S(1)} %get-tuple-element.44), channel_id=1, source_target_pairs={{0,33},{1,97},{32,1},{33,65},{64,32},{65,96},{96,0},{97,64},{2,35}... | collective-permute-start | bytes 614408 | tf_op jit(solution)/shard_map/ppermute | solution.py:492
  14.0 5.6 %collective-permute-start.5 = (bf16[800,128]{1,0:T(8,128)(2,1)S(1)}, bf16[800,128]{1,0:T(8,128)(2,1)S(1)}, u32[]{:S(2)}, u32[]{:S(2)}) collective-permute-start(bf16[800,128]{1,0:T(8,128)(2,1)S(1)} %get-tuple-element.43), channel_id=1, source_target_pairs={{0,1},{1,65},{32,33},{33,97},{64,0},{65,64},{96,32},{97,96},{2,3},... | collective-permute-start | bytes 614408 | tf_op jit(solution)/shard_map/ppermute | solution.py:492
  15.7 7.3 %collective-permute-start.4 = (bf16[800,128]{1,0:T(8,128)(2,1)S(1)}, bf16[800,128]{1,0:T(8,128)(2,1)S(1)}, u32[]{:S(2)}, u32[]{:S(2)}) collective-permute-start(bf16[800,128]{1,0:T(8,128)(2,1)S(1)} %get-tuple-element.42), channel_id=1, source_target_pairs={{0,32},{1,96},{32,0},{33,64},{64,33},{65,97},{96,1},{97,65},{2,34}... | collective-permute-start | bytes 614408 | tf_op jit(solution)/shard_map/ppermute | solution.py:492
  15.7 14.3 %copy-start.10 = (bf16[1024,128]{1,0:T(8,128)(2,1)S(1)}, bf16[1024,128]{1,0:T(8,128)(2,1)}, u32[]{:S(2)}) copy-start(bf16[1024,128]{1,0:T(8,128)(2,1)} %param.20) | copy-start | bytes 786436
  15.7 9.7 %collective-permute-start.3 = (bf16[800,128]{1,0:T(8,128)(2,1)S(1)}, bf16[800,128]{1,0:T(8,128)(2,1)S(1)}, u32[]{:S(2)}, u32[]{:S(2)}) collective-permute-start(bf16[800,128]{1,0:T(8,128)(2,1)S(1)} %get-tuple-element.41), channel_id=1, source_target_pairs={{0,0},{1,64},{32,32},{33,96},{64,1},{65,65},{96,33},{97,97},{2,2},... | collective-permute-start | bytes 614408 | tf_op jit(solution)/shard_map/ppermute | solution.py:492
  25.4 5.0 %copy-start.11 = (bf16[128,1024]{1,0:T(8,128)(2,1)S(1)}, bf16[128,1024]{1,0:T(8,128)(2,1)}, u32[]{:S(2)}) copy-start(bf16[128,1024]{1,0:T(8,128)(2,1)} %param.19) | copy-start | bytes 786436
  25.5 5.8 %copy-start.2 = (bf16[4,544,128]{2,1,0:T(8,128)(2,1)}, bf16[4,544,128]{2,1,0:T(8,128)(2,1)S(1)}, u32[]{:S(2)}) copy-start(bf16[4,544,128]{2,1,0:T(8,128)(2,1)S(1)} %pad_maximum_fusion.rest_0_) | copy-start | bytes 1671172
  25.5 24.0 %collective-permute-start.7 = (bf16[4,544,128]{2,1,0:T(8,128)(2,1)S(1)}, bf16[4,544,128]{2,1,0:T(8,128)(2,1)}, u32[]{:S(2)}, u32[]{:S(2)}) collective-permute-start(bf16[4,544,128]{2,1,0:T(8,128)(2,1)S(1)} %pad_maximum_fusion.rest_0_), channel_id=1, source_target_pairs={{0,24},{8,0},{16,8},{24,16},{1,25},{9,1},{17,9},{25,17},{2,26},{10... | collective-permute-start | bytes 1671176 | tf_op jit(solution)/shard_map/ppermute | solution.py:450
  28.3 24.7 %collective-permute-start.8 = (bf16[4,544,128]{2,1,0:T(8,128)(2,1)S(1)}, bf16[4,544,128]{2,1,0:T(8,128)(2,1)}, u32[]{:S(2)}, u32[]{:S(2)}) collective-permute-start(bf16[4,544,128]{2,1,0:T(8,128)(2,1)S(1)} %pad_maximum_fusion.rest_0_), channel_id=1, source_target_pairs={{0,8},{8,16},{16,24},{24,0},{1,9},{9,17},{17,25},{25,1},{2,10},{10... | collective-permute-start | bytes 1671176 | tf_op jit(solution)/shard_map/ppermute | solution.py:450
  28.3 24.7 %collective-permute-start.9 = (bf16[4,544,128]{2,1,0:T(8,128)(2,1)S(1)}, bf16[4,544,128]{2,1,0:T(8,128)(2,1)}, u32[]{:S(2)}, u32[]{:S(2)}) collective-permute-start(bf16[4,544,128]{2,1,0:T(8,128)(2,1)S(1)} %pad_maximum_fusion.rest_0_), channel_id=1, source_target_pairs={{0,16},{8,24},{16,0},{24,8},{1,17},{9,25},{17,1},{25,9},{2,18},{10... | collective-permute-start | bytes 1671176 | tf_op jit(solution)/shard_map/ppermute | solution.py:450
  30.1 2.0 %collective-permute-start.10 = (bf16[4,544,128]{2,1,0:T(8,128)(2,1)S(1)}, bf16[4,544,128]{2,1,0:T(8,128)(2,1)S(1)}, u32[]{:S(2)}, u32[]{:S(2)}) collective-permute-start(bf16[4,544,128]{2,1,0:T(8,128)(2,1)S(1)} %pad_maximum_fusion.rest_0_), channel_id=1, source_target_pairs={{0,1},{1,0},{2,3},{3,2},{4,5},{5,4},{6,7},{7,6},{8,9},{9,8},{10,11... | collective-permute-start | bytes 1671176 | tf_op jit(solution)/shard_map/ppermute | solution.py:454
  31.3 22.4 %copy-start.19 = (bf16[256]{0:T(256)(128)(2,1)S(1)}, bf16[256]{0:T(256)(128)(2,1)}, u32[]{:S(2)}) copy-start(bf16[256]{0:T(256)(128)(2,1)} %param.18) | copy-start | bytes 1540
  31.3 22.4 %copy-start.9 = (bf16[128,2048]{1,0:T(8,128)(2,1)S(1)}, bf16[128,2048]{1,0:T(8,128)(2,1)}, u32[]{:S(2)}) copy-start(bf16[128,2048]{1,0:T(8,128)(2,1)} %param.17) | copy-start | bytes 1572868
  32.1 0.8 copy-start.12
  53.0 8.5 %collective-permute-start.11 = (bf16[4,544,128]{2,1,0:T(8,128)(2,1)}, bf16[4,544,128]{2,1,0:T(8,128)(2,1)}, u32[]{:S(2)}, u32[]{:S(2)}) collective-permute-start(bf16[4,544,128]{2,1,0:T(8,128)(2,1)} %collective-permute-done.7.rest_0_), channel_id=1, source_target_pairs={{0,1},{1,0},{2,3},{3,2},{4,5},{5,4},{6,7},{7,6},{8,9},{9,8},{10,11... | collective-permute-start | bytes 1671176 | tf_op jit(solution)/shard_map/ppermute | solution.py:454
  53.1 11.3 %collective-permute-start.12 = (bf16[4,544,128]{2,1,0:T(8,128)(2,1)}, bf16[4,544,128]{2,1,0:T(8,128)(2,1)}, u32[]{:S(2)}, u32[]{:S(2)}) collective-permute-start(bf16[4,544,128]{2,1,0:T(8,128)(2,1)} %collective-permute-done.8.rest_2_), channel_id=1, source_target_pairs={{0,1},{1,0},{2,3},{3,2},{4,5},{5,4},{6,7},{7,6},{8,9},{9,8},{10,11... | collective-permute-start | bytes 1671176 | tf_op jit(solution)/shard_map/ppermute | solution.py:454
  53.6 10.8 %collective-permute-start.13 = (bf16[4,544,128]{2,1,0:T(8,128)(2,1)}, bf16[4,544,128]{2,1,0:T(8,128)(2,1)}, u32[]{:S(2)}, u32[]{:S(2)}) collective-permute-start(bf16[4,544,128]{2,1,0:T(8,128)(2,1)} %collective-permute-done.9.rest_4_), channel_id=1, source_target_pairs={{0,1},{1,0},{2,3},{3,2},{4,5},{5,4},{6,7},{7,6},{8,9},{9,8},{10,11... | collective-permute-start | bytes 1671176 | tf_op jit(solution)/shard_map/ppermute | solution.py:454
  53.7 36.1 %copy-start.1 = (bf16[136,2048]{1,0:T(8,128)(2,1)}, bf16[136,2048]{1,0:T(8,128)(2,1)S(1)}, u32[]{:S(2)}) copy-start(bf16[136,2048]{1,0:T(8,128)(2,1)S(1)} %fusion.1.rest_0_) | copy-start | bytes 1671172
  53.8 25.2 %collective-permute-start = (bf16[136,2048]{1,0:T(8,128)(2,1)S(1)}, bf16[136,2048]{1,0:T(8,128)(2,1)S(1)}, u32[]{:S(2)}, u32[]{:S(2)}) collective-permute-start(bf16[136,2048]{1,0:T(8,128)(2,1)S(1)} %fusion.1.rest_0_), channel_id=1, source_target_pairs={{0,6},{2,0},{4,2},{6,4},{1,7},{3,1},{5,3},{7,5},{8,14},{10,8},{12,... | collective-permute-start | bytes 1671176 | tf_op jit(solution)/shard_map/ppermute | solution.py:450
  56.3 22.7 %collective-permute-start.1 = (bf16[136,2048]{1,0:T(8,128)(2,1)S(1)}, bf16[136,2048]{1,0:T(8,128)(2,1)S(1)}, u32[]{:S(2)}, u32[]{:S(2)}) collective-permute-start(bf16[136,2048]{1,0:T(8,128)(2,1)S(1)} %fusion.1.rest_0_), channel_id=1, source_target_pairs={{0,2},{2,4},{4,6},{6,0},{1,3},{3,5},{5,7},{7,1},{8,10},{10,12},{12... | collective-permute-start | bytes 1671176 | tf_op jit(solution)/shard_map/ppermute | solution.py:450
  56.3 33.5 %all-to-all-start = ((bf16[8,128,256]{2,1,0:T(8,128)(2,1)}), bf16[8,128,256]{2,1,0:T(8,128)(2,1)S(1)}, u32[]{:S(2)}, u32[]{:S(2)}) async-start(bf16[8,128,256]{2,1,0:T(8,128)(2,1)} %bitcast.7), calls=%async_computation | async-start | bytes 1048576 | tf_op jit(solution)/shard_map/all_to_all | solution.py:510
  61.5 26.2 %collective-permute-start.2 = (bf16[136,2048]{1,0:T(8,128)(2,1)S(1)}, bf16[136,2048]{1,0:T(8,128)(2,1)}, u32[]{:S(2)}, u32[]{:S(2)}) collective-permute-start(bf16[136,2048]{1,0:T(8,128)(2,1)S(1)} %fusion.1.rest_0_), channel_id=1, source_target_pairs={{0,4},{2,6},{4,0},{6,2},{1,5},{3,7},{5,1},{7,3},{8,12},{10,14},{12... | collective-permute-start | bytes 1671176 | tf_op jit(solution)/shard_map/ppermute | solution.py:450
  79.0 23.5 %copy-start.3 = (bf16[136,2048]{1,0:T(8,128)(2,1)}, bf16[136,2048]{1,0:T(8,128)(2,1)S(1)}, u32[]{:S(2)}) copy-start(bf16[136,2048]{1,0:T(8,128)(2,1)S(1)} %collective-permute-done.rest_2_) | copy-start | bytes 1671172
  79.0 23.4 %copy-start.4 = (bf16[136,2048]{1,0:T(8,128)(2,1)}, bf16[136,2048]{1,0:T(8,128)(2,1)S(1)}, u32[]{:S(2)}) copy-start(bf16[136,2048]{1,0:T(8,128)(2,1)S(1)} %collective-permute-done.1.rest_4_) | copy-start | bytes 1671172
  89.8 12.6 %collective-permute-start.14 = (bf16[136,2048]{1,0:T(8,128)(2,1)S(1)}, bf16[136,2048]{1,0:T(8,128)(2,1)S(1)}, u32[]{:S(2)}, u32[]{:S(2)}) collective-permute-start(bf16[136,2048]{1,0:T(8,128)(2,1)S(1)} %fusion.1.rest_0_), channel_id=1, source_target_pairs={{0,1},{1,0},{2,3},{3,2},{4,5},{5,4},{6,7},{7,6},{8,9},{9,8},{10,11... | collective-permute-start | bytes 1671176 | tf_op jit(solution)/shard_map/ppermute | solution.py:454
  89.8 12.6 %collective-permute-start.15 = (bf16[136,2048]{1,0:T(8,128)(2,1)S(1)}, bf16[136,2048]{1,0:T(8,128)(2,1)S(1)}, u32[]{:S(2)}, u32[]{:S(2)}) collective-permute-start(bf16[136,2048]{1,0:T(8,128)(2,1)S(1)} %collective-permute-done.rest_2_), channel_id=1, source_target_pairs={{0,1},{1,0},{2,3},{3,2},{4,5},{5,4},{6,7},{7,6},{8,9},{9,8},{10,11... | collective-permute-start | bytes 1671176 | tf_op jit(solution)/shard_map/ppermute | solution.py:454
  90.3 12.1 %collective-permute-start.16 = (bf16[136,2048]{1,0:T(8,128)(2,1)S(1)}, bf16[136,2048]{1,0:T(8,128)(2,1)S(1)}, u32[]{:S(2)}, u32[]{:S(2)}) collective-permute-start(bf16[136,2048]{1,0:T(8,128)(2,1)S(1)} %collective-permute-done.1.rest_4_), channel_id=1, source_target_pairs={{0,1},{1,0},{2,3},{3,2},{4,5},{5,4},{6,7},{7,6},{8,9},{9,8},{10,11... | collective-permute-start | bytes 1671176 | tf_op jit(solution)/shard_map/ppermute | solution.py:454
  90.3 12.1 %collective-permute-start.17 = (bf16[136,2048]{1,0:T(8,128)(2,1)}, bf16[136,2048]{1,0:T(8,128)(2,1)S(1)}, u32[]{:S(2)}, u32[]{:S(2)}) collective-permute-start(bf16[136,2048]{1,0:T(8,128)(2,1)} %collective-permute-done.2.rest_6_), channel_id=1, source_target_pairs={{0,1},{1,0},{2,3},{3,2},{4,5},{5,4},{6,7},{7,6},{8,9},{9,8},{10,11... | collective-permute-start | bytes 1671176 | tf_op jit(solution)/shard_map/ppermute | solution.py:454
  102.4 0.8 copy-start.5
  102.4 1.0 copy-start.6
  102.4 1.2 copy-start.7
  103.6 0.8 copy-start.8
  108.2 30.7 %copy-start = (bf16[128,2048]{1,0:T(8,128)(2,1)}, bf16[128,2048]{1,0:T(8,128)(2,1)S(1)}, u32[]{:S(2)}) copy-start(bf16[128,2048]{1,0:T(8,128)(2,1)S(1)} %get-tuple-element.66.rest_0_) | copy-start | bytes 1572868
  108.2 12.1 %collective-permute-start.19 = (bf16[128,2048]{1,0:T(8,128)(2,1)S(1)}, bf16[128,2048]{1,0:T(8,128)(2,1)S(1)}, u32[]{:S(2)}, u32[]{:S(2)}) collective-permute-start(bf16[128,2048]{1,0:T(8,128)(2,1)S(1)} %get-tuple-element.66.rest_0_), channel_id=1, source_target_pairs={{0,6},{2,0},{4,2},{6,4},{1,7},{3,1},{5,3},{7,5},{8,14},{10,8},{12,... | collective-permute-start | bytes 1572872 | tf_op jit(solution)/shard_map/ppermute | solution.py:450
  109.7 15.1 %collective-permute-start.21 = (bf16[128,2048]{1,0:T(8,128)(2,1)S(1)}, bf16[128,2048]{1,0:T(8,128)(2,1)S(1)}, u32[]{:S(2)}, u32[]{:S(2)}) collective-permute-start(bf16[128,2048]{1,0:T(8,128)(2,1)S(1)} %get-tuple-element.66.rest_0_), channel_id=1, source_target_pairs={{0,2},{2,4},{4,6},{6,0},{1,3},{3,5},{5,7},{7,1},{8,10},{10,12},{12... | collective-permute-start | bytes 1572872 | tf_op jit(solution)/shard_map/ppermute | solution.py:450
  109.8 26.8 %collective-permute-start.23 = (bf16[128,2048]{1,0:T(8,128)(2,1)S(1)}, bf16[128,2048]{1,0:T(8,128)(2,1)S(1)}, u32[]{:S(2)}, u32[]{:S(2)}) collective-permute-start(bf16[128,2048]{1,0:T(8,128)(2,1)S(1)} %get-tuple-element.66.rest_0_), channel_id=1, source_target_pairs={{0,4},{2,6},{4,0},{6,2},{1,5},{3,7},{5,1},{7,3},{8,12},{10,14},{12... | collective-permute-start | bytes 1572872 | tf_op jit(solution)/shard_map/ppermute | solution.py:450
  111.2 25.4 %collective-permute-start.18 = (bf16[128,2048]{1,0:T(8,128)(2,1)S(1)}, bf16[128,2048]{1,0:T(8,128)(2,1)S(1)}, u32[]{:S(2)}, u32[]{:S(2)}) collective-permute-start(bf16[128,2048]{1,0:T(8,128)(2,1)S(1)} %get-tuple-element.66.rest_0_), channel_id=1, source_target_pairs={{0,1},{1,0},{2,3},{3,2},{4,5},{5,4},{6,7},{7,6},{8,9},{9,8},{10,11... | collective-permute-start | bytes 1572872 | tf_op jit(solution)/shard_map/ppermute | solution.py:454
  120.3 18.6 %copy-start.13 = (bf16[128,2048]{1,0:T(8,128)(2,1)}, bf16[128,2048]{1,0:T(8,128)(2,1)S(1)}, u32[]{:S(2)}) copy-start(bf16[128,2048]{1,0:T(8,128)(2,1)S(1)} %collective-permute-done.19.rest_2_) | copy-start | bytes 1572868
  120.3 16.3 %collective-permute-start.20 = (bf16[128,2048]{1,0:T(8,128)(2,1)S(1)}, bf16[128,2048]{1,0:T(8,128)(2,1)S(1)}, u32[]{:S(2)}, u32[]{:S(2)}) collective-permute-start(bf16[128,2048]{1,0:T(8,128)(2,1)S(1)} %collective-permute-done.19.rest_2_), channel_id=1, source_target_pairs={{0,1},{1,0},{2,3},{3,2},{4,5},{5,4},{6,7},{7,6},{8,9},{9,8},{10,11... | collective-permute-start | bytes 1572872 | tf_op jit(solution)/shard_map/ppermute | solution.py:454
  124.8 14.1 %copy-start.14 = (bf16[128,2048]{1,0:T(8,128)(2,1)}, bf16[128,2048]{1,0:T(8,128)(2,1)S(1)}, u32[]{:S(2)}) copy-start(bf16[128,2048]{1,0:T(8,128)(2,1)S(1)} %collective-permute-done.21.rest_4_) | copy-start | bytes 1572868
  124.8 13.2 %collective-permute-start.22 = (bf16[128,2048]{1,0:T(8,128)(2,1)S(1)}, bf16[128,2048]{1,0:T(8,128)(2,1)S(1)}, u32[]{:S(2)}, u32[]{:S(2)}) collective-permute-start(bf16[128,2048]{1,0:T(8,128)(2,1)S(1)} %collective-permute-done.21.rest_4_), channel_id=1, source_target_pairs={{0,1},{1,0},{2,3},{3,2},{4,5},{5,4},{6,7},{7,6},{8,9},{9,8},{10,11... | collective-permute-start | bytes 1572872 | tf_op jit(solution)/shard_map/ppermute | solution.py:454
  136.5 2.4 %copy-start.15 = (bf16[128,2048]{1,0:T(8,128)(2,1)}, bf16[128,2048]{1,0:T(8,128)(2,1)S(1)}, u32[]{:S(2)}) copy-start(bf16[128,2048]{1,0:T(8,128)(2,1)S(1)} %collective-permute-done.23.rest_6_) | copy-start | bytes 1572868
  136.5 2.4 %collective-permute-start.24 = (bf16[128,2048]{1,0:T(8,128)(2,1)S(1)}, bf16[128,2048]{1,0:T(8,128)(2,1)}, u32[]{:S(2)}, u32[]{:S(2)}) collective-permute-start(bf16[128,2048]{1,0:T(8,128)(2,1)S(1)} %collective-permute-done.23.rest_6_), channel_id=1, source_target_pairs={{0,1},{1,0},{2,3},{3,2},{4,5},{5,4},{6,7},{7,6},{8,9},{9,8},{10,11... | collective-permute-start | bytes 1572872 | tf_op jit(solution)/shard_map/ppermute | solution.py:454
  136.6 2.3 %copy-start.16 = (bf16[128,2048]{1,0:T(8,128)(2,1)}, bf16[128,2048]{1,0:T(8,128)(2,1)S(1)}, u32[]{:S(2)}) copy-start(bf16[128,2048]{1,0:T(8,128)(2,1)S(1)} %collective-permute-done.18.rest_1_) | copy-start | bytes 1572868
  136.6 2.3 %copy-start.17 = (bf16[128,2048]{1,0:T(8,128)(2,1)}, bf16[128,2048]{1,0:T(8,128)(2,1)S(1)}, u32[]{:S(2)}) copy-start(bf16[128,2048]{1,0:T(8,128)(2,1)S(1)} %collective-permute-done.20.rest_3_) | copy-start | bytes 1572868
  138.1 0.8 copy-start.18
  150.7 8.7 %collective-permute-start.26 = (bf16[1024,256]{1,0:T(8,128)(2,1)S(1)}, bf16[1024,256]{1,0:T(8,128)(2,1)S(1)}, u32[]{:S(2)}, u32[]{:S(2)}) collective-permute-start(bf16[1024,256]{1,0:T(8,128)(2,1)S(1)} %get-tuple-element.72), channel_id=1, source_target_pairs={{0,1},{1,0},{2,3},{3,2},{4,5},{5,4},{6,7},{7,6},{8,9},{9,8},{10,11... | collective-permute-start | bytes 1572872 | tf_op jit(solution)/shard_map/ppermute | solution.py:454
  155.5 4.1 %collective-permute-start.28 = (bf16[1024,256]{1,0:T(8,128)(2,1)S(1)}, bf16[1024,256]{1,0:T(8,128)(2,1)S(1)}, u32[]{:S(2)}, u32[]{:S(2)}) collective-permute-start(bf16[1024,256]{1,0:T(8,128)(2,1)S(1)} %get-tuple-element.74), channel_id=1, source_target_pairs={{0,1},{1,0},{2,3},{3,2},{4,5},{5,4},{6,7},{7,6},{8,9},{9,8},{10,11... | collective-permute-start | bytes 1572872 | tf_op jit(solution)/shard_map/ppermute | solution.py:454
  158.8 4.0 %collective-permute-start.25 = (bf16[1024,256]{1,0:T(8,128)(2,1)S(1)}, bf16[1024,256]{1,0:T(8,128)(2,1)S(1)}, u32[]{:S(2)}, u32[]{:S(2)}) collective-permute-start(bf16[1024,256]{1,0:T(8,128)(2,1)S(1)} %get-tuple-element.70), channel_id=1, source_target_pairs={{0,1},{1,0},{2,3},{3,2},{4,5},{5,4},{6,7},{7,6},{8,9},{9,8},{10,11... | collective-permute-start | bytes 1572872 | tf_op jit(solution)/shard_map/ppermute | solution.py:454
  159.3 2.3 %collective-permute-start.30 = (bf16[1024,256]{1,0:T(8,128)(2,1)S(1)}, bf16[1024,256]{1,0:T(8,128)(2,1)S(1)}, u32[]{:S(2)}, u32[]{:S(2)}) collective-permute-start(bf16[1024,256]{1,0:T(8,128)(2,1)S(1)} %get-tuple-element.76), channel_id=1, source_target_pairs={{0,1},{1,0},{2,3},{3,2},{4,5},{5,4},{6,7},{7,6},{8,9},{9,8},{10,11... | collective-permute-start | bytes 1572872 | tf_op jit(solution)/shard_map/ppermute | solution.py:454
  159.5 14.7 %collective-permute-start.27 = (bf16[1024,256]{1,0:T(8,128)(2,1)S(1)}, bf16[1024,256]{1,0:T(8,128)(2,1)S(1)}, u32[]{:S(2)}, u32[]{:S(2)}) collective-permute-start(bf16[1024,256]{1,0:T(8,128)(2,1)S(1)} %add_convert_fusion.3), channel_id=1, source_target_pairs={{0,4},{2,6},{4,0},{6,2},{1,5},{3,7},{5,1},{7,3},{8,12},{10,14},{12... | collective-permute-start | bytes 1572872 | tf_op jit(solution)/shard_map/ppermute | solution.py:450
  159.8 26.3 %collective-permute-start.29 = (bf16[1024,256]{1,0:T(8,128)(2,1)S(1)}, bf16[1024,256]{1,0:T(8,128)(2,1)S(1)}, u32[]{:S(2)}, u32[]{:S(2)}) collective-permute-start(bf16[1024,256]{1,0:T(8,128)(2,1)S(1)} %add_convert_fusion.2), channel_id=1, source_target_pairs={{0,2},{2,4},{4,6},{6,0},{1,3},{3,5},{5,7},{7,1},{8,10},{10,12},{12... | collective-permute-start | bytes 1572872 | tf_op jit(solution)/shard_map/ppermute | solution.py:450
  161.7 24.4 %collective-permute-start.31 = (bf16[1024,256]{1,0:T(8,128)(2,1)S(1)}, bf16[1024,256]{1,0:T(8,128)(2,1)S(1)}, u32[]{:S(2)}, u32[]{:S(2)}) collective-permute-start(bf16[1024,256]{1,0:T(8,128)(2,1)S(1)} %add_convert_fusion.1), channel_id=1, source_target_pairs={{0,6},{2,0},{4,2},{6,4},{1,7},{3,1},{5,3},{7,5},{8,14},{10,8},{12,... | collective-permute-start | bytes 1572872 | tf_op jit(solution)/shard_map/ppermute | solution.py:450
Sparse Core Ops, SparseCore 0:
  53.1 71.7 all-gather.1

commit v4 on v3

--- a/solution.py
+++ b/solution.py
@@ -357,12 +357,16 @@
 
 
 def up_kernel(sc, gain_ref, w_in, *rest):
-    mids, (h_ref, own_ref, w_up, mid_all, normed, sems) = rest[:8], rest[8:]
+    mids, (h_ref, own_ref, other_ref, mine_ref, w_up, mid_all, normed, w_down, sems) = rest[:8], rest[8:]
     fetches = [pltpu.make_async_copy(mids[n], mid_all.at[pl.ds(128 * n, 128)], sems.at[16 + n]) for n in range(8)]
     copies = [
         pltpu.make_async_copy(w_in.at[pl.ds(256 * n, 128)], w_up.at[pl.ds(128 * n, 128)], sems.at[n]) for n in range(16)
     ]
-    for copy in fetches + copies:
+    far = []
+    for k in range(4):
+        at = pl.multiple_of((sc[36 + 2] + k) * 256 + 128, 128)
+        far.append(pltpu.make_async_copy(w_in.at[pl.ds(at, 128)], w_down.at[pl.ds(128 * k, 128)], sems.at[24 + k]))
+    for copy in fetches + copies + far:
         copy.start()
     gain = gain_ref[0:1, :].astype(jnp.float32)
     lanes = pl.ds(pl.multiple_of(sc[34], 256), 256)
@@ -379,6 +383,12 @@
         h = jnp.square(jnp.maximum(h, 0.0)).astype(jnp.bfloat16)
         for k in range(2):
             h_ref[pl.ds(pl.multiple_of(sc[26 + n + k], 128), 128), :] = h[128 * k : 128 * (k + 1)]
+    for copy in far:
+        copy.wait()
+    for which, out_ref in ((1 - sc[35], other_ref), (sc[35], mine_ref)):
+        rows = w_down[pl.ds(pl.multiple_of(which * 256, 256), 256), :]
+        product = lax.dot_general(h_ref[...], rows, (((1,), (1,)), ((), ())), preferred_element_type=jnp.float32)
+        out_ref[...] = product.astype(out_ref.dtype)
 
 
 def up(scalars, gain, w, mids):
@@ -388,17 +398,20 @@
         out_shape=[
             jax.ShapeDtypeStruct((1024, 1024), jnp.bfloat16),
             jax.ShapeDtypeStruct((1024, 256), jnp.bfloat16),
+            jax.ShapeDtypeStruct((1024, 256), jnp.bfloat16),
+            jax.ShapeDtypeStruct((1024, 256), jnp.bfloat16),
         ],
         in_specs=[pl.BlockSpec(memory_space=pltpu.SMEM), vmem] + [pl.BlockSpec(memory_space=pltpu.HBM)] * 9,
-        out_specs=[vmem, vmem],
+        out_specs=[vmem] * 4,
         scratch_shapes=[
             pltpu.VMEM((D, 1024), jnp.bfloat16),
             pltpu.VMEM((1024, D), jnp.bfloat16),
             pltpu.VMEM((1024, D), jnp.bfloat16),
-            pltpu.SemaphoreType.DMA((24,)),
+            pltpu.VMEM((512, 1024), jnp.bfloat16),
+            pltpu.SemaphoreType.DMA((28,)),
         ],
         compiler_params=pltpu.CompilerParams(vmem_limit_bytes=40 * 1024 * 1024),
-        cost_estimate=pl.CostEstimate(flops=4_300_000_000, bytes_accessed=8_000_000, transcendentals=0),
+        cost_estimate=pl.CostEstimate(flops=5_400_000_000, bytes_accessed=8_000_000, transcendentals=0),
         name="up",
     )(scalars, gain, *in_hbm([w, *mids]))
 
@@ -508,8 +521,9 @@
     kv_near = partner(kv_own)
     state = attend(table, zeros_q, qt, [kv_own, kv_near], (), True, False)
     res = lax.all_to_all(residual.reshape(8, 128, 256), ("c", "x"), 0, 0, tiled=True)
-    kv_mine[1:], state, both = lax.optimization_barrier((kv_mine[1:], state, both))
+    state, both = lax.optimization_barrier((state, both))
     both = lax.all_gather(both, ("z", "y"), axis=0, tiled=True)
+    kv_mine[1:], state = lax.optimization_barrier((kv_mine[1:], state))
     kv_other = [None] + [partner(piece) for piece in kv_mine[1:]]
     pieces = [piece for pair in zip(kv_mine[1:], kv_other[1:]) for piece in pair]
     out = attend(table, zeros_q, qt, pieces, state, False, True)
@@ -523,11 +537,14 @@
 
     mid_mine = [middle] + [shifted(middle, "x", r) for r in RING]
     mids = [m for mine in mid_mine for m in (mine, partner(mine))]
-    hidden, middle_own = up(table, gain, both, mids)
+    hidden, middle_own, *far = up(table, gain, both, mids)
 
     parts = {}
-    for steps in ((2,), (0,), (1, 3)):
-        products = down(table, hidden, both, steps)
+    for name, steps in (("far", (2,)), ("own", (0,)), ("near", (1, 3))):
+        if name == "far":
+            products = far
+        else:
+            products = down(table, hidden, both, steps)
         for n, r in enumerate(steps):
             parts[r] = products[2 * n + 1].astype(jnp.float32) + partner(products[2 * n]).astype(jnp.float32)
     total = middle_own.astype(jnp.float32) + parts[0]

time: 195 us -> 213 us (1.092)
  the two profiles are of different devices: /device:TPU:1 before, /device:TPU:25 now
where the time goes in v4:
time: 213 us; the launch traced here: 211 us
  waiting for transfers between devices  85.4 us (40%)
  Pallas kernels  49.4 us (23%)
  starting transfers between devices  44.2 us (21%)
  between operations  13.7 us (6%)
  blocking collectives  11.3 us (5%)
  local copies, waits for them, and re-layouts  4.54 us (2%)
  other arithmetic  2.79 us (1%)
    ppermute x12, waiting for transfers between devices, shifted(): return lax.ppermute(value, axis, [(i, (i - by) % n) for i in range(n)])  76 us
    pallas_call x2, Pallas kernels, attend(): pl.pallas_call(functools.partial(attend_kernel, n_arr, first, last), out_...  26.3 us
    ppermute x12, starting transfers between devices, shifted(): return lax.ppermute(value, axis, [(i, (i - by) % n) for i in range(n)])  16 us
    ppermute x16, starting transfers between devices, partner(): return lax.ppermute(value, 'c', [(0, 1), (1, 0)])  14.5 us
    all_to_all x1, blocking collectives, body(): attended = lax.all_to_all(out, ('x', 'z'), 0, 0, tiled=True)  11.3 us
    pallas_call x1, Pallas kernels, up(): pl.pallas_call(up_kernel, out_shape=[jax.ShapeDtypeStruct((1024, 1024), j...  9.96 us
    ppermute x4, starting transfers between devices, body(): received.append(lax.ppermute(messages[step], ('z', 'c'), pairs))  9.22 us
    pallas_call x2, Pallas kernels, down(): pl.pallas_call(functools.partial(down_kernel, steps), out_shape=[jax.Shap...  7.43 us
  transfers between devices with their start and end apart: 34, of which 17 were waited for; matrix products, arithmetic and copies ran while one was open for 1% of the time, Pallas kernels for 14%

profile of v4, /device:TPU:25, one launch (start us, length us, event | category | flops | bytes accessed | tf_op | source)
XLA Modules:
  0.0 211.4 jit_solution(8290187347351665975)
XLA Ops:
  6.5 0.7 dynamic-slice_bitcast_fusion.tab.sc
  7.2 2.1 pack.1
  9.3 6.1 %collective-permute-start.3 = (bf16[800,128]{1,0:T(8,128)(2,1)S(1)}, bf16[800,128]{1,0:T(8,128)(2,1)S(1)}, u32[]{:S(2)}, u32[]{:S(2)}) collective-permute-start(bf16[800,128]{1,0:T(8,128)(2,1)S(1)} %get-tuple-element.44), channel_id=1, source_target_pairs={{0,0},{1,64},{32,32},{33,96},{64,1},{65,65},{96,33},{97,97},{2,2},... | collective-permute-start | bytes 614408 | tf_op jit(solution)/shard_map/ppermute | solution.py:505
  15.4 0.3 collective-permute-start.4
  15.6 2.9 %collective-permute-start.6 = (bf16[800,128]{1,0:T(8,128)(2,1)S(1)}, bf16[800,128]{1,0:T(8,128)(2,1)S(1)}, u32[]{:S(2)}, u32[]{:S(2)}) collective-permute-start(bf16[800,128]{1,0:T(8,128)(2,1)S(1)} %get-tuple-element.47), channel_id=1, source_target_pairs={{0,33},{1,97},{32,1},{33,65},{64,32},{65,96},{96,0},{97,64},{2,35}... | collective-permute-start | bytes 614408 | tf_op jit(solution)/shard_map/ppermute | solution.py:505
  18.5 1.9 collective-permute-done.3
  20.5 4.4 %collective-permute-done.4 = bf16[800,128]{1,0:T(8,128)(2,1)S(1)} collective-permute-done((bf16[800,128]{1,0:T(8,128)(2,1)S(1)}, bf16[800,128]{1,0:T(8,128)(2,1)S(1)}, u32[]{:S(2)}, u32[]{:S(2)}) %collective-permute-start.4) | collective-permute-done | bytes 204832 | tf_op jit(solution)/shard_map/ppermute | solution.py:505
  25.0 0.1 copy.12
  25.2 2.8 %collective-permute-start.10 = (bf16[4,544,128]{2,1,0:T(8,128)(2,1)S(1)}, bf16[4,544,128]{2,1,0:T(8,128)(2,1)S(1)}, u32[]{:S(2)}, u32[]{:S(2)}) collective-permute-start(bf16[4,544,128]{2,1,0:T(8,128)(2,1)S(1)} %pad_maximum_fusion.rest_0_), channel_id=1, source_target_pairs={{0,1},{1,0},{2,3},{3,2},{4,5},{5,4},{6,7},{7,6},{8,9},{9,8},{10,11... | collective-permute-start | bytes 1671176 | tf_op jit(solution)/shard_map/ppermute | solution.py:467
  28.0 0.1 convert_reduce_fusion
  28.2 0.8 pad_maximum_fusion.1
  29.0 0.5 collective-permute-done.10.rest_1_
  29.6 0.8 copy-done.12
  30.4 8.4 %attend_first.1 = (f32[4,1,512]{2,1,0:T(1,128)S(1)}, f32[4,1,512]{2,1,0:T(1,128)S(1)}, f32[4,64,512]{2,1,0:T(8,128)S(1)}) custom-call(s32[44]{0:T(128)S(1)} %dynamic-slice_bitcast_fusion.tab.sc, s32[4]{0:T(128)S(1)} %subtract_convert_fusion.zeros_q, bf16[4,256,128]{2,1,0:T(8,128)(2,1)S(1)} %pad_maximum_fusion.2.qt_ref, bf16[4,544,128]{2,1,0:T(8,128)(2,1)} %copy-done.2, ...), custom_call_target="tpu_custom_call" | custom-call | flops 8000000000 | bytes 2000000 | tf_op jit(solution)/shard_map/attend_first/pallas_call | solution.py:301
  38.8 1.4 collective-permute-start.9
  40.2 1.5 collective-permute-start.8
  41.7 16.9 %collective-permute-done.9.rest_4_ = bf16[4,544,128]{2,1,0:T(8,128)(2,1)} collective-permute-done((bf16[4,544,128]{2,1,0:T(8,128)(2,1)}, bf16[4,544,128]{2,1,0:T(8,128)(2,1)}, u32[]{:S(2)}, u32[]{:S(2)}) %collective-permute-start.9) | collective-permute-done | bytes 557088 | tf_op jit(solution)/shard_map/ppermute | solution.py:463
  58.6 14.7 %collective-permute-done.8.rest_2_ = bf16[4,544,128]{2,1,0:T(8,128)(2,1)} collective-permute-done((bf16[4,544,128]{2,1,0:T(8,128)(2,1)}, bf16[4,544,128]{2,1,0:T(8,128)(2,1)}, u32[]{:S(2)}, u32[]{:S(2)}) %collective-permute-start.8) | collective-permute-done | bytes 557088 | tf_op jit(solution)/shard_map/ppermute | solution.py:463
  73.3 1.8 collective-permute-done.7.rest_0_
  75.2 0.4 collective-permute-start.11
  75.6 0.1 collective-permute-start.12
  75.7 0.4 collective-permute-start.13
  76.2 2.8 %collective-permute-start.2 = (bf16[136,2048]{1,0:T(8,128)(2,1)S(1)}, bf16[136,2048]{1,0:T(8,128)(2,1)S(1)}, u32[]{:S(2)}, u32[]{:S(2)}) collective-permute-start(bf16[136,2048]{1,0:T(8,128)(2,1)S(1)} %fusion.1.rest_0_), channel_id=1, source_target_pairs={{0,4},{2,6},{4,0},{6,2},{1,5},{3,7},{5,1},{7,3},{8,12},{10,14},{12... | collective-permute-start | bytes 1671176 | tf_op jit(solution)/shard_map/ppermute | solution.py:463
  79.0 0.3 collective-permute-start.1
  79.3 4.6 %all-to-all-start = ((bf16[8,128,256]{2,1,0:T(8,128)(2,1)}), bf16[8,128,256]{2,1,0:T(8,128)(2,1)S(1)}, u32[]{:S(2)}, u32[]{:S(2)}) async-start(bf16[8,128,256]{2,1,0:T(8,128)(2,1)} %bitcast.7), calls=%async_computation | async-start | bytes 1048576 | tf_op jit(solution)/shard_map/all_to_all | solution.py:523
  83.9 2.6 %collective-permute-start = (bf16[136,2048]{1,0:T(8,128)(2,1)S(1)}, bf16[136,2048]{1,0:T(8,128)(2,1)}, u32[]{:S(2)}, u32[]{:S(2)}) collective-permute-start(bf16[136,2048]{1,0:T(8,128)(2,1)S(1)} %fusion.1.rest_0_), channel_id=1, source_target_pairs={{0,6},{2,0},{4,2},{6,4},{1,7},{3,1},{5,3},{7,5},{8,14},{10,8},{12,... | collective-permute-start | bytes 1671176 | tf_op jit(solution)/shard_map/ppermute | solution.py:463
  86.5 17.9 %attend_last.1 = bf16[16,64,128]{2,1,0:T(8,128)(2,1)S(1)} custom-call(s32[44]{0:T(128)S(1)} %dynamic-slice_bitcast_fusion.tab.sc, s32[4]{0:T(128)S(1)} %subtract_convert_fusion.zeros_q, bf16[4,256,128]{2,1,0:T(8,128)(2,1)S(1)} %pad_maximum_fusion.2.qt_ref, bf16[4,544,128]{2,1,0:T(8,128)(2,1)} %collective-permute-done.7.rest_0_, ...), custom_call_target="tpu_custom_call" | custom-call | flops 24000000000 | bytes 6000000 | tf_op jit(solution)/shard_map/attend_last/pallas_call | solution.py:301
  104.4 0.4 collective-permute-done.1.rest_4_
  104.8 4.9 %collective-permute-done.rest_2_ = bf16[136,2048]{1,0:T(8,128)(2,1)} collective-permute-done((bf16[136,2048]{1,0:T(8,128)(2,1)S(1)}, bf16[136,2048]{1,0:T(8,128)(2,1)}, u32[]{:S(2)}, u32[]{:S(2)}) %collective-permute-start) | collective-permute-done | bytes 557088 | tf_op jit(solution)/shard_map/ppermute | solution.py:463
  109.7 0.4 all-to-all-done.res_ref
  110.1 0.6 collective-permute-start.14
  110.7 0.4 collective-permute-start.16
  111.2 11.3 %all_to_all.10.att_ref = bf16[16,64,128]{2,1,0:T(8,128)(2,1)S(1)} all-to-all(bf16[16,64,128]{2,1,0:T(8,128)(2,1)S(1)} %attend_last.1), channel_id=1, replica_groups=mesh['z'=4,'y'=4,'x'=4,'c'=2] {'x','z'}, dimensions={0} | all-to-all | bytes 524288 | tf_op jit(solution)/shard_map/all_to_all | solution.py:534
  122.6 0.8 copy-done.5
  123.3 0.2 copy-done.6
  123.5 0.2 copy-done.7
  123.7 0.8 copy-done.8
  124.6 3.6 %dense.1 = (bf16[128,2048]{1,0:T(8,128)(2,1)S(1)}, bf16[8,2048]{1,0:T(8,128)(2,1)S(1)}) custom-call(s32[44]{0:T(128)S(1)} %dynamic-slice_bitcast_fusion.tab.sc, bf16[16,64,128]{2,1,0:T(8,128)(2,1)S(1)} %all_to_all.10.att_ref, bf16[8,128,256]{2,1,0:T(8,128)(2,1)S(1)} %all-to-all-done.res_ref, bf16[136,2048]{1,0:T(8,128)(2,1)} %copy-done.1, ...), custom_call_target="tpu_custom_call" | custom-call | flops 1000000000 | bytes 4000000 | tf_op jit(solution)/shard_map/dense/pallas_call | solution.py:344
  128.2 1.2 collective-permute-start.23
  129.4 0.6 collective-permute-start.21
  130.0 2.1 collective-permute-start.19
  132.1 2.6 %collective-permute-start.18 = (bf16[128,2048]{1,0:T(8,128)(2,1)S(1)}, bf16[128,2048]{1,0:T(8,128)(2,1)S(1)}, u32[]{:S(2)}, u32[]{:S(2)}) collective-permute-start(bf16[128,2048]{1,0:T(8,128)(2,1)S(1)} %get-tuple-element.72.rest_0_), channel_id=1, source_target_pairs={{0,1},{1,0},{2,3},{3,2},{4,5},{5,4},{6,7},{7,6},{8,9},{9,8},{10,11... | collective-permute-start | bytes 1572872 | tf_op jit(solution)/shard_map/ppermute | solution.py:467
  134.7 6.7 %collective-permute-done.23.rest_6_ = bf16[128,2048]{1,0:T(8,128)(2,1)S(1)} collective-permute-done((bf16[128,2048]{1,0:T(8,128)(2,1)S(1)}, bf16[128,2048]{1,0:T(8,128)(2,1)S(1)}, u32[]{:S(2)}, u32[]{:S(2)}) %collective-permute-start.23) | collective-permute-done | bytes 524320 | tf_op jit(solution)/shard_map/ppermute | solution.py:463
  141.4 5.1 %collective-permute-start.24 = (bf16[128,2048]{1,0:T(8,128)(2,1)S(1)}, bf16[128,2048]{1,0:T(8,128)(2,1)S(1)}, u32[]{:S(2)}, u32[]{:S(2)}) collective-permute-start(bf16[128,2048]{1,0:T(8,128)(2,1)S(1)} %collective-permute-done.23.rest_6_), channel_id=1, source_target_pairs={{0,1},{1,0},{2,3},{3,2},{4,5},{5,4},{6,7},{7,6},{8,9},{9,8},{10,11... | collective-permute-start | bytes 1572872 | tf_op jit(solution)/shard_map/ppermute | solution.py:467
  146.5 8.3 %collective-permute-done.21.rest_4_ = bf16[128,2048]{1,0:T(8,128)(2,1)S(1)} collective-permute-done((bf16[128,2048]{1,0:T(8,128)(2,1)S(1)}, bf16[128,2048]{1,0:T(8,128)(2,1)S(1)}, u32[]{:S(2)}, u32[]{:S(2)}) %collective-permute-start.21) | collective-permute-done | bytes 524320 | tf_op jit(solution)/shard_map/ppermute | solution.py:463
  154.9 0.5 collective-permute-start.22
  155.5 1.4 collective-permute-done.22.rest_5_
  156.9 0.8 copy-done.18
  157.8 10.0 %up.1 = (bf16[1024,1024]{1,0:T(8,128)(2,1)S(1)}, bf16[1024,256]{1,0:T(8,128)(2,1)S(1)}, bf16[1024,256]{1,0:T(8,128)(2,1)S(1)}, bf16[1024,256]{1,0:T(8,128)(2,1)S(1)}) custom-call(s32[44]{0:T(128)S(1)} %dynamic-slice_bitcast_fusion.tab.sc, bf16[8,2048]{1,0:T(8,128)(2,1)S(1)} %get-tuple-element.70.gain_ref, ...), custom_call_target="tpu_custom_call" | custom-call | flops 5400000000 | bytes 8000000 | tf_op jit(solution)/shard_map/up/pallas_call | solution.py:396
  167.8 0.5 collective-permute-start.26
  168.2 4.4 %down.3 = (bf16[1024,256]{1,0:T(8,128)(2,1)S(1)}, bf16[1024,256]{1,0:T(8,128)(2,1)S(1)}, bf16[1024,256]{1,0:T(8,128)(2,1)S(1)}, bf16[1024,256]{1,0:T(8,128)(2,1)S(1)}) custom-call(s32[44]{0:T(128)S(1)} %dynamic-slice_bitcast_fusion.tab.sc, bf16[1024,1024]{1,0:T(8,128)(2,1)S(1)} %get-tuple-element.74.h_ref, bf16[4096,1024]{1,0:T(8,128)(2,1)} %all-gather.2.cloned.1.call-done.w_in), custom_call_target="tpu_custom_call" | custom-call | flops 2200000000 | bytes 4000000 | tf_op jit(solution)/shard_map/down/pallas_call | solution.py:447
  172.6 0.2 collective-permute-start.28
  172.8 3.1 %down.2 = (bf16[1024,256]{1,0:T(8,128)(2,1)S(1)}, bf16[1024,256]{1,0:T(8,128)(2,1)S(1)}) custom-call(s32[44]{0:T(128)S(1)} %dynamic-slice_bitcast_fusion.tab.sc, bf16[1024,1024]{1,0:T(8,128)(2,1)S(1)} %get-tuple-element.74.h_ref, bf16[4096,1024]{1,0:T(8,128)(2,1)} %all-gather.2.cloned.1.call-done.w_in), custom_call_target="tpu_custom_call" | custom-call | flops 1100000000 | bytes 4000000 | tf_op jit(solution)/shard_map/down/pallas_call | solution.py:447
  175.9 0.4 collective-permute-start.25
  176.4 0.1 collective-permute-start.30
  176.5 0.1 add_convert_fusion.3
  176.7 1.2 collective-permute-start.27
  177.9 0.1 add_convert_fusion.2
  178.1 0.6 collective-permute-done.30
  178.6 0.2 add_convert_fusion.1
  178.8 2.2 %collective-permute-start.31 = (bf16[1024,256]{1,0:T(8,128)(2,1)S(1)}, bf16[1024,256]{1,0:T(8,128)(2,1)S(1)}, u32[]{:S(2)}, u32[]{:S(2)}) collective-permute-start(bf16[1024,256]{1,0:T(8,128)(2,1)S(1)} %add_convert_fusion.1), channel_id=1, source_target_pairs={{0,6},{2,0},{4,2},{6,4},{1,7},{3,1},{5,3},{7,5},{8,14},{10,8},{12,... | collective-permute-start | bytes 1572872 | tf_op jit(solution)/shard_map/ppermute | solution.py:463
  181.0 10.4 %collective-permute-done.27 = bf16[1024,256]{1,0:T(8,128)(2,1)S(1)} collective-permute-done((bf16[1024,256]{1,0:T(8,128)(2,1)S(1)}, bf16[1024,256]{1,0:T(8,128)(2,1)S(1)}, u32[]{:S(2)}, u32[]{:S(2)}) %collective-permute-start.27) | collective-permute-done | bytes 524320 | tf_op jit(solution)/shard_map/ppermute | solution.py:463
  191.4 11.9 %collective-permute-done.29 = bf16[1024,256]{1,0:T(8,128)(2,1)S(1)} collective-permute-done((bf16[1024,256]{1,0:T(8,128)(2,1)S(1)}, bf16[1024,256]{1,0:T(8,128)(2,1)S(1)}, u32[]{:S(2)}, u32[]{:S(2)}) %collective-permute-start.29) | collective-permute-done | bytes 524320 | tf_op jit(solution)/shard_map/ppermute | solution.py:463
  203.3 1.2 add_convert_fusion
  (74 shorter events, 0.8 us)
Async XLA Ops:
  6.5 151.2 %all-gather.2.cloned.1.call-start = ((), (), s32[]{:S(2)}) async-start(), calls=%async_computation.2 | async-start | bytes 8912896 | tf_op jit(solution)/shard_map/all_gather | solution.py:525
  9.3 11.1 %collective-permute-start.3 = (bf16[800,128]{1,0:T(8,128)(2,1)S(1)}, bf16[800,128]{1,0:T(8,128)(2,1)S(1)}, u32[]{:S(2)}, u32[]{:S(2)}) collective-permute-start(bf16[800,128]{1,0:T(8,128)(2,1)S(1)} %get-tuple-element.44), channel_id=1, source_target_pairs={{0,0},{1,64},{32,32},{33,96},{64,1},{65,65},{96,33},{97,97},{2,2},... | collective-permute-start | bytes 614408 | tf_op jit(solution)/shard_map/ppermute | solution.py:505
  15.4 9.4 %collective-permute-start.4 = (bf16[800,128]{1,0:T(8,128)(2,1)S(1)}, bf16[800,128]{1,0:T(8,128)(2,1)S(1)}, u32[]{:S(2)}, u32[]{:S(2)}) collective-permute-start(bf16[800,128]{1,0:T(8,128)(2,1)S(1)} %get-tuple-element.45), channel_id=1, source_target_pairs={{0,32},{1,96},{32,0},{33,64},{64,33},{65,97},{96,1},{97,65},{2,34}... | collective-permute-start | bytes 614408 | tf_op jit(solution)/shard_map/ppermute | solution.py:505
  15.6 9.2 %collective-permute-start.5 = (bf16[800,128]{1,0:T(8,128)(2,1)S(1)}, bf16[800,128]{1,0:T(8,128)(2,1)S(1)}, u32[]{:S(2)}, u32[]{:S(2)}) collective-permute-start(bf16[800,128]{1,0:T(8,128)(2,1)S(1)} %get-tuple-element.46), channel_id=1, source_target_pairs={{0,1},{1,65},{32,33},{33,97},{64,0},{65,64},{96,32},{97,96},{2,3},... | collective-permute-start | bytes 614408 | tf_op jit(solution)/shard_map/ppermute | solution.py:505
  15.6 9.4 %copy-start.10 = (bf16[1024,128]{1,0:T(8,128)(2,1)S(1)}, bf16[1024,128]{1,0:T(8,128)(2,1)}, u32[]{:S(2)}) copy-start(bf16[1024,128]{1,0:T(8,128)(2,1)} %param.20) | copy-start | bytes 786436
  15.6 9.3 %collective-permute-start.6 = (bf16[800,128]{1,0:T(8,128)(2,1)S(1)}, bf16[800,128]{1,0:T(8,128)(2,1)S(1)}, u32[]{:S(2)}, u32[]{:S(2)}) collective-permute-start(bf16[800,128]{1,0:T(8,128)(2,1)S(1)} %get-tuple-element.47), channel_id=1, source_target_pairs={{0,33},{1,97},{32,1},{33,65},{64,32},{65,96},{96,0},{97,64},{2,35}... | collective-permute-start | bytes 614408 | tf_op jit(solution)/shard_map/ppermute | solution.py:505
  24.9 3.2 %copy-start.11 = (bf16[128,1024]{1,0:T(8,128)(2,1)S(1)}, bf16[128,1024]{1,0:T(8,128)(2,1)}, u32[]{:S(2)}) copy-start(bf16[128,1024]{1,0:T(8,128)(2,1)} %param.19) | copy-start | bytes 786436
  25.0 4.5 %copy-start.2 = (bf16[4,544,128]{2,1,0:T(8,128)(2,1)}, bf16[4,544,128]{2,1,0:T(8,128)(2,1)S(1)}, u32[]{:S(2)}) copy-start(bf16[4,544,128]{2,1,0:T(8,128)(2,1)S(1)} %pad_maximum_fusion.rest_0_) | copy-start | bytes 1671172
  25.2 4.3 %collective-permute-start.10 = (bf16[4,544,128]{2,1,0:T(8,128)(2,1)S(1)}, bf16[4,544,128]{2,1,0:T(8,128)(2,1)S(1)}, u32[]{:S(2)}, u32[]{:S(2)}) collective-permute-start(bf16[4,544,128]{2,1,0:T(8,128)(2,1)S(1)} %pad_maximum_fusion.rest_0_), channel_id=1, source_target_pairs={{0,1},{1,0},{2,3},{3,2},{4,5},{5,4},{6,7},{7,6},{8,9},{9,8},{10,11... | collective-permute-start | bytes 1671176 | tf_op jit(solution)/shard_map/ppermute | solution.py:467
  29.0 47.1 %copy-start.19 = (bf16[256]{0:T(256)(128)(2,1)S(1)}, bf16[256]{0:T(256)(128)(2,1)}, u32[]{:S(2)}) copy-start(bf16[256]{0:T(256)(128)(2,1)} %param.18) | copy-start | bytes 1540
  29.0 47.1 %copy-start.9 = (bf16[128,2048]{1,0:T(8,128)(2,1)S(1)}, bf16[128,2048]{1,0:T(8,128)(2,1)}, u32[]{:S(2)}) copy-start(bf16[128,2048]{1,0:T(8,128)(2,1)} %param.17) | copy-start | bytes 1572868
  29.5 0.8 copy-start.12
  38.8 19.8 %collective-permute-start.9 = (bf16[4,544,128]{2,1,0:T(8,128)(2,1)}, bf16[4,544,128]{2,1,0:T(8,128)(2,1)}, u32[]{:S(2)}, u32[]{:S(2)}) collective-permute-start(bf16[4,544,128]{2,1,0:T(8,128)(2,1)} %copy-done.2), channel_id=1, source_target_pairs={{0,16},{8,24},{16,0},{24,8},{1,17},{9,25},{17,1},{25,9},{2,18},{10... | collective-permute-start | bytes 1671176 | tf_op jit(solution)/shard_map/ppermute | solution.py:463
  40.2 33.1 %collective-permute-start.8 = (bf16[4,544,128]{2,1,0:T(8,128)(2,1)}, bf16[4,544,128]{2,1,0:T(8,128)(2,1)}, u32[]{:S(2)}, u32[]{:S(2)}) collective-permute-start(bf16[4,544,128]{2,1,0:T(8,128)(2,1)} %copy-done.2), channel_id=1, source_target_pairs={{0,8},{8,16},{16,24},{24,0},{1,9},{9,17},{17,25},{25,1},{2,10},{10... | collective-permute-start | bytes 1671176 | tf_op jit(solution)/shard_map/ppermute | solution.py:463
  41.7 33.5 %collective-permute-start.7 = (bf16[4,544,128]{2,1,0:T(8,128)(2,1)}, bf16[4,544,128]{2,1,0:T(8,128)(2,1)}, u32[]{:S(2)}, u32[]{:S(2)}) collective-permute-start(bf16[4,544,128]{2,1,0:T(8,128)(2,1)} %copy-done.2), channel_id=1, source_target_pairs={{0,24},{8,0},{16,8},{24,16},{1,25},{9,1},{17,9},{25,17},{2,26},{10... | collective-permute-start | bytes 1671176 | tf_op jit(solution)/shard_map/ppermute | solution.py:463
  75.2 8.7 %collective-permute-start.11 = (bf16[4,544,128]{2,1,0:T(8,128)(2,1)}, bf16[4,544,128]{2,1,0:T(8,128)(2,1)}, u32[]{:S(2)}, u32[]{:S(2)}) collective-permute-start(bf16[4,544,128]{2,1,0:T(8,128)(2,1)} %collective-permute-done.7.rest_0_), channel_id=1, source_target_pairs={{0,1},{1,0},{2,3},{3,2},{4,5},{5,4},{6,7},{7,6},{8,9},{9,8},{10,11... | collective-permute-start | bytes 1671176 | tf_op jit(solution)/shard_map/ppermute | solution.py:467
  75.6 10.9 %collective-permute-start.12 = (bf16[4,544,128]{2,1,0:T(8,128)(2,1)}, bf16[4,544,128]{2,1,0:T(8,128)(2,1)}, u32[]{:S(2)}, u32[]{:S(2)}) collective-permute-start(bf16[4,544,128]{2,1,0:T(8,128)(2,1)} %collective-permute-done.8.rest_2_), channel_id=1, source_target_pairs={{0,1},{1,0},{2,3},{3,2},{4,5},{5,4},{6,7},{7,6},{8,9},{9,8},{10,11... | collective-permute-start | bytes 1671176 | tf_op jit(solution)/shard_map/ppermute | solution.py:467
  75.7 10.8 %collective-permute-start.13 = (bf16[4,544,128]{2,1,0:T(8,128)(2,1)}, bf16[4,544,128]{2,1,0:T(8,128)(2,1)}, u32[]{:S(2)}, u32[]{:S(2)}) collective-permute-start(bf16[4,544,128]{2,1,0:T(8,128)(2,1)} %collective-permute-done.9.rest_4_), channel_id=1, source_target_pairs={{0,1},{1,0},{2,3},{3,2},{4,5},{5,4},{6,7},{7,6},{8,9},{9,8},{10,11... | collective-permute-start | bytes 1671176 | tf_op jit(solution)/shard_map/ppermute | solution.py:467
  76.2 33.9 %copy-start.1 = (bf16[136,2048]{1,0:T(8,128)(2,1)}, bf16[136,2048]{1,0:T(8,128)(2,1)S(1)}, u32[]{:S(2)}) copy-start(bf16[136,2048]{1,0:T(8,128)(2,1)S(1)} %fusion.1.rest_0_) | copy-start | bytes 1671172
  76.2 28.2 %collective-permute-start.2 = (bf16[136,2048]{1,0:T(8,128)(2,1)S(1)}, bf16[136,2048]{1,0:T(8,128)(2,1)S(1)}, u32[]{:S(2)}, u32[]{:S(2)}) collective-permute-start(bf16[136,2048]{1,0:T(8,128)(2,1)S(1)} %fusion.1.rest_0_), channel_id=1, source_target_pairs={{0,4},{2,6},{4,0},{6,2},{1,5},{3,7},{5,1},{7,3},{8,12},{10,14},{12... | collective-permute-start | bytes 1671176 | tf_op jit(solution)/shard_map/ppermute | solution.py:463
  79.0 25.8 %collective-permute-start.1 = (bf16[136,2048]{1,0:T(8,128)(2,1)S(1)}, bf16[136,2048]{1,0:T(8,128)(2,1)S(1)}, u32[]{:S(2)}, u32[]{:S(2)}) collective-permute-start(bf16[136,2048]{1,0:T(8,128)(2,1)S(1)} %fusion.1.rest_0_), channel_id=1, source_target_pairs={{0,2},{2,4},{4,6},{6,0},{1,3},{3,5},{5,7},{7,1},{8,10},{10,12},{12... | collective-permute-start | bytes 1671176 | tf_op jit(solution)/shard_map/ppermute | solution.py:463
  79.3 30.8 %all-to-all-start = ((bf16[8,128,256]{2,1,0:T(8,128)(2,1)}), bf16[8,128,256]{2,1,0:T(8,128)(2,1)S(1)}, u32[]{:S(2)}, u32[]{:S(2)}) async-start(bf16[8,128,256]{2,1,0:T(8,128)(2,1)} %bitcast.7), calls=%async_computation | async-start | bytes 1048576 | tf_op jit(solution)/shard_map/all_to_all | solution.py:523
  83.9 25.8 %collective-permute-start = (bf16[136,2048]{1,0:T(8,128)(2,1)S(1)}, bf16[136,2048]{1,0:T(8,128)(2,1)}, u32[]{:S(2)}, u32[]{:S(2)}) collective-permute-start(bf16[136,2048]{1,0:T(8,128)(2,1)S(1)} %fusion.1.rest_0_), channel_id=1, source_target_pairs={{0,6},{2,0},{4,2},{6,4},{1,7},{3,1},{5,3},{7,5},{8,14},{10,8},{12,... | collective-permute-start | bytes 1671176 | tf_op jit(solution)/shard_map/ppermute | solution.py:463
  104.4 18.2 %copy-start.3 = (bf16[136,2048]{1,0:T(8,128)(2,1)}, bf16[136,2048]{1,0:T(8,128)(2,1)S(1)}, u32[]{:S(2)}) copy-start(bf16[136,2048]{1,0:T(8,128)(2,1)S(1)} %collective-permute-done.2.rest_6_) | copy-start | bytes 1671172
  104.8 17.8 %copy-start.4 = (bf16[136,2048]{1,0:T(8,128)(2,1)}, bf16[136,2048]{1,0:T(8,128)(2,1)S(1)}, u32[]{:S(2)}) copy-start(bf16[136,2048]{1,0:T(8,128)(2,1)S(1)} %collective-permute-done.1.rest_4_) | copy-start | bytes 1671172
  110.1 12.5 %collective-permute-start.14 = (bf16[136,2048]{1,0:T(8,128)(2,1)S(1)}, bf16[136,2048]{1,0:T(8,128)(2,1)S(1)}, u32[]{:S(2)}, u32[]{:S(2)}) collective-permute-start(bf16[136,2048]{1,0:T(8,128)(2,1)S(1)} %fusion.1.rest_0_), channel_id=1, source_target_pairs={{0,1},{1,0},{2,3},{3,2},{4,5},{5,4},{6,7},{7,6},{8,9},{9,8},{10,11... | collective-permute-start | bytes 1671176 | tf_op jit(solution)/shard_map/ppermute | solution.py:467
  110.6 11.9 %collective-permute-start.15 = (bf16[136,2048]{1,0:T(8,128)(2,1)}, bf16[136,2048]{1,0:T(8,128)(2,1)S(1)}, u32[]{:S(2)}, u32[]{:S(2)}) collective-permute-start(bf16[136,2048]{1,0:T(8,128)(2,1)} %collective-permute-done.rest_2_), channel_id=1, source_target_pairs={{0,1},{1,0},{2,3},{3,2},{4,5},{5,4},{6,7},{7,6},{8,9},{9,8},{10,11... | collective-permute-start | bytes 1671176 | tf_op jit(solution)/shard_map/ppermute | solution.py:467
  110.7 11.8 %collective-permute-start.16 = (bf16[136,2048]{1,0:T(8,128)(2,1)S(1)}, bf16[136,2048]{1,0:T(8,128)(2,1)S(1)}, u32[]{:S(2)}, u32[]{:S(2)}) collective-permute-start(bf16[136,2048]{1,0:T(8,128)(2,1)S(1)} %collective-permute-done.1.rest_4_), channel_id=1, source_target_pairs={{0,1},{1,0},{2,3},{3,2},{4,5},{5,4},{6,7},{7,6},{8,9},{9,8},{10,11... | collective-permute-start | bytes 1671176 | tf_op jit(solution)/shard_map/ppermute | solution.py:467
  111.1 11.4 %collective-permute-start.17 = (bf16[136,2048]{1,0:T(8,128)(2,1)S(1)}, bf16[136,2048]{1,0:T(8,128)(2,1)S(1)}, u32[]{:S(2)}, u32[]{:S(2)}) collective-permute-start(bf16[136,2048]{1,0:T(8,128)(2,1)S(1)} %collective-permute-done.2.rest_6_), channel_id=1, source_target_pairs={{0,1},{1,0},{2,3},{3,2},{4,5},{5,4},{6,7},{7,6},{8,9},{9,8},{10,11... | collective-permute-start | bytes 1671176 | tf_op jit(solution)/shard_map/ppermute | solution.py:467
  122.5 0.8 copy-start.5
  122.5 1.0 copy-start.6
  122.5 1.2 copy-start.7
  123.7 0.8 copy-start.8
  128.2 29.6 %copy-start = (bf16[128,2048]{1,0:T(8,128)(2,1)}, bf16[128,2048]{1,0:T(8,128)(2,1)S(1)}, u32[]{:S(2)}) copy-start(bf16[128,2048]{1,0:T(8,128)(2,1)S(1)} %get-tuple-element.72.rest_0_) | copy-start | bytes 1572868
  128.2 13.2 %collective-permute-start.23 = (bf16[128,2048]{1,0:T(8,128)(2,1)S(1)}, bf16[128,2048]{1,0:T(8,128)(2,1)S(1)}, u32[]{:S(2)}, u32[]{:S(2)}) collective-permute-start(bf16[128,2048]{1,0:T(8,128)(2,1)S(1)} %get-tuple-element.72.rest_0_), channel_id=1, source_target_pairs={{0,4},{2,6},{4,0},{6,2},{1,5},{3,7},{5,1},{7,3},{8,12},{10,14},{12... | collective-permute-start | bytes 1572872 | tf_op jit(solution)/shard_map/ppermute | solution.py:463
  129.4 25.5 %collective-permute-start.21 = (bf16[128,2048]{1,0:T(8,128)(2,1)S(1)}, bf16[128,2048]{1,0:T(8,128)(2,1)S(1)}, u32[]{:S(2)}, u32[]{:S(2)}) collective-permute-start(bf16[128,2048]{1,0:T(8,128)(2,1)S(1)} %get-tuple-element.72.rest_0_), channel_id=1, source_target_pairs={{0,2},{2,4},{4,6},{6,0},{1,3},{3,5},{5,7},{7,1},{8,10},{10,12},{12... | collective-permute-start | bytes 1572872 | tf_op jit(solution)/shard_map/ppermute | solution.py:463
  130.0 25.4 %collective-permute-start.19 = (bf16[128,2048]{1,0:T(8,128)(2,1)S(1)}, bf16[128,2048]{1,0:T(8,128)(2,1)S(1)}, u32[]{:S(2)}, u32[]{:S(2)}) collective-permute-start(bf16[128,2048]{1,0:T(8,128)(2,1)S(1)} %get-tuple-element.72.rest_0_), channel_id=1, source_target_pairs={{0,6},{2,0},{4,2},{6,4},{1,7},{3,1},{5,3},{7,5},{8,14},{10,8},{12,... | collective-permute-start | bytes 1572872 | tf_op jit(solution)/shard_map/ppermute | solution.py:463
  132.1 23.4 %collective-permute-start.18 = (bf16[128,2048]{1,0:T(8,128)(2,1)S(1)}, bf16[128,2048]{1,0:T(8,128)(2,1)S(1)}, u32[]{:S(2)}, u32[]{:S(2)}) collective-permute-start(bf16[128,2048]{1,0:T(8,128)(2,1)S(1)} %get-tuple-element.72.rest_0_), channel_id=1, source_target_pairs={{0,1},{1,0},{2,3},{3,2},{4,5},{5,4},{6,7},{7,6},{8,9},{9,8},{10,11... | collective-permute-start | bytes 1572872 | tf_op jit(solution)/shard_map/ppermute | solution.py:467
  141.4 16.4 %copy-start.13 = (bf16[128,2048]{1,0:T(8,128)(2,1)}, bf16[128,2048]{1,0:T(8,128)(2,1)S(1)}, u32[]{:S(2)}) copy-start(bf16[128,2048]{1,0:T(8,128)(2,1)S(1)} %collective-permute-done.23.rest_6_) | copy-start | bytes 1572868
  141.4 14.1 %collective-permute-start.24 = (bf16[128,2048]{1,0:T(8,128)(2,1)S(1)}, bf16[128,2048]{1,0:T(8,128)(2,1)S(1)}, u32[]{:S(2)}, u32[]{:S(2)}) collective-permute-start(bf16[128,2048]{1,0:T(8,128)(2,1)S(1)} %collective-permute-done.23.rest_6_), channel_id=1, source_target_pairs={{0,1},{1,0},{2,3},{3,2},{4,5},{5,4},{6,7},{7,6},{8,9},{9,8},{10,11... | collective-permute-start | bytes 1572872 | tf_op jit(solution)/shard_map/ppermute | solution.py:467
  154.9 2.9 %copy-start.14 = (bf16[128,2048]{1,0:T(8,128)(2,1)}, bf16[128,2048]{1,0:T(8,128)(2,1)S(1)}, u32[]{:S(2)}) copy-start(bf16[128,2048]{1,0:T(8,128)(2,1)S(1)} %collective-permute-done.21.rest_4_) | copy-start | bytes 1572868
  154.9 2.0 collective-permute-start.22
  155.4 2.4 %copy-start.15 = (bf16[128,2048]{1,0:T(8,128)(2,1)}, bf16[128,2048]{1,0:T(8,128)(2,1)S(1)}, u32[]{:S(2)}) copy-start(bf16[128,2048]{1,0:T(8,128)(2,1)S(1)} %collective-permute-done.19.rest_2_) | copy-start | bytes 1572868
  155.4 2.4 %collective-permute-start.20 = (bf16[128,2048]{1,0:T(8,128)(2,1)S(1)}, bf16[128,2048]{1,0:T(8,128)(2,1)}, u32[]{:S(2)}, u32[]{:S(2)}) collective-permute-start(bf16[128,2048]{1,0:T(8,128)(2,1)S(1)} %collective-permute-done.19.rest_2_), channel_id=1, source_target_pairs={{0,1},{1,0},{2,3},{3,2},{4,5},{5,4},{6,7},{7,6},{8,9},{9,8},{10,11... | collective-permute-start | bytes 1572872 | tf_op jit(solution)/shard_map/ppermute | solution.py:467
  155.5 2.3 %copy-start.16 = (bf16[128,2048]{1,0:T(8,128)(2,1)}, bf16[128,2048]{1,0:T(8,128)(2,1)S(1)}, u32[]{:S(2)}) copy-start(bf16[128,2048]{1,0:T(8,128)(2,1)S(1)} %collective-permute-done.18.rest_1_) | copy-start | bytes 1572868
  155.5 2.3 %copy-start.17 = (bf16[128,2048]{1,0:T(8,128)(2,1)}, bf16[128,2048]{1,0:T(8,128)(2,1)S(1)}, u32[]{:S(2)}) copy-start(bf16[128,2048]{1,0:T(8,128)(2,1)S(1)} %collective-permute-done.24.rest_7_) | copy-start | bytes 1572868
  156.9 0.8 copy-start.18
  167.8 8.7 %collective-permute-start.26 = (bf16[1024,256]{1,0:T(8,128)(2,1)S(1)}, bf16[1024,256]{1,0:T(8,128)(2,1)S(1)}, u32[]{:S(2)}, u32[]{:S(2)}) collective-permute-start(bf16[1024,256]{1,0:T(8,128)(2,1)S(1)} %get-tuple-element.78), channel_id=1, source_target_pairs={{0,1},{1,0},{2,3},{3,2},{4,5},{5,4},{6,7},{7,6},{8,9},{9,8},{10,11... | collective-permute-start | bytes 1572872 | tf_op jit(solution)/shard_map/ppermute | solution.py:467
  172.6 5.2 %collective-permute-start.28 = (bf16[1024,256]{1,0:T(8,128)(2,1)S(1)}, bf16[1024,256]{1,0:T(8,128)(2,1)S(1)}, u32[]{:S(2)}, u32[]{:S(2)}) collective-permute-start(bf16[1024,256]{1,0:T(8,128)(2,1)S(1)} %get-tuple-element.80), channel_id=1, source_target_pairs={{0,1},{1,0},{2,3},{3,2},{4,5},{5,4},{6,7},{7,6},{8,9},{9,8},{10,11... | collective-permute-start | bytes 1572872 | tf_op jit(solution)/shard_map/ppermute | solution.py:467
  175.9 5.1 %collective-permute-start.25 = (bf16[1024,256]{1,0:T(8,128)(2,1)S(1)}, bf16[1024,256]{1,0:T(8,128)(2,1)S(1)}, u32[]{:S(2)}, u32[]{:S(2)}) collective-permute-start(bf16[1024,256]{1,0:T(8,128)(2,1)S(1)} %get-tuple-element.76), channel_id=1, source_target_pairs={{0,1},{1,0},{2,3},{3,2},{4,5},{5,4},{6,7},{7,6},{8,9},{9,8},{10,11... | collective-permute-start | bytes 1572872 | tf_op jit(solution)/shard_map/ppermute | solution.py:467
  176.4 2.3 %collective-permute-start.30 = (bf16[1024,256]{1,0:T(8,128)(2,1)S(1)}, bf16[1024,256]{1,0:T(8,128)(2,1)S(1)}, u32[]{:S(2)}, u32[]{:S(2)}) collective-permute-start(bf16[1024,256]{1,0:T(8,128)(2,1)S(1)} %get-tuple-element.82), channel_id=1, source_target_pairs={{0,1},{1,0},{2,3},{3,2},{4,5},{5,4},{6,7},{7,6},{8,9},{9,8},{10,11... | collective-permute-start | bytes 1572872 | tf_op jit(solution)/shard_map/ppermute | solution.py:467
  176.7 14.7 %collective-permute-start.27 = (bf16[1024,256]{1,0:T(8,128)(2,1)S(1)}, bf16[1024,256]{1,0:T(8,128)(2,1)S(1)}, u32[]{:S(2)}, u32[]{:S(2)}) collective-permute-start(bf16[1024,256]{1,0:T(8,128)(2,1)S(1)} %add_convert_fusion.3), channel_id=1, source_target_pairs={{0,4},{2,6},{4,0},{6,2},{1,5},{3,7},{5,1},{7,3},{8,12},{10,14},{12... | collective-permute-start | bytes 1572872 | tf_op jit(solution)/shard_map/ppermute | solution.py:463
  178.0 25.3 %collective-permute-start.29 = (bf16[1024,256]{1,0:T(8,128)(2,1)S(1)}, bf16[1024,256]{1,0:T(8,128)(2,1)S(1)}, u32[]{:S(2)}, u32[]{:S(2)}) collective-permute-start(bf16[1024,256]{1,0:T(8,128)(2,1)S(1)} %add_convert_fusion.2), channel_id=1, source_target_pairs={{0,2},{2,4},{4,6},{6,0},{1,3},{3,5},{5,7},{7,1},{8,10},{10,12},{12... | collective-permute-start | bytes 1572872 | tf_op jit(solution)/shard_map/ppermute | solution.py:463
  178.8 24.5 %collective-permute-start.31 = (bf16[1024,256]{1,0:T(8,128)(2,1)S(1)}, bf16[1024,256]{1,0:T(8,128)(2,1)S(1)}, u32[]{:S(2)}, u32[]{:S(2)}) collective-permute-start(bf16[1024,256]{1,0:T(8,128)(2,1)S(1)} %add_convert_fusion.1), channel_id=1, source_target_pairs={{0,6},{2,0},{4,2},{6,4},{1,7},{3,1},{5,3},{7,5},{8,14},{10,8},{12,... | collective-permute-start | bytes 1572872 | tf_op jit(solution)/shard_map/ppermute | solution.py:463
Sparse Core Ops, SparseCore 0:
  38.9 76.9 all-gather.1

commit v5 on v4

--- a/solution.py
+++ b/solution.py
@@ -26,6 +26,10 @@
 
 def in_hbm(arrays):
     return [pltpu.with_memory_space_constraint(a, pltpu.HBM) for a in arrays]
+
+
+def near_in_hbm(arrays):
+    return [pltpu.with_memory_space_constraint(a, pltpu.HBM) if n % 2 == 0 else a for n, a in enumerate(arrays)]
 
 
 def pack_kernel(tab, *rest):
@@ -303,7 +307,7 @@
         out_shape=out_shape,
         in_specs=[pl.BlockSpec(memory_space=pltpu.SMEM)] * 2
         + [vmem]
-        + [pl.BlockSpec(memory_space=pltpu.HBM)] * n_arr
+        + [pl.BlockSpec(memory_space=pl.ANY)] * n_arr
         + [vmem] * len(state),
         out_specs=out_specs,
         scratch_shapes=scratch,
@@ -312,7 +316,7 @@
             flops=4_000_000_000 * n_arr, bytes_accessed=1_000_000 * n_arr, transcendentals=0
         ),
         name="attend_first" if first else ("attend_last" if last else "attend_more"),
-    )(table, zeros_q, qt, *in_hbm(arrays), *state)
+    )(table, zeros_q, qt, *near_in_hbm(arrays), *state)
 
 
 def dense_kernel(sc, att_ref, res_ref, *rest):
@@ -401,7 +405,7 @@
             jax.ShapeDtypeStruct((1024, 256), jnp.bfloat16),
             jax.ShapeDtypeStruct((1024, 256), jnp.bfloat16),
         ],
-        in_specs=[pl.BlockSpec(memory_space=pltpu.SMEM), vmem] + [pl.BlockSpec(memory_space=pltpu.HBM)] * 9,
+        in_specs=[pl.BlockSpec(memory_space=pltpu.SMEM), vmem] + [pl.BlockSpec(memory_space=pl.ANY)] * 9,
         out_specs=[vmem] * 4,
         scratch_shapes=[
             pltpu.VMEM((D, 1024), jnp.bfloat16),
@@ -413,7 +417,7 @@
         compiler_params=pltpu.CompilerParams(vmem_limit_bytes=40 * 1024 * 1024),
         cost_estimate=pl.CostEstimate(flops=5_400_000_000, bytes_accessed=8_000_000, transcendentals=0),
         name="up",
-    )(scalars, gain, *in_hbm([w, *mids]))
+    )(scalars, gain, *in_hbm([w]), *near_in_hbm(mids))
 
 
 def down_kernel(steps, sc, h_ref, w_in, *rest):

time: 213 us -> 212 us (level)
  no operation moved by 1% of the time
where the time goes in v5:
time: 212 us; the launch traced here: 211 us
  waiting for transfers between devices  86.7 us (41%)
  Pallas kernels  48.2 us (23%)
  starting transfers between devices  44.1 us (21%)
  between operations  13.7 us (6%)
  blocking collectives  11.4 us (5%)
  other arithmetic  3.61 us (2%)
  local copies, waits for them, and re-layouts  2.96 us (1%)
    ppermute x12, waiting for transfers between devices, shifted(): return lax.ppermute(value, axis, [(i, (i - by) % n) for i in range(n)])  76.7 us
    pallas_call x2, Pallas kernels, attend(): pl.pallas_call(functools.partial(attend_kernel, n_arr, first, last), out_...  25.7 us
    ppermute x12, starting transfers between devices, shifted(): return lax.ppermute(value, axis, [(i, (i - by) % n) for i in range(n)])  15.9 us
    ppermute x16, starting transfers between devices, partner(): return lax.ppermute(value, 'c', [(0, 1), (1, 0)])  14.4 us
    all_to_all x1, blocking collectives, body(): attended = lax.all_to_all(out, ('x', 'z'), 0, 0, tiled=True)  11.4 us
    pallas_call x1, Pallas kernels, up(): pl.pallas_call(up_kernel, out_shape=[jax.ShapeDtypeStruct((1024, 1024), j...  9.44 us
    ppermute x4, starting transfers between devices, body(): received.append(lax.ppermute(messages[step], ('z', 'c'), pairs))  9.22 us
    pallas_call x2, Pallas kernels, down(): pl.pallas_call(functools.partial(down_kernel, steps), out_shape=[jax.Shap...  7.43 us
  transfers between devices with their start and end apart: 34, of which 17 were waited for; matrix products, arithmetic and copies ran while one was open for 1% of the time, Pallas kernels for 14%

profile of v5, /device:TPU:25, one launch (start us, length us, event | category | flops | bytes accessed | tf_op | source)
XLA Modules:
  0.0 210.7 jit_solution(8007924301301118765)
XLA Ops:
  6.5 0.7 dynamic-slice_bitcast_fusion.tab.sc
  7.2 2.1 pack.1
  9.3 6.1 %collective-permute-start.3 = (bf16[800,128]{1,0:T(8,128)(2,1)S(1)}, bf16[800,128]{1,0:T(8,128)(2,1)S(1)}, u32[]{:S(2)}, u32[]{:S(2)}) collective-permute-start(bf16[800,128]{1,0:T(8,128)(2,1)S(1)} %get-tuple-element.44), channel_id=1, source_target_pairs={{0,0},{1,64},{32,32},{33,96},{64,1},{65,65},{96,33},{97,97},{2,2},... | collective-permute-start | bytes 614408 | tf_op jit(solution)/shard_map/ppermute | solution.py:509
  15.4 0.3 collective-permute-start.4
  15.6 2.9 %collective-permute-start.6 = (bf16[800,128]{1,0:T(8,128)(2,1)S(1)}, bf16[800,128]{1,0:T(8,128)(2,1)S(1)}, u32[]{:S(2)}, u32[]{:S(2)}) collective-permute-start(bf16[800,128]{1,0:T(8,128)(2,1)S(1)} %get-tuple-element.47), channel_id=1, source_target_pairs={{0,33},{1,97},{32,1},{33,65},{64,32},{65,96},{96,0},{97,64},{2,35}... | collective-permute-start | bytes 614408 | tf_op jit(solution)/shard_map/ppermute | solution.py:509
  18.5 1.9 collective-permute-done.3
  20.5 4.4 %collective-permute-done.4 = bf16[800,128]{1,0:T(8,128)(2,1)S(1)} collective-permute-done((bf16[800,128]{1,0:T(8,128)(2,1)S(1)}, bf16[800,128]{1,0:T(8,128)(2,1)S(1)}, u32[]{:S(2)}, u32[]{:S(2)}) %collective-permute-start.4) | collective-permute-done | bytes 204832 | tf_op jit(solution)/shard_map/ppermute | solution.py:509
  25.0 0.1 copy.12
  25.2 2.8 %collective-permute-start.10 = (bf16[4,544,128]{2,1,0:T(8,128)(2,1)S(1)}, bf16[4,544,128]{2,1,0:T(8,128)(2,1)S(1)}, u32[]{:S(2)}, u32[]{:S(2)}) collective-permute-start(bf16[4,544,128]{2,1,0:T(8,128)(2,1)S(1)} %pad_maximum_fusion.rest_0_), channel_id=1, source_target_pairs={{0,1},{1,0},{2,3},{3,2},{4,5},{5,4},{6,7},{7,6},{8,9},{9,8},{10,11... | collective-permute-start | bytes 1671176 | tf_op jit(solution)/shard_map/ppermute | solution.py:471
  28.0 0.1 convert_reduce_fusion
  28.2 0.8 pad_maximum_fusion.1
  29.0 0.5 collective-permute-done.10.rest_1_
  29.5 8.2 %attend_first.1 = (f32[4,1,512]{2,1,0:T(1,128)S(1)}, f32[4,1,512]{2,1,0:T(1,128)S(1)}, f32[4,64,512]{2,1,0:T(8,128)S(1)}) custom-call(s32[44]{0:T(128)S(1)} %dynamic-slice_bitcast_fusion.tab.sc, s32[4]{0:T(128)S(1)} %subtract_convert_fusion.zeros_q, bf16[4,256,128]{2,1,0:T(8,128)(2,1)S(1)} %pad_maximum_fusion.2.qt_ref, bf16[4,544,128]{2,1,0:T(8,128)(2,1)} %copy-done.1, ...), custom_call_target="tpu_custom_call" | custom-call | flops 8000000000 | bytes 2000000 | tf_op jit(solution)/shard_map/attend_first/pallas_call | solution.py:305
  37.8 1.4 collective-permute-start.9
  39.2 1.5 collective-permute-start.8
  40.7 16.9 %collective-permute-done.9.rest_4_ = bf16[4,544,128]{2,1,0:T(8,128)(2,1)} collective-permute-done((bf16[4,544,128]{2,1,0:T(8,128)(2,1)}, bf16[4,544,128]{2,1,0:T(8,128)(2,1)}, u32[]{:S(2)}, u32[]{:S(2)}) %collective-permute-start.9) | collective-permute-done | bytes 557088 | tf_op jit(solution)/shard_map/ppermute | solution.py:467
  57.6 14.7 %collective-permute-done.8.rest_2_ = bf16[4,544,128]{2,1,0:T(8,128)(2,1)} collective-permute-done((bf16[4,544,128]{2,1,0:T(8,128)(2,1)}, bf16[4,544,128]{2,1,0:T(8,128)(2,1)}, u32[]{:S(2)}, u32[]{:S(2)}) %collective-permute-start.8) | collective-permute-done | bytes 557088 | tf_op jit(solution)/shard_map/ppermute | solution.py:467
  72.3 1.8 collective-permute-done.7.rest_0_
  74.2 0.4 collective-permute-start.11
  74.6 0.1 collective-permute-start.12
  74.7 0.4 collective-permute-start.13
  75.1 0.9 fusion.1.rest_0_
  76.0 2.7 %collective-permute-start.2 = (bf16[136,2048]{1,0:T(8,128)(2,1)}, bf16[136,2048]{1,0:T(8,128)(2,1)}, u32[]{:S(2)}, u32[]{:S(2)}) collective-permute-start(bf16[136,2048]{1,0:T(8,128)(2,1)} %fusion.1.rest_0_), channel_id=1, source_target_pairs={{0,4},{2,6},{4,0},{6,2},{1,5},{3,7},{5,1},{7,3},{8,12},{10,14},{12... | collective-permute-start | bytes 1671176 | tf_op jit(solution)/shard_map/ppermute | solution.py:467
  78.7 0.3 collective-permute-start.1
  79.0 4.6 %all-to-all-start = ((bf16[8,128,256]{2,1,0:T(8,128)(2,1)}), bf16[8,128,256]{2,1,0:T(8,128)(2,1)S(1)}, u32[]{:S(2)}, u32[]{:S(2)}) async-start(bf16[8,128,256]{2,1,0:T(8,128)(2,1)} %bitcast.7), calls=%async_computation | async-start | bytes 1048576 | tf_op jit(solution)/shard_map/all_to_all | solution.py:527
  83.6 2.6 %collective-permute-start = (bf16[136,2048]{1,0:T(8,128)(2,1)}, bf16[136,2048]{1,0:T(8,128)(2,1)}, u32[]{:S(2)}, u32[]{:S(2)}) collective-permute-start(bf16[136,2048]{1,0:T(8,128)(2,1)} %fusion.1.rest_0_), channel_id=1, source_target_pairs={{0,6},{2,0},{4,2},{6,4},{1,7},{3,1},{5,3},{7,5},{8,14},{10,8},{12,... | collective-permute-start | bytes 1671176 | tf_op jit(solution)/shard_map/ppermute | solution.py:467
  86.2 17.5 %attend_last.1 = bf16[16,64,128]{2,1,0:T(8,128)(2,1)S(1)} custom-call(s32[44]{0:T(128)S(1)} %dynamic-slice_bitcast_fusion.tab.sc, s32[4]{0:T(128)S(1)} %subtract_convert_fusion.zeros_q, bf16[4,256,128]{2,1,0:T(8,128)(2,1)S(1)} %pad_maximum_fusion.2.qt_ref, bf16[4,544,128]{2,1,0:T(8,128)(2,1)} %collective-permute-done.7.rest_0_, ...), custom_call_target="tpu_custom_call" | custom-call | flops 24000000000 | bytes 6000000 | tf_op jit(solution)/shard_map/attend_last/pallas_call | solution.py:305
  103.7 1.1 collective-permute-done.1.rest_4_
  104.7 4.9 %collective-permute-done.rest_2_ = bf16[136,2048]{1,0:T(8,128)(2,1)} collective-permute-done((bf16[136,2048]{1,0:T(8,128)(2,1)}, bf16[136,2048]{1,0:T(8,128)(2,1)}, u32[]{:S(2)}, u32[]{:S(2)}) %collective-permute-start) | collective-permute-done | bytes 557088 | tf_op jit(solution)/shard_map/ppermute | solution.py:467
  109.6 0.4 all-to-all-done.res_ref
  110.0 0.6 collective-permute-start.14
  110.6 0.5 collective-permute-start.16
  111.1 11.4 %all_to_all.10.att_ref = bf16[16,64,128]{2,1,0:T(8,128)(2,1)S(1)} all-to-all(bf16[16,64,128]{2,1,0:T(8,128)(2,1)S(1)} %attend_last.1), channel_id=1, replica_groups=mesh['z'=4,'y'=4,'x'=4,'c'=2] {'x','z'}, dimensions={0} | all-to-all | bytes 524288 | tf_op jit(solution)/shard_map/all_to_all | solution.py:538
  122.5 0.8 copy-done.2
  123.3 0.2 copy-done.3
  123.5 0.2 copy-done.4
  123.7 0.8 copy-done.5
  124.5 3.6 %dense.1 = (bf16[128,2048]{1,0:T(8,128)(2,1)S(1)}, bf16[8,2048]{1,0:T(8,128)(2,1)S(1)}) custom-call(s32[44]{0:T(128)S(1)} %dynamic-slice_bitcast_fusion.tab.sc, bf16[16,64,128]{2,1,0:T(8,128)(2,1)S(1)} %all_to_all.10.att_ref, bf16[8,128,256]{2,1,0:T(8,128)(2,1)S(1)} %all-to-all-done.res_ref, bf16[136,2048]{1,0:T(8,128)(2,1)} %fusion.1.rest_0_, ...), custom_call_target="tpu_custom_call" | custom-call | flops 1000000000 | bytes 4000000 | tf_op jit(solution)/shard_map/dense/pallas_call | solution.py:348
  128.2 1.2 collective-permute-start.23
  129.4 0.6 collective-permute-start.21
  130.0 2.1 collective-permute-start.19
  132.1 2.6 %collective-permute-start.18 = (bf16[128,2048]{1,0:T(8,128)(2,1)S(1)}, bf16[128,2048]{1,0:T(8,128)(2,1)S(1)}, u32[]{:S(2)}, u32[]{:S(2)}) collective-permute-start(bf16[128,2048]{1,0:T(8,128)(2,1)S(1)} %get-tuple-element.72.rest_0_), channel_id=1, source_target_pairs={{0,1},{1,0},{2,3},{3,2},{4,5},{5,4},{6,7},{7,6},{8,9},{9,8},{10,11... | collective-permute-start | bytes 1572872 | tf_op jit(solution)/shard_map/ppermute | solution.py:471
  134.7 6.7 %collective-permute-done.23.rest_6_ = bf16[128,2048]{1,0:T(8,128)(2,1)S(1)} collective-permute-done((bf16[128,2048]{1,0:T(8,128)(2,1)S(1)}, bf16[128,2048]{1,0:T(8,128)(2,1)S(1)}, u32[]{:S(2)}, u32[]{:S(2)}) %collective-permute-start.23) | collective-permute-done | bytes 524320 | tf_op jit(solution)/shard_map/ppermute | solution.py:467
  141.4 5.2 %collective-permute-start.24 = (bf16[128,2048]{1,0:T(8,128)(2,1)S(1)}, bf16[128,2048]{1,0:T(8,128)(2,1)S(1)}, u32[]{:S(2)}, u32[]{:S(2)}) collective-permute-start(bf16[128,2048]{1,0:T(8,128)(2,1)S(1)} %collective-permute-done.23.rest_6_), channel_id=1, source_target_pairs={{0,1},{1,0},{2,3},{3,2},{4,5},{5,4},{6,7},{7,6},{8,9},{9,8},{10,11... | collective-permute-start | bytes 1572872 | tf_op jit(solution)/shard_map/ppermute | solution.py:471
  146.5 8.3 %collective-permute-done.21.rest_4_ = bf16[128,2048]{1,0:T(8,128)(2,1)S(1)} collective-permute-done((bf16[128,2048]{1,0:T(8,128)(2,1)S(1)}, bf16[128,2048]{1,0:T(8,128)(2,1)S(1)}, u32[]{:S(2)}, u32[]{:S(2)}) %collective-permute-start.21) | collective-permute-done | bytes 524320 | tf_op jit(solution)/shard_map/ppermute | solution.py:467
  154.8 0.5 collective-permute-start.22
  155.4 1.4 collective-permute-done.22.rest_5_
  156.9 0.7 collective-permute-done.20.rest_3_
  157.6 9.4 %up.1 = (bf16[1024,1024]{1,0:T(8,128)(2,1)S(1)}, bf16[1024,256]{1,0:T(8,128)(2,1)S(1)}, bf16[1024,256]{1,0:T(8,128)(2,1)S(1)}, bf16[1024,256]{1,0:T(8,128)(2,1)S(1)}) custom-call(s32[44]{0:T(128)S(1)} %dynamic-slice_bitcast_fusion.tab.sc, bf16[8,2048]{1,0:T(8,128)(2,1)S(1)} %get-tuple-element.70.gain_ref, ...), custom_call_target="tpu_custom_call" | custom-call | flops 5400000000 | bytes 8000000 | tf_op jit(solution)/shard_map/up/pallas_call | solution.py:400
  167.1 0.4 collective-permute-start.26
  167.5 4.4 %down.3 = (bf16[1024,256]{1,0:T(8,128)(2,1)S(1)}, bf16[1024,256]{1,0:T(8,128)(2,1)S(1)}, bf16[1024,256]{1,0:T(8,128)(2,1)S(1)}, bf16[1024,256]{1,0:T(8,128)(2,1)S(1)}) custom-call(s32[44]{0:T(128)S(1)} %dynamic-slice_bitcast_fusion.tab.sc, bf16[1024,1024]{1,0:T(8,128)(2,1)S(1)} %get-tuple-element.74.h_ref, bf16[4096,1024]{1,0:T(8,128)(2,1)} %all-gather.2.cloned.1.call-done.w_in), custom_call_target="tpu_custom_call" | custom-call | flops 2200000000 | bytes 4000000 | tf_op jit(solution)/shard_map/down/pallas_call | solution.py:451
  171.9 0.2 collective-permute-start.28
  172.1 3.1 %down.2 = (bf16[1024,256]{1,0:T(8,128)(2,1)S(1)}, bf16[1024,256]{1,0:T(8,128)(2,1)S(1)}) custom-call(s32[44]{0:T(128)S(1)} %dynamic-slice_bitcast_fusion.tab.sc, bf16[1024,1024]{1,0:T(8,128)(2,1)S(1)} %get-tuple-element.74.h_ref, bf16[4096,1024]{1,0:T(8,128)(2,1)} %all-gather.2.cloned.1.call-done.w_in), custom_call_target="tpu_custom_call" | custom-call | flops 1100000000 | bytes 4000000 | tf_op jit(solution)/shard_map/down/pallas_call | solution.py:451
  175.2 0.5 collective-permute-start.25
  175.6 0.1 collective-permute-start.30
  175.8 0.1 add_convert_fusion.3
  175.9 1.2 collective-permute-start.27
  177.1 0.1 add_convert_fusion.2
  177.4 0.6 collective-permute-done.30
  177.9 0.2 add_convert_fusion.1
  178.1 2.2 %collective-permute-start.31 = (bf16[1024,256]{1,0:T(8,128)(2,1)S(1)}, bf16[1024,256]{1,0:T(8,128)(2,1)S(1)}, u32[]{:S(2)}, u32[]{:S(2)}) collective-permute-start(bf16[1024,256]{1,0:T(8,128)(2,1)S(1)} %add_convert_fusion.1), channel_id=1, source_target_pairs={{0,6},{2,0},{4,2},{6,4},{1,7},{3,1},{5,3},{7,5},{8,14},{10,8},{12,... | collective-permute-start | bytes 1572872 | tf_op jit(solution)/shard_map/ppermute | solution.py:467
  180.3 10.4 %collective-permute-done.27 = bf16[1024,256]{1,0:T(8,128)(2,1)S(1)} collective-permute-done((bf16[1024,256]{1,0:T(8,128)(2,1)S(1)}, bf16[1024,256]{1,0:T(8,128)(2,1)S(1)}, u32[]{:S(2)}, u32[]{:S(2)}) %collective-permute-start.27) | collective-permute-done | bytes 524320 | tf_op jit(solution)/shard_map/ppermute | solution.py:467
  190.7 11.9 %collective-permute-done.29 = bf16[1024,256]{1,0:T(8,128)(2,1)S(1)} collective-permute-done((bf16[1024,256]{1,0:T(8,128)(2,1)S(1)}, bf16[1024,256]{1,0:T(8,128)(2,1)S(1)}, u32[]{:S(2)}, u32[]{:S(2)}) %collective-permute-start.29) | collective-permute-done | bytes 524320 | tf_op jit(solution)/shard_map/ppermute | solution.py:467
  202.6 1.2 add_convert_fusion
  (60 shorter events, 0.5 us)
Async XLA Ops:
  6.5 151.1 %all-gather.2.cloned.1.call-start = ((), (), s32[]{:S(2)}) async-start(), calls=%async_computation.2 | async-start | bytes 8912896 | tf_op jit(solution)/shard_map/all_gather | solution.py:529
  9.3 11.1 %collective-permute-start.3 = (bf16[800,128]{1,0:T(8,128)(2,1)S(1)}, bf16[800,128]{1,0:T(8,128)(2,1)S(1)}, u32[]{:S(2)}, u32[]{:S(2)}) collective-permute-start(bf16[800,128]{1,0:T(8,128)(2,1)S(1)} %get-tuple-element.44), channel_id=1, source_target_pairs={{0,0},{1,64},{32,32},{33,96},{64,1},{65,65},{96,33},{97,97},{2,2},... | collective-permute-start | bytes 614408 | tf_op jit(solution)/shard_map/ppermute | solution.py:509
  15.4 9.4 %collective-permute-start.4 = (bf16[800,128]{1,0:T(8,128)(2,1)S(1)}, bf16[800,128]{1,0:T(8,128)(2,1)S(1)}, u32[]{:S(2)}, u32[]{:S(2)}) collective-permute-start(bf16[800,128]{1,0:T(8,128)(2,1)S(1)} %get-tuple-element.45), channel_id=1, source_target_pairs={{0,32},{1,96},{32,0},{33,64},{64,33},{65,97},{96,1},{97,65},{2,34}... | collective-permute-start | bytes 614408 | tf_op jit(solution)/shard_map/ppermute | solution.py:509
  15.6 9.2 %collective-permute-start.5 = (bf16[800,128]{1,0:T(8,128)(2,1)S(1)}, bf16[800,128]{1,0:T(8,128)(2,1)S(1)}, u32[]{:S(2)}, u32[]{:S(2)}) collective-permute-start(bf16[800,128]{1,0:T(8,128)(2,1)S(1)} %get-tuple-element.46), channel_id=1, source_target_pairs={{0,1},{1,65},{32,33},{33,97},{64,0},{65,64},{96,32},{97,96},{2,3},... | collective-permute-start | bytes 614408 | tf_op jit(solution)/shard_map/ppermute | solution.py:509
  15.6 9.4 %copy-start.7 = (bf16[1024,128]{1,0:T(8,128)(2,1)S(1)}, bf16[1024,128]{1,0:T(8,128)(2,1)}, u32[]{:S(2)}) copy-start(bf16[1024,128]{1,0:T(8,128)(2,1)} %param.20) | copy-start | bytes 786436
  15.6 9.3 %collective-permute-start.6 = (bf16[800,128]{1,0:T(8,128)(2,1)S(1)}, bf16[800,128]{1,0:T(8,128)(2,1)S(1)}, u32[]{:S(2)}, u32[]{:S(2)}) collective-permute-start(bf16[800,128]{1,0:T(8,128)(2,1)S(1)} %get-tuple-element.47), channel_id=1, source_target_pairs={{0,33},{1,97},{32,1},{33,65},{64,32},{65,96},{96,0},{97,64},{2,35}... | collective-permute-start | bytes 614408 | tf_op jit(solution)/shard_map/ppermute | solution.py:509
  24.9 3.2 %copy-start.8 = (bf16[128,1024]{1,0:T(8,128)(2,1)S(1)}, bf16[128,1024]{1,0:T(8,128)(2,1)}, u32[]{:S(2)}) copy-start(bf16[128,1024]{1,0:T(8,128)(2,1)} %param.19) | copy-start | bytes 786436
  25.0 4.5 %copy-start.1 = (bf16[4,544,128]{2,1,0:T(8,128)(2,1)}, bf16[4,544,128]{2,1,0:T(8,128)(2,1)S(1)}, u32[]{:S(2)}) copy-start(bf16[4,544,128]{2,1,0:T(8,128)(2,1)S(1)} %pad_maximum_fusion.rest_0_) | copy-start | bytes 1671172
  25.2 4.3 %collective-permute-start.10 = (bf16[4,544,128]{2,1,0:T(8,128)(2,1)S(1)}, bf16[4,544,128]{2,1,0:T(8,128)(2,1)S(1)}, u32[]{:S(2)}, u32[]{:S(2)}) collective-permute-start(bf16[4,544,128]{2,1,0:T(8,128)(2,1)S(1)} %pad_maximum_fusion.rest_0_), channel_id=1, source_target_pairs={{0,1},{1,0},{2,3},{3,2},{4,5},{5,4},{6,7},{7,6},{8,9},{9,8},{10,11... | collective-permute-start | bytes 1671176 | tf_op jit(solution)/shard_map/ppermute | solution.py:471
  29.0 46.1 %copy-start.12 = (bf16[256]{0:T(256)(128)(2,1)S(1)}, bf16[256]{0:T(256)(128)(2,1)}, u32[]{:S(2)}) copy-start(bf16[256]{0:T(256)(128)(2,1)} %param.18) | copy-start | bytes 1540
  29.0 46.1 %copy-start.6 = (bf16[128,2048]{1,0:T(8,128)(2,1)S(1)}, bf16[128,2048]{1,0:T(8,128)(2,1)}, u32[]{:S(2)}) copy-start(bf16[128,2048]{1,0:T(8,128)(2,1)} %param.17) | copy-start | bytes 1572868
  37.8 19.8 %collective-permute-start.9 = (bf16[4,544,128]{2,1,0:T(8,128)(2,1)}, bf16[4,544,128]{2,1,0:T(8,128)(2,1)}, u32[]{:S(2)}, u32[]{:S(2)}) collective-permute-start(bf16[4,544,128]{2,1,0:T(8,128)(2,1)} %copy-done.1), channel_id=1, source_target_pairs={{0,16},{8,24},{16,0},{24,8},{1,17},{9,25},{17,1},{25,9},{2,18},{10... | collective-permute-start | bytes 1671176 | tf_op jit(solution)/shard_map/ppermute | solution.py:467
  39.2 33.1 %collective-permute-start.8 = (bf16[4,544,128]{2,1,0:T(8,128)(2,1)}, bf16[4,544,128]{2,1,0:T(8,128)(2,1)}, u32[]{:S(2)}, u32[]{:S(2)}) collective-permute-start(bf16[4,544,128]{2,1,0:T(8,128)(2,1)} %copy-done.1), channel_id=1, source_target_pairs={{0,8},{8,16},{16,24},{24,0},{1,9},{9,17},{17,25},{25,1},{2,10},{10... | collective-permute-start | bytes 1671176 | tf_op jit(solution)/shard_map/ppermute | solution.py:467
  40.7 33.5 %collective-permute-start.7 = (bf16[4,544,128]{2,1,0:T(8,128)(2,1)}, bf16[4,544,128]{2,1,0:T(8,128)(2,1)}, u32[]{:S(2)}, u32[]{:S(2)}) collective-permute-start(bf16[4,544,128]{2,1,0:T(8,128)(2,1)} %copy-done.1), channel_id=1, source_target_pairs={{0,24},{8,0},{16,8},{24,16},{1,25},{9,1},{17,9},{25,17},{2,26},{10... | collective-permute-start | bytes 1671176 | tf_op jit(solution)/shard_map/ppermute | solution.py:467
  74.2 9.4 %collective-permute-start.11 = (bf16[4,544,128]{2,1,0:T(8,128)(2,1)}, bf16[4,544,128]{2,1,0:T(8,128)(2,1)S(1)}, u32[]{:S(2)}, u32[]{:S(2)}) collective-permute-start(bf16[4,544,128]{2,1,0:T(8,128)(2,1)} %collective-permute-done.7.rest_0_), channel_id=1, source_target_pairs={{0,1},{1,0},{2,3},{3,2},{4,5},{5,4},{6,7},{7,6},{8,9},{9,8},{10,11... | collective-permute-start | bytes 1671176 | tf_op jit(solution)/shard_map/ppermute | solution.py:471
  74.6 11.6 %collective-permute-start.12 = (bf16[4,544,128]{2,1,0:T(8,128)(2,1)}, bf16[4,544,128]{2,1,0:T(8,128)(2,1)S(1)}, u32[]{:S(2)}, u32[]{:S(2)}) collective-permute-start(bf16[4,544,128]{2,1,0:T(8,128)(2,1)} %collective-permute-done.8.rest_2_), channel_id=1, source_target_pairs={{0,1},{1,0},{2,3},{3,2},{4,5},{5,4},{6,7},{7,6},{8,9},{9,8},{10,11... | collective-permute-start | bytes 1671176 | tf_op jit(solution)/shard_map/ppermute | solution.py:471
  74.7 11.5 %collective-permute-start.13 = (bf16[4,544,128]{2,1,0:T(8,128)(2,1)}, bf16[4,544,128]{2,1,0:T(8,128)(2,1)S(1)}, u32[]{:S(2)}, u32[]{:S(2)}) collective-permute-start(bf16[4,544,128]{2,1,0:T(8,128)(2,1)} %collective-permute-done.9.rest_4_), channel_id=1, source_target_pairs={{0,1},{1,0},{2,3},{3,2},{4,5},{5,4},{6,7},{7,6},{8,9},{9,8},{10,11... | collective-permute-start | bytes 1671176 | tf_op jit(solution)/shard_map/ppermute | solution.py:471
  76.0 27.7 %collective-permute-start.2 = (bf16[136,2048]{1,0:T(8,128)(2,1)}, bf16[136,2048]{1,0:T(8,128)(2,1)}, u32[]{:S(2)}, u32[]{:S(2)}) collective-permute-start(bf16[136,2048]{1,0:T(8,128)(2,1)} %fusion.1.rest_0_), channel_id=1, source_target_pairs={{0,4},{2,6},{4,0},{6,2},{1,5},{3,7},{5,1},{7,3},{8,12},{10,14},{12... | collective-permute-start | bytes 1671176 | tf_op jit(solution)/shard_map/ppermute | solution.py:467
  78.7 26.0 %collective-permute-start.1 = (bf16[136,2048]{1,0:T(8,128)(2,1)}, bf16[136,2048]{1,0:T(8,128)(2,1)}, u32[]{:S(2)}, u32[]{:S(2)}) collective-permute-start(bf16[136,2048]{1,0:T(8,128)(2,1)} %fusion.1.rest_0_), channel_id=1, source_target_pairs={{0,2},{2,4},{4,6},{6,0},{1,3},{3,5},{5,7},{7,1},{8,10},{10,12},{12... | collective-permute-start | bytes 1671176 | tf_op jit(solution)/shard_map/ppermute | solution.py:467
  79.0 31.0 %all-to-all-start = ((bf16[8,128,256]{2,1,0:T(8,128)(2,1)}), bf16[8,128,256]{2,1,0:T(8,128)(2,1)S(1)}, u32[]{:S(2)}, u32[]{:S(2)}) async-start(bf16[8,128,256]{2,1,0:T(8,128)(2,1)} %bitcast.7), calls=%async_computation | async-start | bytes 1048576 | tf_op jit(solution)/shard_map/all_to_all | solution.py:527
  83.6 26.0 %collective-permute-start = (bf16[136,2048]{1,0:T(8,128)(2,1)}, bf16[136,2048]{1,0:T(8,128)(2,1)}, u32[]{:S(2)}, u32[]{:S(2)}) collective-permute-start(bf16[136,2048]{1,0:T(8,128)(2,1)} %fusion.1.rest_0_), channel_id=1, source_target_pairs={{0,6},{2,0},{4,2},{6,4},{1,7},{3,1},{5,3},{7,5},{8,14},{10,8},{12,... | collective-permute-start | bytes 1671176 | tf_op jit(solution)/shard_map/ppermute | solution.py:467
  110.0 12.5 %collective-permute-start.14 = (bf16[136,2048]{1,0:T(8,128)(2,1)}, bf16[136,2048]{1,0:T(8,128)(2,1)S(1)}, u32[]{:S(2)}, u32[]{:S(2)}) collective-permute-start(bf16[136,2048]{1,0:T(8,128)(2,1)} %fusion.1.rest_0_), channel_id=1, source_target_pairs={{0,1},{1,0},{2,3},{3,2},{4,5},{5,4},{6,7},{7,6},{8,9},{9,8},{10,11... | collective-permute-start | bytes 1671176 | tf_op jit(solution)/shard_map/ppermute | solution.py:471
  110.6 11.9 %collective-permute-start.15 = (bf16[136,2048]{1,0:T(8,128)(2,1)}, bf16[136,2048]{1,0:T(8,128)(2,1)S(1)}, u32[]{:S(2)}, u32[]{:S(2)}) collective-permute-start(bf16[136,2048]{1,0:T(8,128)(2,1)} %collective-permute-done.rest_2_), channel_id=1, source_target_pairs={{0,1},{1,0},{2,3},{3,2},{4,5},{5,4},{6,7},{7,6},{8,9},{9,8},{10,11... | collective-permute-start | bytes 1671176 | tf_op jit(solution)/shard_map/ppermute | solution.py:471
  110.6 11.9 %collective-permute-start.16 = (bf16[136,2048]{1,0:T(8,128)(2,1)}, bf16[136,2048]{1,0:T(8,128)(2,1)S(1)}, u32[]{:S(2)}, u32[]{:S(2)}) collective-permute-start(bf16[136,2048]{1,0:T(8,128)(2,1)} %collective-permute-done.1.rest_4_), channel_id=1, source_target_pairs={{0,1},{1,0},{2,3},{3,2},{4,5},{5,4},{6,7},{7,6},{8,9},{9,8},{10,11... | collective-permute-start | bytes 1671176 | tf_op jit(solution)/shard_map/ppermute | solution.py:471
  111.1 11.4 %collective-permute-start.17 = (bf16[136,2048]{1,0:T(8,128)(2,1)}, bf16[136,2048]{1,0:T(8,128)(2,1)S(1)}, u32[]{:S(2)}, u32[]{:S(2)}) collective-permute-start(bf16[136,2048]{1,0:T(8,128)(2,1)} %collective-permute-done.2.rest_6_), channel_id=1, source_target_pairs={{0,1},{1,0},{2,3},{3,2},{4,5},{5,4},{6,7},{7,6},{8,9},{9,8},{10,11... | collective-permute-start | bytes 1671176 | tf_op jit(solution)/shard_map/ppermute | solution.py:471
  122.5 0.8 copy-start.2
  122.5 1.0 copy-start.3
  122.5 1.2 copy-start.4
  123.7 0.8 copy-start.5
  128.2 29.5 %copy-start = (bf16[128,2048]{1,0:T(8,128)(2,1)}, bf16[128,2048]{1,0:T(8,128)(2,1)S(1)}, u32[]{:S(2)}) copy-start(bf16[128,2048]{1,0:T(8,128)(2,1)S(1)} %get-tuple-element.72.rest_0_) | copy-start | bytes 1572868
  128.2 13.2 %collective-permute-start.23 = (bf16[128,2048]{1,0:T(8,128)(2,1)S(1)}, bf16[128,2048]{1,0:T(8,128)(2,1)S(1)}, u32[]{:S(2)}, u32[]{:S(2)}) collective-permute-start(bf16[128,2048]{1,0:T(8,128)(2,1)S(1)} %get-tuple-element.72.rest_0_), channel_id=1, source_target_pairs={{0,4},{2,6},{4,0},{6,2},{1,5},{3,7},{5,1},{7,3},{8,12},{10,14},{12... | collective-permute-start | bytes 1572872 | tf_op jit(solution)/shard_map/ppermute | solution.py:467
  129.4 25.5 %collective-permute-start.21 = (bf16[128,2048]{1,0:T(8,128)(2,1)S(1)}, bf16[128,2048]{1,0:T(8,128)(2,1)S(1)}, u32[]{:S(2)}, u32[]{:S(2)}) collective-permute-start(bf16[128,2048]{1,0:T(8,128)(2,1)S(1)} %get-tuple-element.72.rest_0_), channel_id=1, source_target_pairs={{0,2},{2,4},{4,6},{6,0},{1,3},{3,5},{5,7},{7,1},{8,10},{10,12},{12... | collective-permute-start | bytes 1572872 | tf_op jit(solution)/shard_map/ppermute | solution.py:467
  130.0 25.4 %collective-permute-start.19 = (bf16[128,2048]{1,0:T(8,128)(2,1)S(1)}, bf16[128,2048]{1,0:T(8,128)(2,1)S(1)}, u32[]{:S(2)}, u32[]{:S(2)}) collective-permute-start(bf16[128,2048]{1,0:T(8,128)(2,1)S(1)} %get-tuple-element.72.rest_0_), channel_id=1, source_target_pairs={{0,6},{2,0},{4,2},{6,4},{1,7},{3,1},{5,3},{7,5},{8,14},{10,8},{12,... | collective-permute-start | bytes 1572872 | tf_op jit(solution)/shard_map/ppermute | solution.py:467
  132.1 23.4 %collective-permute-start.18 = (bf16[128,2048]{1,0:T(8,128)(2,1)S(1)}, bf16[128,2048]{1,0:T(8,128)(2,1)S(1)}, u32[]{:S(2)}, u32[]{:S(2)}) collective-permute-start(bf16[128,2048]{1,0:T(8,128)(2,1)S(1)} %get-tuple-element.72.rest_0_), channel_id=1, source_target_pairs={{0,1},{1,0},{2,3},{3,2},{4,5},{5,4},{6,7},{7,6},{8,9},{9,8},{10,11... | collective-permute-start | bytes 1572872 | tf_op jit(solution)/shard_map/ppermute | solution.py:471
  141.4 16.3 %copy-start.9 = (bf16[128,2048]{1,0:T(8,128)(2,1)}, bf16[128,2048]{1,0:T(8,128)(2,1)S(1)}, u32[]{:S(2)}) copy-start(bf16[128,2048]{1,0:T(8,128)(2,1)S(1)} %collective-permute-done.23.rest_6_) | copy-start | bytes 1572868
  141.4 14.1 %collective-permute-start.24 = (bf16[128,2048]{1,0:T(8,128)(2,1)S(1)}, bf16[128,2048]{1,0:T(8,128)(2,1)S(1)}, u32[]{:S(2)}, u32[]{:S(2)}) collective-permute-start(bf16[128,2048]{1,0:T(8,128)(2,1)S(1)} %collective-permute-done.23.rest_6_), channel_id=1, source_target_pairs={{0,1},{1,0},{2,3},{3,2},{4,5},{5,4},{6,7},{7,6},{8,9},{9,8},{10,11... | collective-permute-start | bytes 1572872 | tf_op jit(solution)/shard_map/ppermute | solution.py:471
  154.8 2.0 copy-start.10
  154.8 2.0 collective-permute-start.22
  155.3 1.5 copy-start.11
  155.3 2.3 %collective-permute-start.20 = (bf16[128,2048]{1,0:T(8,128)(2,1)S(1)}, bf16[128,2048]{1,0:T(8,128)(2,1)S(1)}, u32[]{:S(2)}, u32[]{:S(2)}) collective-permute-start(bf16[128,2048]{1,0:T(8,128)(2,1)S(1)} %collective-permute-done.19.rest_2_), channel_id=1, source_target_pairs={{0,1},{1,0},{2,3},{3,2},{4,5},{5,4},{6,7},{7,6},{8,9},{9,8},{10,11... | collective-permute-start | bytes 1572872 | tf_op jit(solution)/shard_map/ppermute | solution.py:471
  167.1 8.7 %collective-permute-start.26 = (bf16[1024,256]{1,0:T(8,128)(2,1)S(1)}, bf16[1024,256]{1,0:T(8,128)(2,1)S(1)}, u32[]{:S(2)}, u32[]{:S(2)}) collective-permute-start(bf16[1024,256]{1,0:T(8,128)(2,1)S(1)} %get-tuple-element.78), channel_id=1, source_target_pairs={{0,1},{1,0},{2,3},{3,2},{4,5},{5,4},{6,7},{7,6},{8,9},{9,8},{10,11... | collective-permute-start | bytes 1572872 | tf_op jit(solution)/shard_map/ppermute | solution.py:471
  171.9 5.2 %collective-permute-start.28 = (bf16[1024,256]{1,0:T(8,128)(2,1)S(1)}, bf16[1024,256]{1,0:T(8,128)(2,1)S(1)}, u32[]{:S(2)}, u32[]{:S(2)}) collective-permute-start(bf16[1024,256]{1,0:T(8,128)(2,1)S(1)} %get-tuple-element.80), channel_id=1, source_target_pairs={{0,1},{1,0},{2,3},{3,2},{4,5},{5,4},{6,7},{7,6},{8,9},{9,8},{10,11... | collective-permute-start | bytes 1572872 | tf_op jit(solution)/shard_map/ppermute | solution.py:471
  175.2 5.1 %collective-permute-start.25 = (bf16[1024,256]{1,0:T(8,128)(2,1)S(1)}, bf16[1024,256]{1,0:T(8,128)(2,1)S(1)}, u32[]{:S(2)}, u32[]{:S(2)}) collective-permute-start(bf16[1024,256]{1,0:T(8,128)(2,1)S(1)} %get-tuple-element.76), channel_id=1, source_target_pairs={{0,1},{1,0},{2,3},{3,2},{4,5},{5,4},{6,7},{7,6},{8,9},{9,8},{10,11... | collective-permute-start | bytes 1572872 | tf_op jit(solution)/shard_map/ppermute | solution.py:471
  175.6 2.3 %collective-permute-start.30 = (bf16[1024,256]{1,0:T(8,128)(2,1)S(1)}, bf16[1024,256]{1,0:T(8,128)(2,1)S(1)}, u32[]{:S(2)}, u32[]{:S(2)}) collective-permute-start(bf16[1024,256]{1,0:T(8,128)(2,1)S(1)} %get-tuple-element.82), channel_id=1, source_target_pairs={{0,1},{1,0},{2,3},{3,2},{4,5},{5,4},{6,7},{7,6},{8,9},{9,8},{10,11... | collective-permute-start | bytes 1572872 | tf_op jit(solution)/shard_map/ppermute | solution.py:471
  175.9 14.7 %collective-permute-start.27 = (bf16[1024,256]{1,0:T(8,128)(2,1)S(1)}, bf16[1024,256]{1,0:T(8,128)(2,1)S(1)}, u32[]{:S(2)}, u32[]{:S(2)}) collective-permute-start(bf16[1024,256]{1,0:T(8,128)(2,1)S(1)} %add_convert_fusion.3), channel_id=1, source_target_pairs={{0,4},{2,6},{4,0},{6,2},{1,5},{3,7},{5,1},{7,3},{8,12},{10,14},{12... | collective-permute-start | bytes 1572872 | tf_op jit(solution)/shard_map/ppermute | solution.py:467
  177.3 25.3 %collective-permute-start.29 = (bf16[1024,256]{1,0:T(8,128)(2,1)S(1)}, bf16[1024,256]{1,0:T(8,128)(2,1)S(1)}, u32[]{:S(2)}, u32[]{:S(2)}) collective-permute-start(bf16[1024,256]{1,0:T(8,128)(2,1)S(1)} %add_convert_fusion.2), channel_id=1, source_target_pairs={{0,2},{2,4},{4,6},{6,0},{1,3},{3,5},{5,7},{7,1},{8,10},{10,12},{12... | collective-permute-start | bytes 1572872 | tf_op jit(solution)/shard_map/ppermute | solution.py:467
  178.1 24.5 %collective-permute-start.31 = (bf16[1024,256]{1,0:T(8,128)(2,1)S(1)}, bf16[1024,256]{1,0:T(8,128)(2,1)S(1)}, u32[]{:S(2)}, u32[]{:S(2)}) collective-permute-start(bf16[1024,256]{1,0:T(8,128)(2,1)S(1)} %add_convert_fusion.1), channel_id=1, source_target_pairs={{0,6},{2,0},{4,2},{6,4},{1,7},{3,1},{5,3},{7,5},{8,14},{10,8},{12,... | collective-permute-start | bytes 1572872 | tf_op jit(solution)/shard_map/ppermute | solution.py:467
Sparse Core Ops, SparseCore 0:
  37.9 76.9 all-gather.1
